TPU v7x, 128 devices: a whole 4x4x4 slice. The times are simulated.
128 devices in a mesh: sp: 16 (over z, y), tp: 8 (over x, core).
Axes of the slice: x: 4, y: 4, z: 4, core: 2. Of those that a mesh axis runs over, the one named last changes fastest.
Arguments:
- stream_in: bfloat16 [8192, 4096], P('sp', 'tp'), may hold values from -12 to 12
- norm_gain: float32 [2, 4096], replicated, may hold values from 0.1 to 1.9
- value_proj: bfloat16 [2, 4096, 4096], P(None, 'sp', 'tp'), may hold values from -0.09375 to 0.09375
- gate_proj: bfloat16 [2, 4096, 4096], P(None, 'sp', 'tp'), may hold values from -0.09375 to 0.09375
- out_proj: bfloat16 [2, 4096, 4096], P(None, 'sp', 'tp'), may hold values from -0.1875 to 0.1875
- conv_taps: float32 [2, 4, 4096], replicated, may hold values from -3 to 3
- block_gates: bfloat16 [2, 2, 2, 4096, 128], P(None, None, None, 'tp'), may hold values from -0.5 to 0.5
- forget_rate: float32 [2, 2, 4096], replicated, may hold values from 0 to 0.05, as said below
Outputs:
- stream_out: bfloat16 [8192, 4096], P('sp', 'tp')
Inputs may be any that keep to these rules, and one draw needn't show every extreme that they name: `forget_rate`: positive.
All inputs are finite; a program needn't handle non-finite values.
Results may differ from a plain program's by a relative error of at most 0.025.
Values may be sent and summed in bfloat16 or wider, within the bound.
No kernel may reach another device: no remote copies, remote signals or barrier semaphores. Data moves between devices by JAX's collectives and lax.ppermute only.
A program may use at most 192 MiB of HBM per device.

v0:
```python
import jax
import jax.numpy as jnp
from jax import lax
from jax.experimental import pallas as pl
from jax.experimental.pallas import tpu as pltpu
from jax.sharding import PartitionSpec as P


GATE_SCALE = 8.0
NORM_EPS = 1e-06
F32 = jnp.float32
BF16 = jnp.bfloat16


CHUNKS = 8
SCAN_LIMIT = 24 * 2**20
VALUE_LIMIT = 54 * 2**20
GATE_LIMIT = 54 * 2**20
GIVE_LIMIT = 12 * 2**20
KEEP_LIMIT = 8 * 2**20
HALO = 16


def to_tiles(array):
    rows, width = array.shape
    return array.reshape(CHUNKS, rows // CHUNKS, width).swapaxes(0, 1).reshape(rows, width)


def to_tokens(array):
    rows, width = array.shape
    return array.reshape(rows // CHUNKS, CHUNKS, width).swapaxes(0, 1).reshape(rows, width)


def shifted(array, axis, move):
    count = lax.axis_size(axis)
    return lax.ppermute(array, axis, [(i, move(i)) for i in range(count)])


def across(array):
    return shifted(array, "tp", lambda i: i ^ 1)


def along_x(array, step):
    return shifted(array, "tp", lambda i: (i + 2 * step) % 8)


def token_halo(top, end):
    rows, width = end.shape
    count = lax.axis_size("sp")
    owners = lax.axis_size("tp")
    ends = jnp.concatenate([end[rows - 9 : rows - 8], end[rows - 1 :], top[:1], top[:1]], axis=0)
    copies = jnp.broadcast_to(ends[None], (owners, *ends.shape))
    every = lax.all_to_all(copies, "tp", 0, 0, tiled=True)
    before = lax.ppermute(every[:, :2], "sp", [(i, i + 1) for i in range(count - 1)])
    after = lax.ppermute(every[:, 2:], "sp", [(i + 1, i) for i in range(count - 1)])
    rest = jnp.zeros((owners, HALO - 4, width), end.dtype)
    return jnp.concatenate([before, after, rest], axis=1)


def gathered_stream(top, end):
    left_top = along_x(top, 1)
    right_end = along_x(end, -1)
    left_end = along_x(end, 1)
    right_top = along_x(top, -1)
    far_top = along_x(left_top, 1)
    far_end = along_x(right_end, -1)
    same = (top, end, left_top, left_end, right_top, right_end, far_top, far_end)
    return same + tuple(across(part) for part in same)


def block_of(rank, dx, flip):
    core = rank % 2
    return 2 * ((rank // 2 + dx + 4) % 4) + (1 - core if flip else core)


SHIFTS = (0, -1, 1, 2)


def along_plane(array, axis, step):
    dz, dy = (step, 0) if axis == "z" else (0, step)
    pairs = [
        (4 * z + y, 4 * ((z + dz) % 4) + (y + dy) % 4) for z in range(4) for y in range(4)
    ]
    return lax.ppermute(array, "sp", pairs)


def around(array, axis):
    half = array.shape[0] // 2
    before = along_plane(array, axis, 1)
    after = along_plane(array, axis, -1)
    return (
        before,
        after,
        along_plane(before[:half], axis, 1),
        along_plane(after[half:], axis, -1),
    )


def gathered_pieces(weights):
    half = weights[0].shape[0] // 2
    pieces = []
    for at, (first, second) in ((0, "yz"), (half, "zy")):
        own = jnp.concatenate([w[at : at + half] for w in weights], axis=0)
        before, after, far_top, far_end = around(own, first)
        top = jnp.concatenate([own, before], axis=0)
        end = jnp.concatenate([after, far_top, far_end], axis=0)
        top_before = along_plane(top, second, 1)
        top_after = along_plane(top, second, -1)
        end_after = along_plane(end, second, -1)
        end_before = along_plane(end, second, 1)
        pieces += [top, end, top_before, end_before, top_after, end_after]
        pieces += [along_plane(top_before, second, 1), along_plane(end_after, second, -1)]
    return tuple(pieces)


def block_copies(weight, which, rank, offsets, target, sems):
    size = target.shape[1]
    copies = []
    for n, (dx, flip) in enumerate(offsets):
        at = pl.multiple_of(block_of(rank, dx, flip) * size, size)
        copies.append(
            pltpu.make_async_copy(
                weight.at[which, pl.ds(at, size), :], target.at[n], sems.at[n]
            )
        )
    return copies


def weight_copies(sources, which, place, target, sems):
    blocks, size, _ = target.shape
    if len(sources) == 1:
        return [
            pltpu.make_async_copy(
                sources[0].at[which, pl.ds(n * size, size), :], target.at[n], sems.at[n]
            )
            for n in range(blocks)
        ]
    copies = []
    rows = size // 4
    group = sources[0].shape[0] // 2
    for half in range(2):
        for outer in range(4):
            for inner in range(4):
                ref = sources[8 * half + 2 * outer + inner // 2]
                start = (inner % 2) * group
                dz, dy = (outer, inner) if half == 0 else (inner, outer)
                z = (place // 4 + 4 + SHIFTS[dz]) % 4
                y = (place % 4 + 4 + SHIFTS[dy]) % 4
                at = pl.multiple_of((y % 2) * (2 * rows) + half * rows, rows)
                copies.append(
                    pltpu.make_async_copy(
                        ref.at[pl.ds(start + which * rows, rows), :],
                        target.at[2 * z + y // 2, pl.ds(at, rows), :],
                        sems.at[len(copies)],
                    )
                )
    return copies


ARRIVE = [(dx, flip) for flip in (0, 1) for dx in (0, -1, 1, 2)]
LEAVE = [(dx, flip) for flip in (1, 0) for dx in (2, 1, -1, 0)]


def contracted(rows, weight, total):
    total[...] = jnp.zeros_like(total)

    def step(k, carry):
        total[...] += jnp.dot(rows[k], weight[k], preferred_element_type=F32)
        return carry

    lax.fori_loop(0, rows.shape[0], step, 0)


def row_scale(squares, width):
    return lax.rsqrt(jnp.sum(squares[...], axis=1, keepdims=True) / width + NORM_EPS)


def piece_copies(rank, pieces, rows, sems):
    half = pieces[0].shape[0]
    return [
        pltpu.make_async_copy(
            pieces[2 * k + side],
            rows.at[block_of(rank, dx, flip), pl.ds(side * half, half), :],
            sems.at[2 * k + side],
        )
        for k, (dx, flip) in enumerate(ARRIVE)
        for side in range(2)
    ]


WINDOW = 8


def opened(copies):
    for copy in copies[:WINDOW]:
        copy.start()


def awaited(copies, first, last):
    for n in range(first, last):
        copies[n].wait()
        if n + WINDOW < len(copies):
            copies[n + WINDOW].start()


def scaled_rows(layer, rank, gain, copies, halo, rows, squares):
    width = rows.shape[2]
    half = (rows.shape[1] - (0 if halo is None else HALO)) // 2
    step = 64
    for k, (dx, flip) in enumerate(ARRIVE):
        awaited(copies, 2 * k, 2 * k + 2)
        block = block_of(rank, dx, flip)
        scale = gain[layer : layer + 1, pl.ds(pl.multiple_of(block * width, width), width)]

        def put(raw, at, k=k, block=block, scale=scale):
            raw = raw.astype(F32)
            rows[block, at, :] = (raw * scale).astype(BF16)
            power = raw * raw
            lanes = sum(power[:, 128 * q : 128 * (q + 1)] for q in range(width // 128))
            if k == 0:
                squares[at, :] = lanes
            else:
                squares[at, :] += lanes

        def chunk(n, carry, block=block, put=put):
            for side in range(2):
                at = pl.ds(pl.multiple_of(n * step + side * half, step), step)
                put(rows[block, at, :], at)
            return carry

        lax.fori_loop(0, half // step, chunk, 0)
        if halo is not None:
            put(halo[block], pl.ds(2 * half, HALO))


def value_body(layer, rank, place, gain, halo, *refs):
    pieces, sources = refs[:16], refs[16:-7]
    out, rows, squares, value_in, total, sems, piece_sems = refs[-7:]
    values = weight_copies(sources, 0, place[0], value_in, sems)
    copies = piece_copies(rank[0], pieces, rows, piece_sems) + values
    opened(copies)
    scaled_rows(layer, rank[0], gain, copies, halo, rows, squares)
    awaited(copies, 16, len(copies))
    contracted(rows, value_in, total)
    out[...] = (total[...] * row_scale(squares, out.shape[1] * len(ARRIVE))).astype(BF16)


def gate_body(layer, which, rank, place, gain, *refs):
    pieces, sources, full = refs[:16], refs[16:-10], refs[-10]
    out, out_in, rows, squares, gate_in, total, sems, out_sems, piece_sems = refs[-9:]
    gates = weight_copies(sources, 1, place[0], gate_in, sems)
    others = block_copies(full, which, rank[0], LEAVE, out_in, out_sems)
    copies = piece_copies(rank[0], pieces, rows, piece_sems) + gates + others
    opened(copies)
    scaled_rows(layer, rank[0], gain, copies, None, rows, squares)
    awaited(copies, 16, 16 + len(gates))
    contracted(rows, gate_in, total)
    out[...] = (total[...] * row_scale(squares, out.shape[1] * len(ARRIVE))).astype(BF16)
    awaited(copies, 16 + len(gates), len(copies))


def in_smem():
    return pl.BlockSpec(memory_space=pltpu.SMEM)


def in_vmem():
    return pl.BlockSpec(memory_space=pltpu.VMEM)


def in_hbm():
    return pl.BlockSpec(memory_space=pltpu.HBM)


def product_cost(rows, width, count):
    return pl.CostEstimate(
        flops=2 * count * rows * width * width,
        bytes_accessed=2 * count * width * width,
        transcendentals=0,
    )


def value_rows(rank, place, pieces, halo, norm_gain, layer, sources):
    half, width = pieces[0].shape
    count = norm_gain.shape[1] // width
    deep = 2 * half + HALO
    return pl.pallas_call(
        lambda *refs: value_body(layer, *refs),
        out_shape=jax.ShapeDtypeStruct((deep, width), BF16),
        in_specs=[in_smem()] * 2 + [in_vmem()] * 2 + [in_hbm()] * (16 + len(sources)),
        out_specs=in_vmem(),
        scratch_shapes=[
            pltpu.VMEM((count, deep, width), BF16),
            pltpu.VMEM((deep, 128), F32),
            pltpu.VMEM((count, width, width), BF16),
            pltpu.VMEM((deep, width), F32),
            pltpu.SemaphoreType.DMA((32,)),
            pltpu.SemaphoreType.DMA((16,)),
        ],
        compiler_params=pltpu.CompilerParams(vmem_limit_bytes=VALUE_LIMIT),
        cost_estimate=product_cost(deep, width, count),
        name="value_rows",
    )(rank, place, norm_gain, halo, *pieces, *sources)


def gate_rows(rank, place, pieces, norm_gain, layer, sources, full, which):
    half, width = pieces[0].shape
    count = norm_gain.shape[1] // width
    length = 2 * half
    return pl.pallas_call(
        lambda *refs: gate_body(layer, which, *refs),
        out_shape=[
            jax.ShapeDtypeStruct((length, width), BF16),
            jax.ShapeDtypeStruct((count, width, width), BF16),
        ],
        in_specs=[in_smem()] * 2 + [in_vmem()] + [in_hbm()] * (17 + len(sources)),
        out_specs=[in_vmem()] * 2,
        scratch_shapes=[
            pltpu.VMEM((count, length, width), BF16),
            pltpu.VMEM((length, 128), F32),
            pltpu.VMEM((count, width, width), BF16),
            pltpu.VMEM((length, width), F32),
            pltpu.SemaphoreType.DMA((32,)),
            pltpu.SemaphoreType.DMA((count,)),
            pltpu.SemaphoreType.DMA((16,)),
        ],
        compiler_params=pltpu.CompilerParams(vmem_limit_bytes=GATE_LIMIT),
        cost_estimate=product_cost(length, width, count),
        name="gate_rows",
    )(rank, place, norm_gain, *pieces, *sources, full)


def scan_body(
    rank, mix, taps, rate, gates, local, fwd_cum, bwd_cum, coef, edge, padded, conv, pre
):
    steps = conv.shape[0] // CHUNKS
    length = conv.shape[0]
    sub = lax.broadcasted_iota(jnp.int32, (CHUNKS, 128), 0)
    rows = mix[...].astype(F32)
    halo = rows[length : length + 8]
    padded[16 : 16 + length] = rows[:length]
    padded[0:8] = jnp.where(
        sub == 0, halo[0:1], pltpu.roll(rows[length - 16 : length - 8], 1, axis=0)
    )
    padded[8:16] = jnp.where(sub == 0, halo[1:2], pltpu.roll(rows[length - 8 : length], 1, axis=0))
    padded[16 + length : 24 + length] = jnp.where(
        sub == CHUNKS - 1, halo[2:3], pltpu.roll(rows[0:8], CHUNKS - 1, axis=0)
    )
    for part in range(8):
        lo = part * (length // 8)
        hi = lo + length // 8
        conv[lo:hi] = sum(padded[lo + 8 * k : hi + 8 * k] * taps[0, k : k + 1] for k in range(4))
    lhs = conv[...].astype(BF16)
    for g in range(4):
        pre[g] = jnp.dot(lhs, gates[0, g // 2, g % 2], preferred_element_type=F32)

    def cell(i, e):
        at = pl.ds(pl.multiple_of(i * CHUNKS, CHUNKS), CHUNKS)
        recur = jax.nn.sigmoid(pre[2 * e, at, :])
        entry = jax.nn.sigmoid(pre[2 * e + 1, at, :])
        log_a = (-GATE_SCALE) * recur * rate[0, e : e + 1]
        decay = jnp.exp(log_a)
        x = 2.0 * log_a
        near = x * (1.0 + x * (0.5 + x * (1.0 / 6 + x * (1.0 / 24 + x * (1.0 / 120)))))
        room = -jnp.where(x > -0.125, near, decay * decay - 1.0)
        return at, decay, jnp.sqrt(room) * entry * conv[at, :]

    zero = jnp.zeros((CHUNKS, 128), F32)
    one = jnp.ones((CHUNKS, 128), F32)
    inner = 8

    def forward(block, carry):
        state, cum = carry
        for n in range(inner):
            at, decay, drive = cell(block * inner + n, 0)
            state = decay * state + drive
            cum = decay * cum
            local[at, :] = state
            fwd_cum[at, :] = cum
        return state, cum

    def backward(block, carry):
        state, cum = carry
        for n in range(inner):
            at, decay, drive = cell(steps - 1 - (block * inner + n), 1)
            state = decay * state + drive
            cum = decay * cum
            local[at, :] += state
            bwd_cum[at, :] = cum
        return state, cum

    state_f, cum_f = lax.fori_loop(0, steps // inner, forward, (zero, one))
    state_b, cum_b = lax.fori_loop(0, steps // inner, backward, (zero, one))
    alpha = jnp.zeros((1, 128), F32)
    beta = jnp.ones((1, 128), F32)
    for s in range(CHUNKS):
        coef[0, s : s + 1] = alpha
        coef[1, s : s + 1] = beta
        alpha = state_f[s : s + 1] + cum_f[s : s + 1] * alpha
        beta = cum_f[s : s + 1] * beta
    sums_f = (beta, alpha)
    alpha = jnp.zeros((1, 128), F32)
    beta = jnp.ones((1, 128), F32)
    for s in reversed(range(CHUNKS)):
        coef[2, s : s + 1] = alpha
        coef[3, s : s + 1] = beta
        alpha = state_b[s : s + 1] + cum_b[s : s + 1] * alpha
        beta = cum_b[s : s + 1] * beta
    edge[...] = jnp.broadcast_to(
        jnp.concatenate([*sums_f, beta, alpha], axis=0)[None], edge.shape
    )


def scanned(rank, mix, conv_taps, forget_rate, block_gates, layer, copies):
    deep, width = mix.shape
    length = deep - HALO
    blocks = width // 128
    column = lambda b, rank: (0, b)
    owned = lambda b, rank: (layer, 0, rank[0] * blocks + b)
    return pl.pallas_call(
        scan_body,
        grid_spec=pltpu.PrefetchScalarGridSpec(
            num_scalar_prefetch=1,
            grid=(blocks,),
            in_specs=[
                pl.BlockSpec((deep, 128), column),
                pl.BlockSpec((1, 4, 128), owned),
                pl.BlockSpec((1, 2, 128), owned),
                pl.BlockSpec((1, 2, 2, 128, 128), lambda b, rank: (layer, 0, 0, b, 0)),
            ],
            out_specs=[
                pl.BlockSpec((length, 128), column),
                pl.BlockSpec((length, 128), column),
                pl.BlockSpec((length, 128), column),
                pl.BlockSpec((4, CHUNKS, 128), lambda b, rank: (0, 0, b)),
                pl.BlockSpec((copies, 4, 128), lambda b, rank: (0, 0, b)),
            ],
            scratch_shapes=[
                pltpu.VMEM((length + 24, 128), F32),
                pltpu.VMEM((length, 128), F32),
                pltpu.VMEM((4, length, 128), F32),
            ],
        ),
        out_shape=[
            jax.ShapeDtypeStruct((length, width), F32),
            jax.ShapeDtypeStruct((length, width), F32),
            jax.ShapeDtypeStruct((length, width), F32),
            jax.ShapeDtypeStruct((4, CHUNKS, width), F32),
            jax.ShapeDtypeStruct((copies, 4, width), F32),
        ],
        compiler_params=pltpu.CompilerParams(vmem_limit_bytes=SCAN_LIMIT),
        cost_estimate=pl.CostEstimate(
            flops=10_000_000_000, bytes_accessed=4_000_000, transcendentals=4_000_000
        ),
        name="scan",
    )(rank, mix, conv_taps, forget_rate, block_gates)


def features(mixed, weight):
    return lax.dot_general(
        mixed, weight, (((1,), (1,)), ((), ())), preferred_element_type=F32
    ).astype(BF16)


def give_body(
    place, edges, local, fwd_cum, bwd_cum, coef, gate, weight, mixed, far, rest
):
    mine = place[0]
    count, _, width = edges.shape
    enter_f = jnp.zeros((1, width), F32)
    enter_b = jnp.zeros((1, width), F32)
    for r in range(count):
        enter_f = jnp.where(r < mine, edges[r, 1:2] + edges[r, 0:1] * enter_f, enter_f)
        q = count - 1 - r
        enter_b = jnp.where(q > mine, edges[q, 3:4] + edges[q, 2:3] * enter_b, enter_b)
    from_f = coef[0] + coef[1] * enter_f
    from_b = coef[2] + coef[3] * enter_b
    group = 64
    for c in range(width // 128):
        col = slice(128 * c, 128 * (c + 1))
        tiled_f = jnp.concatenate([from_f[:, col]] * (group // CHUNKS), axis=0)
        tiled_b = jnp.concatenate([from_b[:, col]] * (group // CHUNKS), axis=0)

        def part(n, carry, col=col, tiled_f=tiled_f, tiled_b=tiled_b):
            at = pl.ds(pl.multiple_of(n * group, group), group)
            both = local[at, col] + fwd_cum[at, col] * tiled_f + bwd_cum[at, col] * tiled_b
            z = gate[at, col].astype(F32)
            mixed[at, col] = (both * (z * jax.nn.sigmoid(z))).astype(BF16)
            return carry

        lax.fori_loop(0, local.shape[0] // group, part, 0)
    far[...] = features(mixed[...], weight[0])

    def step(n, carry):
        rest[n] = features(mixed[...], weight[n + 1])
        return carry

    lax.fori_loop(0, 3, step, 0)


def given(place, edges, local, fwd_cum, bwd_cum, coef, gate, weight):
    length, width = local.shape
    return pl.pallas_call(
        give_body,
        in_specs=[in_smem()] + [in_vmem()] * 7,
        out_specs=[in_vmem()] * 3,
        out_shape=[
            jax.ShapeDtypeStruct((length, width), BF16),
            jax.ShapeDtypeStruct((length, width), BF16),
            jax.ShapeDtypeStruct((3, length, width), BF16),
        ],
        compiler_params=pltpu.CompilerParams(vmem_limit_bytes=GIVE_LIMIT),
        cost_estimate=product_cost(length, width, 4),
        name="given",
    )(place, edges, local, fwd_cum, bwd_cum, coef, gate, weight)


def keep_body(mixed, weight, far, rest):
    far[...] = features(mixed[...], weight[4])

    def step(n, carry):
        rest[n] = features(mixed[...], weight[n + 5])
        return carry

    lax.fori_loop(0, 3, step, 0)


def kept(mixed, weight):
    length, width = mixed.shape
    return pl.pallas_call(
        keep_body,
        in_specs=[in_vmem()] * 2,
        out_specs=[in_vmem()] * 2,
        out_shape=[
            jax.ShapeDtypeStruct((length, width), BF16),
            jax.ShapeDtypeStruct((3, length, width), BF16),
        ],
        compiler_params=pltpu.CompilerParams(vmem_limit_bytes=KEEP_LIMIT),
        cost_estimate=product_cost(length, width, 4),
        name="kept",
    )(mixed, weight)


def total_of(*parts):
    return sum(part.astype(F32) for part in parts)


def per_device(
    stream_in, norm_gain, value_proj, gate_proj, out_proj, conv_taps, block_gates, forget_rate
):
    rank = lax.axis_index("tp").reshape(1)
    place = lax.axis_index("sp").reshape(1)
    length, _ = stream_in.shape
    half = length // 2
    stream = to_tiles(stream_in)
    top, end = stream[:half], stream[half:]
    pieces_0 = gathered_pieces([value_proj[0], gate_proj[0]])
    outs_0 = lax.all_gather(out_proj[:1], "sp", axis=1, tiled=True)
    held = jnp.stack([value_proj[1], gate_proj[1], out_proj[1]])
    full_1 = lax.all_gather(held, "sp", axis=1, tiled=True)
    weights = [(pieces_0, outs_0, 0), ((full_1,), full_1, 2)]
    for layer in range(value_proj.shape[0]):
        sources, full, which = weights[layer]
        pieces = gathered_stream(top, end)
        halo = token_halo(top, end)
        mix_in = value_rows(rank, place, pieces, halo, norm_gain, layer, sources)
        local, fwd_cum, bwd_cum, coef, edge = scanned(
            rank, mix_in, conv_taps, forget_rate, block_gates, layer, lax.axis_size("sp")
        )
        edges = lax.all_to_all(edge, "sp", 0, 0, tiled=True)
        gate_z, out_weight = gate_rows(rank, place, pieces, norm_gain, layer, sources, full, which)
        mixed, far_give, rest_give = given(
            place, edges, local, fwd_cum, bwd_cum, coef, gate_z, out_weight
        )
        far_away = across(far_give)
        rest_away = across(rest_give)
        far_keep, rest_keep = kept(mixed, out_weight)
        far = total_of(far_keep, far_away).astype(BF16)
        halves = (slice(0, half), slice(half, length))
        up, down, own = (
            [(rest_keep[n, rows], rest_away[n, rows]) for rows in halves] for n in range(3)
        )
        relay_top = along_x(far[:half], 1)
        relay_end = along_x(far[half:], -1)
        up_end = along_x(total_of(*up[1]).astype(BF16), 1)
        down_top = along_x(total_of(*down[0]).astype(BF16), -1)
        up_top = along_x(total_of(*up[0], relay_top).astype(BF16), 1)
        down_end = along_x(total_of(*down[1], relay_end).astype(BF16), -1)
        up_top, down_top, up_end, down_end = lax.optimization_barrier(
            (up_top, down_top, up_end, down_end)
        )
        top = total_of(top, *own[0], up_top, down_top).astype(BF16)
        end = total_of(end, *own[1], up_end, down_end).astype(BF16)
    return to_tokens(jnp.concatenate([top, end], axis=0))


def solution(mesh):
    placed = (
        P("sp", "tp"),
        P(),
        P(None, "sp", "tp"),
        P(None, "sp", "tp"),
        P(None, "sp", "tp"),
        P(),
        P(None, None, None, "tp", None),
        P(),
    )
    return jax.shard_map(
        per_device, mesh=mesh, in_specs=placed, out_specs=P("sp", "tp"), check_vma=False
    )
```

profile of v0, /device:TPU:1, one launch (start us, length us, event | category | flops | bytes accessed | tf_op | source)
XLA Modules:
  0.0 308.2 jit_solution(16710892405090886172)
XLA Ops:
  11.5 5.8 %all-to-all-start = ((bf16[8,4,512]{2,1,0:T(4,128)(2,1)}), bf16[8,4,512]{2,1,0:T(4,128)(2,1)S(1)}, u32[]{:S(2)}, u32[]{:S(2)}) async-start(bf16[8,4,512]{2,1,0:T(4,128)(2,1)} %broadcast_in_dim.4), calls=%async_computation | async-start | bytes 65536 | tf_op jit(solution)/shard_map/all_to_all | solution.py:53
  17.4 2.8 collective-permute-start.17
  22.0 3.2 %collective-permute-start = (bf16[8,2,512]{2,1,0:T(2,128)(2,1)S(1)}, bf16[8,2,512]{2,1,0:T(2,128)(2,1)S(1)}, u32[]{:S(2)}, u32[]{:S(2)}) collective-permute-start(bf16[8,2,512]{2,1,0:T(2,128)(2,1)S(1)} %get-tuple-element.99), channel_id=1, source_target_pairs={{0,8},{8,16},{16,24},{24,32},{32,40},{40,48},{48,56},{56,64},{64,7... | collective-permute-start | bytes 49160 | tf_op jit(solution)/shard_map/ppermute | solution.py:54
  26.6 6.7 %collective-permute-start.27 = (bf16[256,512]{1,0:T(8,128)(2,1)S(1)}, bf16[256,512]{1,0:T(8,128)(2,1)S(1)}, u32[]{:S(2)}, u32[]{:S(2)}) collective-permute-start(bf16[256,512]{1,0:T(8,128)(2,1)S(1)} %pad_maximum_fusion.4), channel_id=1, source_target_pairs={{0,96},{8,104},{16,112},{24,120},{32,0},{40,8},{48,16},{56,24},{64... | collective-permute-start | bytes 786440 | tf_op jit(solution)/shard_map/ppermute | solution.py:84
  36.1 3.4 %collective-permute-done.27 = bf16[256,512]{1,0:T(8,128)(2,1)S(1)} collective-permute-done((bf16[256,512]{1,0:T(8,128)(2,1)S(1)}, bf16[256,512]{1,0:T(8,128)(2,1)S(1)}, u32[]{:S(2)}, u32[]{:S(2)}) %collective-permute-start.27) | collective-permute-done | bytes 262176 | tf_op jit(solution)/shard_map/ppermute | solution.py:84
  51.3 3.4 %collective-permute-done.18 = bf16[128,512]{1,0:T(8,128)(2,1)S(1)} collective-permute-done((bf16[128,512]{1,0:T(8,128)(2,1)S(1)}, bf16[128,512]{1,0:T(8,128)(2,1)S(1)}, u32[]{:S(2)}, u32[]{:S(2)}) %collective-permute-start.18) | collective-permute-done | bytes 131104 | tf_op jit(solution)/shard_map/ppermute | solution.py:84
  57.4 2.7 collective-permute-start.13
  64.9 2.7 collective-permute-start.32
  72.9 6.5 %collective-permute-done.20.refs_22_.refs_21_ = bf16[512,512]{1,0:T(8,128)(2,1)S(1)} collective-permute-done((bf16[512,512]{1,0:T(8,128)(2,1)S(1)}, bf16[512,512]{1,0:T(8,128)(2,1)S(1)}, u32[]{:S(2)}, u32[]{:S(2)}) %collective-permute-start.20) | collective-permute-done | bytes 524320 | tf_op jit(solution)/shard_map/ppermute | solution.py:84
  84.7 4.4 %collective-permute-done.23.refs_25_.refs_24_ = bf16[512,512]{1,0:T(8,128)(2,1)} collective-permute-done((bf16[512,512]{1,0:T(8,128)(2,1)S(1)}, bf16[512,512]{1,0:T(8,128)(2,1)}, u32[]{:S(2)}, u32[]{:S(2)}) %collective-permute-start.23) | collective-permute-done | bytes 524320 | tf_op jit(solution)/shard_map/ppermute | solution.py:84
  90.4 5.4 %collective-permute-done.33.refs_33_.refs_32_ = bf16[512,512]{1,0:T(8,128)(2,1)} collective-permute-done((bf16[512,512]{1,0:T(8,128)(2,1)S(1)}, bf16[512,512]{1,0:T(8,128)(2,1)}, u32[]{:S(2)}, u32[]{:S(2)}) %collective-permute-start.33) | collective-permute-done | bytes 524320 | tf_op jit(solution)/shard_map/ppermute | solution.py:84
  100.2 4.7 %collective-permute-done.31.refs_31_.refs_30_ = bf16[512,512]{1,0:T(8,128)(2,1)S(1)} collective-permute-done((bf16[512,512]{1,0:T(8,128)(2,1)S(1)}, bf16[512,512]{1,0:T(8,128)(2,1)S(1)}, u32[]{:S(2)}, u32[]{:S(2)}) %collective-permute-start.31) | collective-permute-done | bytes 524320 | tf_op jit(solution)/shard_map/ppermute | solution.py:84
  104.9 14.4 %collective-permute-done.24.refs_26_.refs_25_ = bf16[512,512]{1,0:T(8,128)(2,1)} collective-permute-done((bf16[512,512]{1,0:T(8,128)(2,1)S(1)}, bf16[512,512]{1,0:T(8,128)(2,1)}, u32[]{:S(2)}, u32[]{:S(2)}) %collective-permute-start.24) | collective-permute-done | bytes 524320 | tf_op jit(solution)/shard_map/ppermute | solution.py:84
  119.4 3.0 collective-permute-done.34.refs_34_.refs_33_
  122.4 13.1 %value_rows.2.mix = bf16[528,512]{1,0:T(8,128)(2,1)} custom-call(s32[1]{0:T(128)} %bitcast.4.refs_0_.rank, s32[1]{0:T(128)} %bitcast.3.refs_1_.place, f32[2,4096]{1,0:T(2,128)} %refs_2_.7, bf16[8,16,512]{2,1,0:T(8,128)(2,1)} %maximum_maximum_fusion.refs_3_, bf16[256,512]{1,0:T(8,128)(2,1)} %copy-done.21, bf16[256,512]{1,0:T(8,128)(2,1)} %copy-done.20, ...), custom_call_target="tpu_custom_call" | custom-call | flops 2214592512 | bytes 4194304 | tf_op jit(solution)/shard_map/value_rows/pallas_call | solution.py:286
  136.7 6.5 %scan.2 = (f32[512,512]{1,0:T(8,128)S(1)}, f32[512,512]{1,0:T(8,128)S(1)}, f32[512,512]{1,0:T(8,128)S(1)}, f32[4,8,512]{2,1,0:T(8,128)S(1)}, f32[16,4,512]{2,1,0:T(4,128)}) custom-call(s32[1]{0:T(128)} %bitcast.4.refs_0_.rank, bf16[528,512]{1,0:T(8,128)(2,1)S(1)} %copy-done.3, f32[2,4,4096]{2,1,0:T(4,128)S(1)} %copy-done.8, f32[2,2,4096]{2,1,0:T(2,128)S(1)} %copy-done.9, ...), custom_call_target="tpu_custom_call" | custom-call | flops 10000000000 | bytes 4000000 | tf_op jit(solution)/shard_map/scan/pallas_call | solution.py:419
  143.1 4.3 %all-to-all-start.1 = ((f32[16,4,512]{2,1,0:T(4,128)}), f32[16,4,512]{2,1,0:T(4,128)S(1)}, u32[]{:S(2)}, u32[]{:S(2)}) async-start(f32[16,4,512]{2,1,0:T(4,128)} %get-tuple-element.37), calls=%async_computation.1 | async-start | bytes 262144 | tf_op jit(solution)/shard_map/all_to_all | solution.py:569
  147.4 13.9 %gate_rows.2 = (bf16[512,512]{1,0:T(8,128)(2,1)}, bf16[8,512,512]{2,1,0:T(8,128)(2,1)}) custom-call(s32[1]{0:T(128)} %bitcast.4.refs_0_.rank, s32[1]{0:T(128)} %bitcast.3.refs_1_.place, f32[2,4096]{1,0:T(2,128)} %refs_2_.7, bf16[256,512]{1,0:T(8,128)(2,1)} %copy-done.21, bf16[256,512]{1,0:T(8,128)(2,1)} %copy-done.20, bf16[256,512]{1,0:T(8,128)(2,1)} %copy-done.41, ...), custom_call_target="tpu_custom_call" | custom-call | flops 2147483648 | bytes 4194304 | tf_op jit(solution)/shard_map/gate_rows/pallas_call | solution.py:309
  177.3 4.3 %collective-permute-done.38 = bf16[256,512]{1,0:T(8,128)(2,1)S(1)} collective-permute-done((bf16[256,512]{1,0:T(8,128)(2,1)S(1)}, bf16[256,512]{1,0:T(8,128)(2,1)S(1)}, u32[]{:S(2)}, u32[]{:S(2)}) %collective-permute-start.38) | collective-permute-done | bytes 262176 | tf_op jit(solution)/shard_map/ppermute | solution.py:36
  187.3 5.6 %collective-permute-done.39 = bf16[256,512]{1,0:T(8,128)(2,1)S(1)} collective-permute-done((bf16[256,512]{1,0:T(8,128)(2,1)S(1)}, bf16[256,512]{1,0:T(8,128)(2,1)S(1)}, u32[]{:S(2)}, u32[]{:S(2)}) %collective-permute-start.39) | collective-permute-done | bytes 262176 | tf_op jit(solution)/shard_map/ppermute | solution.py:36
  194.0 5.5 %all-to-all-start.2 = ((bf16[8,4,512]{2,1,0:T(4,128)(2,1)}), bf16[8,4,512]{2,1,0:T(4,128)(2,1)S(1)}, u32[]{:S(2)}, u32[]{:S(2)}) async-start(bf16[8,4,512]{2,1,0:T(4,128)(2,1)} %broadcast_in_dim.5), calls=%async_computation.2 | async-start | bytes 65536 | tf_op jit(solution)/shard_map/all_to_all | solution.py:53
  204.9 3.6 %collective-permute-start.44 = (bf16[8,2,512]{2,1,0:T(2,128)(2,1)S(1)}, bf16[8,2,512]{2,1,0:T(2,128)(2,1)S(1)}, u32[]{:S(2)}, u32[]{:S(2)}) collective-permute-start(bf16[8,2,512]{2,1,0:T(2,128)(2,1)S(1)} %get-tuple-element.97), channel_id=1, source_target_pairs={{0,8},{8,16},{16,24},{24,32},{32,40},{40,48},{48,56},{56,64},{64,7... | collective-permute-start | bytes 49160 | tf_op jit(solution)/shard_map/ppermute | solution.py:54
  210.6 4.0 %collective-permute-done.45 = bf16[8,2,512]{2,1,0:T(2,128)(2,1)S(1)} collective-permute-done((bf16[8,2,512]{2,1,0:T(2,128)(2,1)S(1)}, bf16[8,2,512]{2,1,0:T(2,128)(2,1)S(1)}, u32[]{:S(2)}, u32[]{:S(2)}) %collective-permute-start.45) | collective-permute-done | bytes 16416 | tf_op jit(solution)/shard_map/ppermute | solution.py:55
  217.4 2.6 collective-permute-start.51
  221.6 4.5 %collective-permute-done.50.refs_10_.refs_9_ = bf16[256,512]{1,0:T(8,128)(2,1)S(1)} collective-permute-done((bf16[256,512]{1,0:T(8,128)(2,1)S(1)}, bf16[256,512]{1,0:T(8,128)(2,1)S(1)}, u32[]{:S(2)}, u32[]{:S(2)}) %collective-permute-start.50) | collective-permute-done | bytes 262176 | tf_op jit(solution)/shard_map/ppermute | solution.py:36
  230.2 10.3 %value_rows.3.mix = bf16[528,512]{1,0:T(8,128)(2,1)} custom-call(s32[1]{0:T(128)} %bitcast.4.refs_0_.rank, s32[1]{0:T(128)} %bitcast.3.refs_1_.place, f32[2,4096]{1,0:T(2,128)} %refs_2_.7, bf16[8,16,512]{2,1,0:T(8,128)(2,1)} %maximum_maximum_fusion.1.refs_3_, bf16[256,512]{1,0:T(8,128)(2,1)} %copy-done.16, bf16[256,512]{1,0:T(8,128)(2,1)} %copy-done.14, ...), custom_call_target="tpu_custom_call" | custom-call | flops 2214592512 | bytes 4194304 | tf_op jit(solution)/shard_map/value_rows/pallas_call | solution.py:286
  242.8 6.5 %scan.3 = (f32[512,512]{1,0:T(8,128)S(1)}, f32[512,512]{1,0:T(8,128)S(1)}, f32[512,512]{1,0:T(8,128)S(1)}, f32[4,8,512]{2,1,0:T(8,128)S(1)}, f32[16,4,512]{2,1,0:T(4,128)}) custom-call(s32[1]{0:T(128)} %bitcast.4.refs_0_.rank, bf16[528,512]{1,0:T(8,128)(2,1)S(1)} %copy-done.2, f32[2,4,4096]{2,1,0:T(4,128)S(1)} %copy-done.8, f32[2,2,4096]{2,1,0:T(2,128)S(1)} %copy-done.9, ...), custom_call_target="tpu_custom_call" | custom-call | flops 10000000000 | bytes 4000000 | tf_op jit(solution)/shard_map/scan/pallas_call | solution.py:419
  249.3 8.9 %all-to-all-start.3 = ((f32[16,4,512]{2,1,0:T(4,128)}), f32[16,4,512]{2,1,0:T(4,128)S(1)}, u32[]{:S(2)}, u32[]{:S(2)}) async-start(f32[16,4,512]{2,1,0:T(4,128)} %get-tuple-element.53), calls=%async_computation.3 | async-start | bytes 262144 | tf_op jit(solution)/shard_map/all_to_all | solution.py:569
  258.2 11.5 %gate_rows.3 = (bf16[512,512]{1,0:T(8,128)(2,1)}, bf16[8,512,512]{2,1,0:T(8,128)(2,1)}) custom-call(s32[1]{0:T(128)} %bitcast.4.refs_0_.rank, s32[1]{0:T(128)} %bitcast.3.refs_1_.place, f32[2,4096]{1,0:T(2,128)} %refs_2_.7, bf16[256,512]{1,0:T(8,128)(2,1)} %copy-done.16, bf16[256,512]{1,0:T(8,128)(2,1)} %copy-done.14, bf16[256,512]{1,0:T(8,128)(2,1)} %copy-done.28, ...), custom_call_target="tpu_custom_call" | custom-call | flops 2147483648 | bytes 4194304 | tf_op jit(solution)/shard_map/gate_rows/pallas_call | solution.py:309
  280.1 2.7 collective-permute-start.66
  284.4 4.3 %collective-permute-done.62 = bf16[256,512]{1,0:T(8,128)(2,1)S(1)} collective-permute-done((bf16[256,512]{1,0:T(8,128)(2,1)S(1)}, bf16[256,512]{1,0:T(8,128)(2,1)S(1)}, u32[]{:S(2)}, u32[]{:S(2)}) %collective-permute-start.62) | collective-permute-done | bytes 262176 | tf_op jit(solution)/shard_map/ppermute | solution.py:36
  294.4 5.6 %collective-permute-done.63 = bf16[256,512]{1,0:T(8,128)(2,1)S(1)} collective-permute-done((bf16[256,512]{1,0:T(8,128)(2,1)S(1)}, bf16[256,512]{1,0:T(8,128)(2,1)S(1)}, u32[]{:S(2)}, u32[]{:S(2)}) %collective-permute-start.63) | collective-permute-done | bytes 262176 | tf_op jit(solution)/shard_map/ppermute | solution.py:36
  (289 shorter events, 107.0 us)
Async XLA Ops:
  6.5 140.9 %all-gather.3.cloned.1.call-start = ((), (), s32[]{:S(2)}) async-start(), calls=%async_computation.4 | async-start | bytes 4456448 | tf_op jit(solution)/shard_map/all_gather | solution.py:557
  8.4 221.7 %all-gather.5.cloned.1.call-start = ((), (), s32[]{:S(2)}) async-start(), calls=%async_computation.5 | async-start | bytes 13369344 | tf_op jit(solution)/shard_map/all_gather | solution.py:559
  11.5 10.5 %all-to-all-start = ((bf16[8,4,512]{2,1,0:T(4,128)(2,1)}), bf16[8,4,512]{2,1,0:T(4,128)(2,1)S(1)}, u32[]{:S(2)}, u32[]{:S(2)}) async-start(bf16[8,4,512]{2,1,0:T(4,128)(2,1)} %broadcast_in_dim.4), calls=%async_computation | async-start | bytes 65536 | tf_op jit(solution)/shard_map/all_to_all | solution.py:53
  17.4 16.3 %collective-permute-start.17 = (bf16[256,512]{1,0:T(8,128)(2,1)S(1)}, bf16[256,512]{1,0:T(8,128)(2,1)S(1)}, u32[]{:S(2)}, u32[]{:S(2)}) collective-permute-start(bf16[256,512]{1,0:T(8,128)(2,1)S(1)} %pad_maximum_fusion.3), channel_id=1, source_target_pairs={{0,24},{8,0},{16,8},{24,16},{32,56},{40,32},{48,40},{56,48},{64,88... | collective-permute-start | bytes 786440 | tf_op jit(solution)/shard_map/ppermute | solution.py:84
  20.2 15.9 %collective-permute-start.16 = (bf16[256,512]{1,0:T(8,128)(2,1)S(1)}, bf16[256,512]{1,0:T(8,128)(2,1)S(1)}, u32[]{:S(2)}, u32[]{:S(2)}) collective-permute-start(bf16[256,512]{1,0:T(8,128)(2,1)S(1)} %pad_maximum_fusion.3), channel_id=1, source_target_pairs={{0,8},{8,16},{16,24},{24,0},{32,40},{40,48},{48,56},{56,32},{64,72... | collective-permute-start | bytes 786440 | tf_op jit(solution)/shard_map/ppermute | solution.py:84
  22.0 11.3 %collective-permute-start = (bf16[8,2,512]{2,1,0:T(2,128)(2,1)S(1)}, bf16[8,2,512]{2,1,0:T(2,128)(2,1)S(1)}, u32[]{:S(2)}, u32[]{:S(2)}) collective-permute-start(bf16[8,2,512]{2,1,0:T(2,128)(2,1)S(1)} %get-tuple-element.99), channel_id=1, source_target_pairs={{0,8},{8,16},{16,24},{24,32},{32,40},{40,48},{48,56},{56,64},{64,7... | collective-permute-start | bytes 49160 | tf_op jit(solution)/shard_map/ppermute | solution.py:54
  26.6 12.9 %collective-permute-start.27 = (bf16[256,512]{1,0:T(8,128)(2,1)S(1)}, bf16[256,512]{1,0:T(8,128)(2,1)S(1)}, u32[]{:S(2)}, u32[]{:S(2)}) collective-permute-start(bf16[256,512]{1,0:T(8,128)(2,1)S(1)} %pad_maximum_fusion.4), channel_id=1, source_target_pairs={{0,96},{8,104},{16,112},{24,120},{32,0},{40,8},{48,16},{56,24},{64... | collective-permute-start | bytes 786440 | tf_op jit(solution)/shard_map/ppermute | solution.py:84
  33.7 11.7 %collective-permute-start.5 = (bf16[256,512]{1,0:T(8,128)(2,1)S(1)}, bf16[256,512]{1,0:T(8,128)(2,1)S(1)}, u32[]{:S(2)}, u32[]{:S(2)}) collective-permute-start(bf16[256,512]{1,0:T(8,128)(2,1)S(1)} %get-tuple-element.91.refs_5_.refs_4_), channel_id=1, source_target_pairs={{0,6},{1,7},{2,0},{3,1},{4,2},{5,3},{6,4},{7,5},{8,14},{9,15},{10,... | collective-permute-start | bytes 786440 | tf_op jit(solution)/shard_map/ppermute | solution.py:36
  36.1 10.4 %collective-permute-start.3 = (bf16[256,512]{1,0:T(8,128)(2,1)S(1)}, bf16[256,512]{1,0:T(8,128)(2,1)S(1)}, u32[]{:S(2)}, u32[]{:S(2)}) collective-permute-start(bf16[256,512]{1,0:T(8,128)(2,1)S(1)} %get-tuple-element.91.refs_5_.refs_4_), channel_id=1, source_target_pairs={{0,2},{1,3},{2,4},{3,5},{4,6},{5,7},{6,0},{7,1},{8,10},{9,11},{10,... | collective-permute-start | bytes 786440 | tf_op jit(solution)/shard_map/ppermute | solution.py:36
  60.9 18.5 %collective-permute-start.20 = (bf16[512,512]{1,0:T(8,128)(2,1)S(1)}, bf16[512,512]{1,0:T(8,128)(2,1)S(1)}, u32[]{:S(2)}, u32[]{:S(2)}) collective-permute-start(bf16[512,512]{1,0:T(8,128)(2,1)S(1)} %pad_maximum_fusion.1.refs_20_.refs_19_), channel_id=1, source_target_pairs={{0,32},{8,40},{16,48},{24,56},{32,64},{40,72},{48,80},{56,88},{64,... | collective-permute-start | bytes 1572872 | tf_op jit(solution)/shard_map/ppermute | solution.py:84
  62.5 19.3 %collective-permute-start.30 = (bf16[512,512]{1,0:T(8,128)(2,1)S(1)}, bf16[512,512]{1,0:T(8,128)(2,1)S(1)}, u32[]{:S(2)}, u32[]{:S(2)}) collective-permute-start(bf16[512,512]{1,0:T(8,128)(2,1)S(1)} %pad_maximum_fusion.2.refs_28_.refs_27_), channel_id=1, source_target_pairs={{0,8},{8,16},{16,24},{24,0},{32,40},{40,48},{48,56},{56,32},{64,72... | collective-permute-start | bytes 1572872 | tf_op jit(solution)/shard_map/ppermute | solution.py:84
  62.6 19.1 %collective-permute-start.22 = (bf16[512,512]{1,0:T(8,128)(2,1)S(1)}, bf16[512,512]{1,0:T(8,128)(2,1)S(1)}, u32[]{:S(2)}, u32[]{:S(2)}) collective-permute-start(bf16[512,512]{1,0:T(8,128)(2,1)S(1)} %pad_maximum_fusion.1.refs_20_.refs_19_), channel_id=1, source_target_pairs={{0,96},{8,104},{16,112},{24,120},{32,0},{40,8},{48,16},{56,24},{64... | collective-permute-start | bytes 1572872 | tf_op jit(solution)/shard_map/ppermute | solution.py:84
  64.9 18.0 %collective-permute-start.32 = (bf16[512,512]{1,0:T(8,128)(2,1)S(1)}, bf16[512,512]{1,0:T(8,128)(2,1)S(1)}, u32[]{:S(2)}, u32[]{:S(2)}) collective-permute-start(bf16[512,512]{1,0:T(8,128)(2,1)S(1)} %pad_maximum_fusion.2.refs_28_.refs_27_), channel_id=1, source_target_pairs={{0,24},{8,0},{16,8},{24,16},{32,56},{40,32},{48,40},{56,48},{64,88... | collective-permute-start | bytes 1572872 | tf_op jit(solution)/shard_map/ppermute | solution.py:84
  71.3 17.8 %collective-permute-start.23 = (bf16[512,512]{1,0:T(8,128)(2,1)S(1)}, bf16[512,512]{1,0:T(8,128)(2,1)}, u32[]{:S(2)}, u32[]{:S(2)}) collective-permute-start(bf16[512,512]{1,0:T(8,128)(2,1)S(1)} %constant_dynamic-update-slice_fusion.refs_21_.refs_20_), channel_id=1, source_target_pairs={{0,96},{8,104},{16,112},{24,120},{32,0},{40,8},{48,16},{56,24},{64... | collective-permute-start | bytes 1572872 | tf_op jit(solution)/shard_map/ppermute | solution.py:84
  79.3 16.4 %collective-permute-start.33 = (bf16[512,512]{1,0:T(8,128)(2,1)S(1)}, bf16[512,512]{1,0:T(8,128)(2,1)}, u32[]{:S(2)}, u32[]{:S(2)}) collective-permute-start(bf16[512,512]{1,0:T(8,128)(2,1)S(1)} %constant_dynamic-update-slice_fusion.3.refs_29_.refs_28_), channel_id=1, source_target_pairs={{0,24},{8,0},{16,8},{24,16},{32,56},{40,32},{48,40},{56,48},{64,88... | collective-permute-start | bytes 1572872 | tf_op jit(solution)/shard_map/ppermute | solution.py:84
  81.7 16.6 %collective-permute-start.21 = (bf16[512,512]{1,0:T(8,128)(2,1)S(1)}, bf16[512,512]{1,0:T(8,128)(2,1)S(1)}, u32[]{:S(2)}, u32[]{:S(2)}) collective-permute-start(bf16[512,512]{1,0:T(8,128)(2,1)S(1)} %constant_dynamic-update-slice_fusion.refs_21_.refs_20_), channel_id=1, source_target_pairs={{0,32},{8,40},{16,48},{24,56},{32,64},{40,72},{48,80},{56,88},{64,... | collective-permute-start | bytes 1572872 | tf_op jit(solution)/shard_map/ppermute | solution.py:84
  84.0 20.9 %collective-permute-start.31 = (bf16[512,512]{1,0:T(8,128)(2,1)S(1)}, bf16[512,512]{1,0:T(8,128)(2,1)S(1)}, u32[]{:S(2)}, u32[]{:S(2)}) collective-permute-start(bf16[512,512]{1,0:T(8,128)(2,1)S(1)} %constant_dynamic-update-slice_fusion.3.refs_29_.refs_28_), channel_id=1, source_target_pairs={{0,8},{8,16},{16,24},{24,0},{32,40},{40,48},{48,56},{56,32},{64,72... | collective-permute-start | bytes 1572872 | tf_op jit(solution)/shard_map/ppermute | solution.py:84
  84.4 35.0 %collective-permute-start.24 = (bf16[512,512]{1,0:T(8,128)(2,1)S(1)}, bf16[512,512]{1,0:T(8,128)(2,1)}, u32[]{:S(2)}, u32[]{:S(2)}) collective-permute-start(bf16[512,512]{1,0:T(8,128)(2,1)S(1)} %collective-permute-done.20.refs_22_.refs_21_), channel_id=1, source_target_pairs={{0,32},{8,40},{16,48},{24,56},{32,64},{40,72},{48,80},{56,88},{64,... | collective-permute-start | bytes 1572872 | tf_op jit(solution)/shard_map/ppermute | solution.py:84
  89.1 33.3 %collective-permute-start.34 = (bf16[512,512]{1,0:T(8,128)(2,1)S(1)}, bf16[512,512]{1,0:T(8,128)(2,1)}, u32[]{:S(2)}, u32[]{:S(2)}) collective-permute-start(bf16[512,512]{1,0:T(8,128)(2,1)S(1)} %collective-permute-done.30.refs_30_.refs_29_), channel_id=1, source_target_pairs={{0,8},{8,16},{16,24},{24,0},{32,40},{40,48},{48,56},{56,32},{64,72... | collective-permute-start | bytes 1572872 | tf_op jit(solution)/shard_map/ppermute | solution.py:84
  95.7 26.6 %collective-permute-start.25 = (bf16[512,512]{1,0:T(8,128)(2,1)}, bf16[512,512]{1,0:T(8,128)(2,1)}, u32[]{:S(2)}, u32[]{:S(2)}) collective-permute-start(bf16[512,512]{1,0:T(8,128)(2,1)} %collective-permute-done.23.refs_25_.refs_24_), channel_id=1, source_target_pairs={{0,96},{8,104},{16,112},{24,120},{32,0},{40,8},{48,16},{56,24},{64... | collective-permute-start | bytes 1572872 | tf_op jit(solution)/shard_map/ppermute | solution.py:84
  98.4 24.0 %collective-permute-start.35 = (bf16[512,512]{1,0:T(8,128)(2,1)}, bf16[512,512]{1,0:T(8,128)(2,1)}, u32[]{:S(2)}, u32[]{:S(2)}) collective-permute-start(bf16[512,512]{1,0:T(8,128)(2,1)} %collective-permute-done.33.refs_33_.refs_32_), channel_id=1, source_target_pairs={{0,24},{8,0},{16,8},{24,16},{32,56},{40,32},{48,40},{56,48},{64,88... | collective-permute-start | bytes 1572872 | tf_op jit(solution)/shard_map/ppermute | solution.py:84
  143.1 18.2 %all-to-all-start.1 = ((f32[16,4,512]{2,1,0:T(4,128)}), f32[16,4,512]{2,1,0:T(4,128)S(1)}, u32[]{:S(2)}, u32[]{:S(2)}) async-start(f32[16,4,512]{2,1,0:T(4,128)} %get-tuple-element.37), calls=%async_computation.1 | async-start | bytes 262144 | tf_op jit(solution)/shard_map/all_to_all | solution.py:569
  175.8 11.1 %collective-permute-start.40 = (bf16[256,512]{1,0:T(8,128)(2,1)S(1)}, bf16[256,512]{1,0:T(8,128)(2,1)S(1)}, u32[]{:S(2)}, u32[]{:S(2)}) collective-permute-start(bf16[256,512]{1,0:T(8,128)(2,1)S(1)} %get-tuple-element.80), channel_id=1, source_target_pairs={{0,6},{1,7},{2,0},{3,1},{4,2},{5,3},{6,4},{7,5},{8,14},{9,15},{10,... | collective-permute-start | bytes 786440 | tf_op jit(solution)/shard_map/ppermute | solution.py:36
  181.8 11.0 %collective-permute-start.39 = (bf16[256,512]{1,0:T(8,128)(2,1)S(1)}, bf16[256,512]{1,0:T(8,128)(2,1)S(1)}, u32[]{:S(2)}, u32[]{:S(2)}) collective-permute-start(bf16[256,512]{1,0:T(8,128)(2,1)S(1)} %get-tuple-element.78), channel_id=1, source_target_pairs={{0,2},{1,3},{2,4},{3,5},{4,6},{5,7},{6,0},{7,1},{8,10},{9,11},{10,... | collective-permute-start | bytes 786440 | tf_op jit(solution)/shard_map/ppermute | solution.py:36
  194.0 10.8 %all-to-all-start.2 = ((bf16[8,4,512]{2,1,0:T(4,128)(2,1)}), bf16[8,4,512]{2,1,0:T(4,128)(2,1)S(1)}, u32[]{:S(2)}, u32[]{:S(2)}) async-start(bf16[8,4,512]{2,1,0:T(4,128)(2,1)} %broadcast_in_dim.5), calls=%async_computation.2 | async-start | bytes 65536 | tf_op jit(solution)/shard_map/all_to_all | solution.py:53
  199.5 17.8 %collective-permute-start.46 = (bf16[256,512]{1,0:T(8,128)(2,1)S(1)}, bf16[256,512]{1,0:T(8,128)(2,1)S(1)}, u32[]{:S(2)}, u32[]{:S(2)}) collective-permute-start(bf16[256,512]{1,0:T(8,128)(2,1)S(1)} %get-tuple-element.70.refs_4_.refs_3_), channel_id=1, source_target_pairs={{0,2},{1,3},{2,4},{3,5},{4,6},{5,7},{6,0},{7,1},{8,10},{9,11},{10,... | collective-permute-start | bytes 786440 | tf_op jit(solution)/shard_map/ppermute | solution.py:36
  200.8 16.5 %collective-permute-start.49 = (bf16[256,512]{1,0:T(8,128)(2,1)S(1)}, bf16[256,512]{1,0:T(8,128)(2,1)S(1)}, u32[]{:S(2)}, u32[]{:S(2)}) collective-permute-start(bf16[256,512]{1,0:T(8,128)(2,1)S(1)} %get-tuple-element.69.refs_5_.refs_4_), channel_id=1, source_target_pairs={{0,6},{1,7},{2,0},{3,1},{4,2},{5,3},{6,4},{7,5},{8,14},{9,15},{10,... | collective-permute-start | bytes 786440 | tf_op jit(solution)/shard_map/ppermute | solution.py:36
  202.2 15.2 %collective-permute-start.47 = (bf16[256,512]{1,0:T(8,128)(2,1)S(1)}, bf16[256,512]{1,0:T(8,128)(2,1)S(1)}, u32[]{:S(2)}, u32[]{:S(2)}) collective-permute-start(bf16[256,512]{1,0:T(8,128)(2,1)S(1)} %get-tuple-element.69.refs_5_.refs_4_), channel_id=1, source_target_pairs={{0,2},{1,3},{2,4},{3,5},{4,6},{5,7},{6,0},{7,1},{8,10},{9,11},{10,... | collective-permute-start | bytes 786440 | tf_op jit(solution)/shard_map/ppermute | solution.py:36
  202.3 17.7 %collective-permute-start.48 = (bf16[256,512]{1,0:T(8,128)(2,1)S(1)}, bf16[256,512]{1,0:T(8,128)(2,1)S(1)}, u32[]{:S(2)}, u32[]{:S(2)}) collective-permute-start(bf16[256,512]{1,0:T(8,128)(2,1)S(1)} %get-tuple-element.70.refs_4_.refs_3_), channel_id=1, source_target_pairs={{0,6},{1,7},{2,0},{3,1},{4,2},{5,3},{6,4},{7,5},{8,14},{9,15},{10,... | collective-permute-start | bytes 786440 | tf_op jit(solution)/shard_map/ppermute | solution.py:36
  249.3 20.4 %all-to-all-start.3 = ((f32[16,4,512]{2,1,0:T(4,128)}), f32[16,4,512]{2,1,0:T(4,128)S(1)}, u32[]{:S(2)}, u32[]{:S(2)}) async-start(f32[16,4,512]{2,1,0:T(4,128)} %get-tuple-element.53), calls=%async_computation.3 | async-start | bytes 262144 | tf_op jit(solution)/shard_map/all_to_all | solution.py:569
  282.9 10.5 %collective-permute-start.64 = (bf16[256,512]{1,0:T(8,128)(2,1)S(1)}, bf16[256,512]{1,0:T(8,128)(2,1)S(1)}, u32[]{:S(2)}, u32[]{:S(2)}) collective-permute-start(bf16[256,512]{1,0:T(8,128)(2,1)S(1)} %get-tuple-element.76), channel_id=1, source_target_pairs={{0,6},{1,7},{2,0},{3,1},{4,2},{5,3},{6,4},{7,5},{8,14},{9,15},{10,... | collective-permute-start | bytes 786440 | tf_op jit(solution)/shard_map/ppermute | solution.py:36
  289.0 11.0 %collective-permute-start.63 = (bf16[256,512]{1,0:T(8,128)(2,1)S(1)}, bf16[256,512]{1,0:T(8,128)(2,1)S(1)}, u32[]{:S(2)}, u32[]{:S(2)}) collective-permute-start(bf16[256,512]{1,0:T(8,128)(2,1)S(1)} %get-tuple-element.74), channel_id=1, source_target_pairs={{0,2},{1,3},{2,4},{3,5},{4,6},{5,7},{6,0},{7,1},{8,10},{9,11},{10,... | collective-permute-start | bytes 786440 | tf_op jit(solution)/shard_map/ppermute | solution.py:36
  (100 other events, 1213.8 us)
Sparse Core Ops, SparseCore 0:
  9.5 61.6 all-gather.2
  73.3 106.7 all-gather.4
where the time goes:
time: 310 us; the launch traced here: 308 us
  starting transfers between devices  109 us (35%)
  waiting for transfers between devices  92.3 us (30%)
  Pallas kernels  70.8 us (23%)
  local copies, waits for them, and re-layouts  17 us (5%)
  between operations  14.4 us (5%)
  other arithmetic  4.28 us (1%)
    ppermute x20, waiting for transfers between devices, along_plane(): return lax.ppermute(array, 'sp', pairs)  48.5 us
    ppermute x44, starting transfers between devices, shifted(): return lax.ppermute(array, axis, [(i, move(i)) for i in range(count)])  48.1 us
    ppermute x44, waiting for transfers between devices, shifted(): return lax.ppermute(array, axis, [(i, move(i)) for i in range(count)])  37.1 us
    ppermute x20, starting transfers between devices, along_plane(): return lax.ppermute(array, 'sp', pairs)  27.5 us
    pallas_call x2, Pallas kernels, gate_rows(): pl.pallas_call(lambda *refs: gate_body(layer, which, *refs), out_shape=[j...  25.4 us
    pallas_call x2, Pallas kernels, value_rows(): pl.pallas_call(lambda *refs: value_body(layer, *refs), out_shape=jax.Shap...  23.5 us
    all_to_all x2, starting transfers between devices, per_device(): edges = lax.all_to_all(edge, 'sp', 0, 0, tiled=True)  13.2 us
    pallas_call x2, Pallas kernels, scanned(): pl.pallas_call(scan_body, grid_spec=pltpu.PrefetchScalarGridSpec(num_scal...  13 us
  transfers between devices with their start and end apart: 74, of which 30 were waited for; matrix products, arithmetic and copies ran while one was open for 2% of the time, Pallas kernels for 17%

commit v1 on v0

--- a/solution.py
+++ b/solution.py
@@ -188,27 +188,13 @@
     ]
 
 
-WINDOW = 8
-
-
-def opened(copies):
-    for copy in copies[:WINDOW]:
-        copy.start()
-
-
-def awaited(copies, first, last):
-    for n in range(first, last):
-        copies[n].wait()
-        if n + WINDOW < len(copies):
-            copies[n + WINDOW].start()
-
-
 def scaled_rows(layer, rank, gain, copies, halo, rows, squares):
     width = rows.shape[2]
     half = (rows.shape[1] - (0 if halo is None else HALO)) // 2
     step = 64
     for k, (dx, flip) in enumerate(ARRIVE):
-        awaited(copies, 2 * k, 2 * k + 2)
+        copies[2 * k].wait()
+        copies[2 * k + 1].wait()
         block = block_of(rank, dx, flip)
         scale = gain[layer : layer + 1, pl.ds(pl.multiple_of(block * width, width), width)]
 
@@ -237,10 +223,12 @@
     pieces, sources = refs[:16], refs[16:-7]
     out, rows, squares, value_in, total, sems, piece_sems = refs[-7:]
     values = weight_copies(sources, 0, place[0], value_in, sems)
-    copies = piece_copies(rank[0], pieces, rows, piece_sems) + values
-    opened(copies)
-    scaled_rows(layer, rank[0], gain, copies, halo, rows, squares)
-    awaited(copies, 16, len(copies))
+    arriving = piece_copies(rank[0], pieces, rows, piece_sems)
+    for copy in arriving + values:
+        copy.start()
+    scaled_rows(layer, rank[0], gain, arriving, halo, rows, squares)
+    for copy in values:
+        copy.wait()
     contracted(rows, value_in, total)
     out[...] = (total[...] * row_scale(squares, out.shape[1] * len(ARRIVE))).astype(BF16)
 
@@ -250,13 +238,18 @@
     out, out_in, rows, squares, gate_in, total, sems, out_sems, piece_sems = refs[-9:]
     gates = weight_copies(sources, 1, place[0], gate_in, sems)
     others = block_copies(full, which, rank[0], LEAVE, out_in, out_sems)
-    copies = piece_copies(rank[0], pieces, rows, piece_sems) + gates + others
-    opened(copies)
-    scaled_rows(layer, rank[0], gain, copies, None, rows, squares)
-    awaited(copies, 16, 16 + len(gates))
+    arriving = piece_copies(rank[0], pieces, rows, piece_sems)
+    for copy in arriving + gates:
+        copy.start()
+    scaled_rows(layer, rank[0], gain, arriving, None, rows, squares)
+    for copy in gates:
+        copy.wait()
+    for copy in others:
+        copy.start()
     contracted(rows, gate_in, total)
     out[...] = (total[...] * row_scale(squares, out.shape[1] * len(ARRIVE))).astype(BF16)
-    awaited(copies, 16 + len(gates), len(copies))
+    for copy in others:
+        copy.wait()
 
 
 def in_smem():

time: 310 us -> 303 us (0.977)
  Pallas kernels: 70.8 us -> 64.1 us
    pallas_call x2, Pallas kernels: 25.4 us -> 21.8 us  [gate_rows(): pl.pallas_call(lambda *refs: gate_body(layer, which, *refs), out_shape=[j...]
  transfers between devices with their start and end apart: 74 -> 74, of which waited for: 30 -> 30; matrix products, arithmetic and copies ran while one was open for 2% -> 2% of each run, Pallas kernels for 17% -> 15%
where the time goes in v1:
time: 303 us; the launch traced here: 301 us
  starting transfers between devices  109 us (36%)
  waiting for transfers between devices  92.3 us (30%)
  Pallas kernels  64.1 us (21%)
  local copies, waits for them, and re-layouts  17.1 us (6%)
  between operations  14.4 us (5%)
  other arithmetic  4.28 us (1%)
    ppermute x20, waiting for transfers between devices, along_plane(): return lax.ppermute(array, 'sp', pairs)  48.5 us
    ppermute x44, starting transfers between devices, shifted(): return lax.ppermute(array, axis, [(i, move(i)) for i in range(count)])  47.7 us
    ppermute x44, waiting for transfers between devices, shifted(): return lax.ppermute(array, axis, [(i, move(i)) for i in range(count)])  37.1 us
    ppermute x20, starting transfers between devices, along_plane(): return lax.ppermute(array, 'sp', pairs)  27.5 us
    pallas_call x2, Pallas kernels, gate_rows(): pl.pallas_call(lambda *refs: gate_body(layer, which, *refs), out_shape=[j...  21.8 us
    pallas_call x2, Pallas kernels, value_rows(): pl.pallas_call(lambda *refs: value_body(layer, *refs), out_shape=jax.Shap...  20.4 us
    all_to_all x2, starting transfers between devices, per_device(): edges = lax.all_to_all(edge, 'sp', 0, 0, tiled=True)  13.3 us
    pallas_call x2, Pallas kernels, scanned(): pl.pallas_call(scan_body, grid_spec=pltpu.PrefetchScalarGridSpec(num_scal...  13 us
  transfers between devices with their start and end apart: 74, of which 30 were waited for; matrix products, arithmetic and copies ran while one was open for 2% of the time, Pallas kernels for 15%

profile of v1, /device:TPU:1, one launch (start us, length us, event | category | flops | bytes accessed | tf_op | source)
XLA Modules:
  0.0 301.3 jit_solution(12215773356006304886)
XLA Ops:
  11.5 5.8 %all-to-all-start = ((bf16[8,4,512]{2,1,0:T(4,128)(2,1)}), bf16[8,4,512]{2,1,0:T(4,128)(2,1)S(1)}, u32[]{:S(2)}, u32[]{:S(2)}) async-start(bf16[8,4,512]{2,1,0:T(4,128)(2,1)} %broadcast_in_dim.4), calls=%async_computation | async-start | bytes 65536 | tf_op jit(solution)/shard_map/all_to_all | solution.py:53
  17.4 2.8 collective-permute-start.17
  22.0 3.2 %collective-permute-start = (bf16[8,2,512]{2,1,0:T(2,128)(2,1)S(1)}, bf16[8,2,512]{2,1,0:T(2,128)(2,1)S(1)}, u32[]{:S(2)}, u32[]{:S(2)}) collective-permute-start(bf16[8,2,512]{2,1,0:T(2,128)(2,1)S(1)} %get-tuple-element.99), channel_id=1, source_target_pairs={{0,8},{8,16},{16,24},{24,32},{32,40},{40,48},{48,56},{56,64},{64,7... | collective-permute-start | bytes 49160 | tf_op jit(solution)/shard_map/ppermute | solution.py:54
  26.6 6.7 %collective-permute-start.27 = (bf16[256,512]{1,0:T(8,128)(2,1)S(1)}, bf16[256,512]{1,0:T(8,128)(2,1)S(1)}, u32[]{:S(2)}, u32[]{:S(2)}) collective-permute-start(bf16[256,512]{1,0:T(8,128)(2,1)S(1)} %pad_maximum_fusion.4), channel_id=1, source_target_pairs={{0,96},{8,104},{16,112},{24,120},{32,0},{40,8},{48,16},{56,24},{64... | collective-permute-start | bytes 786440 | tf_op jit(solution)/shard_map/ppermute | solution.py:84
  36.1 3.4 %collective-permute-done.27 = bf16[256,512]{1,0:T(8,128)(2,1)S(1)} collective-permute-done((bf16[256,512]{1,0:T(8,128)(2,1)S(1)}, bf16[256,512]{1,0:T(8,128)(2,1)S(1)}, u32[]{:S(2)}, u32[]{:S(2)}) %collective-permute-start.27) | collective-permute-done | bytes 262176 | tf_op jit(solution)/shard_map/ppermute | solution.py:84
  51.3 3.4 %collective-permute-done.18 = bf16[128,512]{1,0:T(8,128)(2,1)S(1)} collective-permute-done((bf16[128,512]{1,0:T(8,128)(2,1)S(1)}, bf16[128,512]{1,0:T(8,128)(2,1)S(1)}, u32[]{:S(2)}, u32[]{:S(2)}) %collective-permute-start.18) | collective-permute-done | bytes 131104 | tf_op jit(solution)/shard_map/ppermute | solution.py:84
  57.4 2.7 collective-permute-start.13
  64.9 2.7 collective-permute-start.32
  72.9 6.5 %collective-permute-done.20.refs_22_.refs_21_ = bf16[512,512]{1,0:T(8,128)(2,1)S(1)} collective-permute-done((bf16[512,512]{1,0:T(8,128)(2,1)S(1)}, bf16[512,512]{1,0:T(8,128)(2,1)S(1)}, u32[]{:S(2)}, u32[]{:S(2)}) %collective-permute-start.20) | collective-permute-done | bytes 524320 | tf_op jit(solution)/shard_map/ppermute | solution.py:84
  84.7 4.4 %collective-permute-done.23.refs_25_.refs_24_ = bf16[512,512]{1,0:T(8,128)(2,1)} collective-permute-done((bf16[512,512]{1,0:T(8,128)(2,1)S(1)}, bf16[512,512]{1,0:T(8,128)(2,1)}, u32[]{:S(2)}, u32[]{:S(2)}) %collective-permute-start.23) | collective-permute-done | bytes 524320 | tf_op jit(solution)/shard_map/ppermute | solution.py:84
  90.4 5.4 %collective-permute-done.33.refs_33_.refs_32_ = bf16[512,512]{1,0:T(8,128)(2,1)} collective-permute-done((bf16[512,512]{1,0:T(8,128)(2,1)S(1)}, bf16[512,512]{1,0:T(8,128)(2,1)}, u32[]{:S(2)}, u32[]{:S(2)}) %collective-permute-start.33) | collective-permute-done | bytes 524320 | tf_op jit(solution)/shard_map/ppermute | solution.py:84
  100.2 4.7 %collective-permute-done.31.refs_31_.refs_30_ = bf16[512,512]{1,0:T(8,128)(2,1)S(1)} collective-permute-done((bf16[512,512]{1,0:T(8,128)(2,1)S(1)}, bf16[512,512]{1,0:T(8,128)(2,1)S(1)}, u32[]{:S(2)}, u32[]{:S(2)}) %collective-permute-start.31) | collective-permute-done | bytes 524320 | tf_op jit(solution)/shard_map/ppermute | solution.py:84
  104.9 14.4 %collective-permute-done.24.refs_26_.refs_25_ = bf16[512,512]{1,0:T(8,128)(2,1)} collective-permute-done((bf16[512,512]{1,0:T(8,128)(2,1)S(1)}, bf16[512,512]{1,0:T(8,128)(2,1)}, u32[]{:S(2)}, u32[]{:S(2)}) %collective-permute-start.24) | collective-permute-done | bytes 524320 | tf_op jit(solution)/shard_map/ppermute | solution.py:84
  119.4 3.0 collective-permute-done.34.refs_34_.refs_33_
  122.4 10.8 %value_rows.2.mix = bf16[528,512]{1,0:T(8,128)(2,1)} custom-call(s32[1]{0:T(128)} %bitcast.4.refs_0_.rank, s32[1]{0:T(128)} %bitcast.3.refs_1_.place, f32[2,4096]{1,0:T(2,128)} %refs_2_.7, bf16[8,16,512]{2,1,0:T(8,128)(2,1)} %maximum_maximum_fusion.refs_3_, bf16[256,512]{1,0:T(8,128)(2,1)} %copy-done.21, bf16[256,512]{1,0:T(8,128)(2,1)} %copy-done.20, ...), custom_call_target="tpu_custom_call" | custom-call | flops 2214592512 | bytes 4194304 | tf_op jit(solution)/shard_map/value_rows/pallas_call | solution.py:279
  134.4 6.5 %scan.2 = (f32[512,512]{1,0:T(8,128)S(1)}, f32[512,512]{1,0:T(8,128)S(1)}, f32[512,512]{1,0:T(8,128)S(1)}, f32[4,8,512]{2,1,0:T(8,128)S(1)}, f32[16,4,512]{2,1,0:T(4,128)}) custom-call(s32[1]{0:T(128)} %bitcast.4.refs_0_.rank, bf16[528,512]{1,0:T(8,128)(2,1)S(1)} %copy-done.3, f32[2,4,4096]{2,1,0:T(4,128)S(1)} %copy-done.8, f32[2,2,4096]{2,1,0:T(2,128)S(1)} %copy-done.9, ...), custom_call_target="tpu_custom_call" | custom-call | flops 10000000000 | bytes 4000000 | tf_op jit(solution)/shard_map/scan/pallas_call | solution.py:412
  140.9 4.2 %all-to-all-start.1 = ((f32[16,4,512]{2,1,0:T(4,128)}), f32[16,4,512]{2,1,0:T(4,128)S(1)}, u32[]{:S(2)}, u32[]{:S(2)}) async-start(f32[16,4,512]{2,1,0:T(4,128)} %get-tuple-element.37), calls=%async_computation.1 | async-start | bytes 262144 | tf_op jit(solution)/shard_map/all_to_all | solution.py:562
  145.1 11.0 %gate_rows.2 = (bf16[512,512]{1,0:T(8,128)(2,1)}, bf16[8,512,512]{2,1,0:T(8,128)(2,1)}) custom-call(s32[1]{0:T(128)} %bitcast.4.refs_0_.rank, s32[1]{0:T(128)} %bitcast.3.refs_1_.place, f32[2,4096]{1,0:T(2,128)} %refs_2_.7, bf16[256,512]{1,0:T(8,128)(2,1)} %copy-done.21, bf16[256,512]{1,0:T(8,128)(2,1)} %copy-done.20, bf16[256,512]{1,0:T(8,128)(2,1)} %copy-done.41, ...), custom_call_target="tpu_custom_call" | custom-call | flops 2147483648 | bytes 4194304 | tf_op jit(solution)/shard_map/gate_rows/pallas_call | solution.py:302
  171.8 4.4 %collective-permute-done.38 = bf16[256,512]{1,0:T(8,128)(2,1)S(1)} collective-permute-done((bf16[256,512]{1,0:T(8,128)(2,1)S(1)}, bf16[256,512]{1,0:T(8,128)(2,1)S(1)}, u32[]{:S(2)}, u32[]{:S(2)}) %collective-permute-start.38) | collective-permute-done | bytes 262176 | tf_op jit(solution)/shard_map/ppermute | solution.py:36
  181.8 5.6 %collective-permute-done.39 = bf16[256,512]{1,0:T(8,128)(2,1)S(1)} collective-permute-done((bf16[256,512]{1,0:T(8,128)(2,1)S(1)}, bf16[256,512]{1,0:T(8,128)(2,1)S(1)}, u32[]{:S(2)}, u32[]{:S(2)}) %collective-permute-start.39) | collective-permute-done | bytes 262176 | tf_op jit(solution)/shard_map/ppermute | solution.py:36
  188.6 5.5 %all-to-all-start.2 = ((bf16[8,4,512]{2,1,0:T(4,128)(2,1)}), bf16[8,4,512]{2,1,0:T(4,128)(2,1)S(1)}, u32[]{:S(2)}, u32[]{:S(2)}) async-start(bf16[8,4,512]{2,1,0:T(4,128)(2,1)} %broadcast_in_dim.5), calls=%async_computation.2 | async-start | bytes 65536 | tf_op jit(solution)/shard_map/all_to_all | solution.py:53
  199.4 3.5 %collective-permute-start.44 = (bf16[8,2,512]{2,1,0:T(2,128)(2,1)S(1)}, bf16[8,2,512]{2,1,0:T(2,128)(2,1)S(1)}, u32[]{:S(2)}, u32[]{:S(2)}) collective-permute-start(bf16[8,2,512]{2,1,0:T(2,128)(2,1)S(1)} %get-tuple-element.97), channel_id=1, source_target_pairs={{0,8},{8,16},{16,24},{24,32},{32,40},{40,48},{48,56},{56,64},{64,7... | collective-permute-start | bytes 49160 | tf_op jit(solution)/shard_map/ppermute | solution.py:54
  205.0 4.0 %collective-permute-done.45 = bf16[8,2,512]{2,1,0:T(2,128)(2,1)S(1)} collective-permute-done((bf16[8,2,512]{2,1,0:T(2,128)(2,1)S(1)}, bf16[8,2,512]{2,1,0:T(2,128)(2,1)S(1)}, u32[]{:S(2)}, u32[]{:S(2)}) %collective-permute-start.45) | collective-permute-done | bytes 16416 | tf_op jit(solution)/shard_map/ppermute | solution.py:55
  211.8 2.6 collective-permute-start.51
  215.9 4.5 %collective-permute-done.50.refs_10_.refs_9_ = bf16[256,512]{1,0:T(8,128)(2,1)S(1)} collective-permute-done((bf16[256,512]{1,0:T(8,128)(2,1)S(1)}, bf16[256,512]{1,0:T(8,128)(2,1)S(1)}, u32[]{:S(2)}, u32[]{:S(2)}) %collective-permute-start.50) | collective-permute-done | bytes 262176 | tf_op jit(solution)/shard_map/ppermute | solution.py:36
  224.6 9.6 %value_rows.3.mix = bf16[528,512]{1,0:T(8,128)(2,1)} custom-call(s32[1]{0:T(128)} %bitcast.4.refs_0_.rank, s32[1]{0:T(128)} %bitcast.3.refs_1_.place, f32[2,4096]{1,0:T(2,128)} %refs_2_.7, bf16[8,16,512]{2,1,0:T(8,128)(2,1)} %maximum_maximum_fusion.1.refs_3_, bf16[256,512]{1,0:T(8,128)(2,1)} %copy-done.16, bf16[256,512]{1,0:T(8,128)(2,1)} %copy-done.14, ...), custom_call_target="tpu_custom_call" | custom-call | flops 2214592512 | bytes 4194304 | tf_op jit(solution)/shard_map/value_rows/pallas_call | solution.py:279
  236.5 6.5 %scan.3 = (f32[512,512]{1,0:T(8,128)S(1)}, f32[512,512]{1,0:T(8,128)S(1)}, f32[512,512]{1,0:T(8,128)S(1)}, f32[4,8,512]{2,1,0:T(8,128)S(1)}, f32[16,4,512]{2,1,0:T(4,128)}) custom-call(s32[1]{0:T(128)} %bitcast.4.refs_0_.rank, bf16[528,512]{1,0:T(8,128)(2,1)S(1)} %copy-done.2, f32[2,4,4096]{2,1,0:T(4,128)S(1)} %copy-done.8, f32[2,2,4096]{2,1,0:T(2,128)S(1)} %copy-done.9, ...), custom_call_target="tpu_custom_call" | custom-call | flops 10000000000 | bytes 4000000 | tf_op jit(solution)/shard_map/scan/pallas_call | solution.py:412
  242.9 9.1 %all-to-all-start.3 = ((f32[16,4,512]{2,1,0:T(4,128)}), f32[16,4,512]{2,1,0:T(4,128)S(1)}, u32[]{:S(2)}, u32[]{:S(2)}) async-start(f32[16,4,512]{2,1,0:T(4,128)} %get-tuple-element.53), calls=%async_computation.3 | async-start | bytes 262144 | tf_op jit(solution)/shard_map/all_to_all | solution.py:562
  252.0 10.8 %gate_rows.3 = (bf16[512,512]{1,0:T(8,128)(2,1)}, bf16[8,512,512]{2,1,0:T(8,128)(2,1)}) custom-call(s32[1]{0:T(128)} %bitcast.4.refs_0_.rank, s32[1]{0:T(128)} %bitcast.3.refs_1_.place, f32[2,4096]{1,0:T(2,128)} %refs_2_.7, bf16[256,512]{1,0:T(8,128)(2,1)} %copy-done.16, bf16[256,512]{1,0:T(8,128)(2,1)} %copy-done.14, bf16[256,512]{1,0:T(8,128)(2,1)} %copy-done.28, ...), custom_call_target="tpu_custom_call" | custom-call | flops 2147483648 | bytes 4194304 | tf_op jit(solution)/shard_map/gate_rows/pallas_call | solution.py:302
  273.2 2.7 collective-permute-start.66
  277.6 4.3 %collective-permute-done.62 = bf16[256,512]{1,0:T(8,128)(2,1)S(1)} collective-permute-done((bf16[256,512]{1,0:T(8,128)(2,1)S(1)}, bf16[256,512]{1,0:T(8,128)(2,1)S(1)}, u32[]{:S(2)}, u32[]{:S(2)}) %collective-permute-start.62) | collective-permute-done | bytes 262176 | tf_op jit(solution)/shard_map/ppermute | solution.py:36
  287.5 5.6 %collective-permute-done.63 = bf16[256,512]{1,0:T(8,128)(2,1)S(1)} collective-permute-done((bf16[256,512]{1,0:T(8,128)(2,1)S(1)}, bf16[256,512]{1,0:T(8,128)(2,1)S(1)}, u32[]{:S(2)}, u32[]{:S(2)}) %collective-permute-start.63) | collective-permute-done | bytes 262176 | tf_op jit(solution)/shard_map/ppermute | solution.py:36
  (289 shorter events, 106.6 us)
Async XLA Ops:
  6.5 138.6 %all-gather.3.cloned.1.call-start = ((), (), s32[]{:S(2)}) async-start(), calls=%async_computation.4 | async-start | bytes 4456448 | tf_op jit(solution)/shard_map/all_gather | solution.py:550
  8.4 216.1 %all-gather.5.cloned.1.call-start = ((), (), s32[]{:S(2)}) async-start(), calls=%async_computation.5 | async-start | bytes 13369344 | tf_op jit(solution)/shard_map/all_gather | solution.py:552
  11.5 10.5 %all-to-all-start = ((bf16[8,4,512]{2,1,0:T(4,128)(2,1)}), bf16[8,4,512]{2,1,0:T(4,128)(2,1)S(1)}, u32[]{:S(2)}, u32[]{:S(2)}) async-start(bf16[8,4,512]{2,1,0:T(4,128)(2,1)} %broadcast_in_dim.4), calls=%async_computation | async-start | bytes 65536 | tf_op jit(solution)/shard_map/all_to_all | solution.py:53
  17.4 16.3 %collective-permute-start.17 = (bf16[256,512]{1,0:T(8,128)(2,1)S(1)}, bf16[256,512]{1,0:T(8,128)(2,1)S(1)}, u32[]{:S(2)}, u32[]{:S(2)}) collective-permute-start(bf16[256,512]{1,0:T(8,128)(2,1)S(1)} %pad_maximum_fusion.3), channel_id=1, source_target_pairs={{0,24},{8,0},{16,8},{24,16},{32,56},{40,32},{48,40},{56,48},{64,88... | collective-permute-start | bytes 786440 | tf_op jit(solution)/shard_map/ppermute | solution.py:84
  20.2 15.9 %collective-permute-start.16 = (bf16[256,512]{1,0:T(8,128)(2,1)S(1)}, bf16[256,512]{1,0:T(8,128)(2,1)S(1)}, u32[]{:S(2)}, u32[]{:S(2)}) collective-permute-start(bf16[256,512]{1,0:T(8,128)(2,1)S(1)} %pad_maximum_fusion.3), channel_id=1, source_target_pairs={{0,8},{8,16},{16,24},{24,0},{32,40},{40,48},{48,56},{56,32},{64,72... | collective-permute-start | bytes 786440 | tf_op jit(solution)/shard_map/ppermute | solution.py:84
  22.0 11.3 %collective-permute-start = (bf16[8,2,512]{2,1,0:T(2,128)(2,1)S(1)}, bf16[8,2,512]{2,1,0:T(2,128)(2,1)S(1)}, u32[]{:S(2)}, u32[]{:S(2)}) collective-permute-start(bf16[8,2,512]{2,1,0:T(2,128)(2,1)S(1)} %get-tuple-element.99), channel_id=1, source_target_pairs={{0,8},{8,16},{16,24},{24,32},{32,40},{40,48},{48,56},{56,64},{64,7... | collective-permute-start | bytes 49160 | tf_op jit(solution)/shard_map/ppermute | solution.py:54
  26.6 12.9 %collective-permute-start.27 = (bf16[256,512]{1,0:T(8,128)(2,1)S(1)}, bf16[256,512]{1,0:T(8,128)(2,1)S(1)}, u32[]{:S(2)}, u32[]{:S(2)}) collective-permute-start(bf16[256,512]{1,0:T(8,128)(2,1)S(1)} %pad_maximum_fusion.4), channel_id=1, source_target_pairs={{0,96},{8,104},{16,112},{24,120},{32,0},{40,8},{48,16},{56,24},{64... | collective-permute-start | bytes 786440 | tf_op jit(solution)/shard_map/ppermute | solution.py:84
  33.7 11.7 %collective-permute-start.5 = (bf16[256,512]{1,0:T(8,128)(2,1)S(1)}, bf16[256,512]{1,0:T(8,128)(2,1)S(1)}, u32[]{:S(2)}, u32[]{:S(2)}) collective-permute-start(bf16[256,512]{1,0:T(8,128)(2,1)S(1)} %get-tuple-element.91.refs_5_.refs_4_), channel_id=1, source_target_pairs={{0,6},{1,7},{2,0},{3,1},{4,2},{5,3},{6,4},{7,5},{8,14},{9,15},{10,... | collective-permute-start | bytes 786440 | tf_op jit(solution)/shard_map/ppermute | solution.py:36
  36.1 10.4 %collective-permute-start.3 = (bf16[256,512]{1,0:T(8,128)(2,1)S(1)}, bf16[256,512]{1,0:T(8,128)(2,1)S(1)}, u32[]{:S(2)}, u32[]{:S(2)}) collective-permute-start(bf16[256,512]{1,0:T(8,128)(2,1)S(1)} %get-tuple-element.91.refs_5_.refs_4_), channel_id=1, source_target_pairs={{0,2},{1,3},{2,4},{3,5},{4,6},{5,7},{6,0},{7,1},{8,10},{9,11},{10,... | collective-permute-start | bytes 786440 | tf_op jit(solution)/shard_map/ppermute | solution.py:36
  60.9 18.5 %collective-permute-start.20 = (bf16[512,512]{1,0:T(8,128)(2,1)S(1)}, bf16[512,512]{1,0:T(8,128)(2,1)S(1)}, u32[]{:S(2)}, u32[]{:S(2)}) collective-permute-start(bf16[512,512]{1,0:T(8,128)(2,1)S(1)} %pad_maximum_fusion.1.refs_20_.refs_19_), channel_id=1, source_target_pairs={{0,32},{8,40},{16,48},{24,56},{32,64},{40,72},{48,80},{56,88},{64,... | collective-permute-start | bytes 1572872 | tf_op jit(solution)/shard_map/ppermute | solution.py:84
  62.5 19.3 %collective-permute-start.30 = (bf16[512,512]{1,0:T(8,128)(2,1)S(1)}, bf16[512,512]{1,0:T(8,128)(2,1)S(1)}, u32[]{:S(2)}, u32[]{:S(2)}) collective-permute-start(bf16[512,512]{1,0:T(8,128)(2,1)S(1)} %pad_maximum_fusion.2.refs_28_.refs_27_), channel_id=1, source_target_pairs={{0,8},{8,16},{16,24},{24,0},{32,40},{40,48},{48,56},{56,32},{64,72... | collective-permute-start | bytes 1572872 | tf_op jit(solution)/shard_map/ppermute | solution.py:84
  62.6 19.1 %collective-permute-start.22 = (bf16[512,512]{1,0:T(8,128)(2,1)S(1)}, bf16[512,512]{1,0:T(8,128)(2,1)S(1)}, u32[]{:S(2)}, u32[]{:S(2)}) collective-permute-start(bf16[512,512]{1,0:T(8,128)(2,1)S(1)} %pad_maximum_fusion.1.refs_20_.refs_19_), channel_id=1, source_target_pairs={{0,96},{8,104},{16,112},{24,120},{32,0},{40,8},{48,16},{56,24},{64... | collective-permute-start | bytes 1572872 | tf_op jit(solution)/shard_map/ppermute | solution.py:84
  64.9 18.0 %collective-permute-start.32 = (bf16[512,512]{1,0:T(8,128)(2,1)S(1)}, bf16[512,512]{1,0:T(8,128)(2,1)S(1)}, u32[]{:S(2)}, u32[]{:S(2)}) collective-permute-start(bf16[512,512]{1,0:T(8,128)(2,1)S(1)} %pad_maximum_fusion.2.refs_28_.refs_27_), channel_id=1, source_target_pairs={{0,24},{8,0},{16,8},{24,16},{32,56},{40,32},{48,40},{56,48},{64,88... | collective-permute-start | bytes 1572872 | tf_op jit(solution)/shard_map/ppermute | solution.py:84
  71.3 17.8 %collective-permute-start.23 = (bf16[512,512]{1,0:T(8,128)(2,1)S(1)}, bf16[512,512]{1,0:T(8,128)(2,1)}, u32[]{:S(2)}, u32[]{:S(2)}) collective-permute-start(bf16[512,512]{1,0:T(8,128)(2,1)S(1)} %constant_dynamic-update-slice_fusion.refs_21_.refs_20_), channel_id=1, source_target_pairs={{0,96},{8,104},{16,112},{24,120},{32,0},{40,8},{48,16},{56,24},{64... | collective-permute-start | bytes 1572872 | tf_op jit(solution)/shard_map/ppermute | solution.py:84
  79.3 16.4 %collective-permute-start.33 = (bf16[512,512]{1,0:T(8,128)(2,1)S(1)}, bf16[512,512]{1,0:T(8,128)(2,1)}, u32[]{:S(2)}, u32[]{:S(2)}) collective-permute-start(bf16[512,512]{1,0:T(8,128)(2,1)S(1)} %constant_dynamic-update-slice_fusion.3.refs_29_.refs_28_), channel_id=1, source_target_pairs={{0,24},{8,0},{16,8},{24,16},{32,56},{40,32},{48,40},{56,48},{64,88... | collective-permute-start | bytes 1572872 | tf_op jit(solution)/shard_map/ppermute | solution.py:84
  81.7 16.6 %collective-permute-start.21 = (bf16[512,512]{1,0:T(8,128)(2,1)S(1)}, bf16[512,512]{1,0:T(8,128)(2,1)S(1)}, u32[]{:S(2)}, u32[]{:S(2)}) collective-permute-start(bf16[512,512]{1,0:T(8,128)(2,1)S(1)} %constant_dynamic-update-slice_fusion.refs_21_.refs_20_), channel_id=1, source_target_pairs={{0,32},{8,40},{16,48},{24,56},{32,64},{40,72},{48,80},{56,88},{64,... | collective-permute-start | bytes 1572872 | tf_op jit(solution)/shard_map/ppermute | solution.py:84
  84.0 20.9 %collective-permute-start.31 = (bf16[512,512]{1,0:T(8,128)(2,1)S(1)}, bf16[512,512]{1,0:T(8,128)(2,1)S(1)}, u32[]{:S(2)}, u32[]{:S(2)}) collective-permute-start(bf16[512,512]{1,0:T(8,128)(2,1)S(1)} %constant_dynamic-update-slice_fusion.3.refs_29_.refs_28_), channel_id=1, source_target_pairs={{0,8},{8,16},{16,24},{24,0},{32,40},{40,48},{48,56},{56,32},{64,72... | collective-permute-start | bytes 1572872 | tf_op jit(solution)/shard_map/ppermute | solution.py:84
  84.4 35.0 %collective-permute-start.24 = (bf16[512,512]{1,0:T(8,128)(2,1)S(1)}, bf16[512,512]{1,0:T(8,128)(2,1)}, u32[]{:S(2)}, u32[]{:S(2)}) collective-permute-start(bf16[512,512]{1,0:T(8,128)(2,1)S(1)} %collective-permute-done.20.refs_22_.refs_21_), channel_id=1, source_target_pairs={{0,32},{8,40},{16,48},{24,56},{32,64},{40,72},{48,80},{56,88},{64,... | collective-permute-start | bytes 1572872 | tf_op jit(solution)/shard_map/ppermute | solution.py:84
  89.1 33.3 %collective-permute-start.34 = (bf16[512,512]{1,0:T(8,128)(2,1)S(1)}, bf16[512,512]{1,0:T(8,128)(2,1)}, u32[]{:S(2)}, u32[]{:S(2)}) collective-permute-start(bf16[512,512]{1,0:T(8,128)(2,1)S(1)} %collective-permute-done.30.refs_30_.refs_29_), channel_id=1, source_target_pairs={{0,8},{8,16},{16,24},{24,0},{32,40},{40,48},{48,56},{56,32},{64,72... | collective-permute-start | bytes 1572872 | tf_op jit(solution)/shard_map/ppermute | solution.py:84
  95.7 26.6 %collective-permute-start.25 = (bf16[512,512]{1,0:T(8,128)(2,1)}, bf16[512,512]{1,0:T(8,128)(2,1)}, u32[]{:S(2)}, u32[]{:S(2)}) collective-permute-start(bf16[512,512]{1,0:T(8,128)(2,1)} %collective-permute-done.23.refs_25_.refs_24_), channel_id=1, source_target_pairs={{0,96},{8,104},{16,112},{24,120},{32,0},{40,8},{48,16},{56,24},{64... | collective-permute-start | bytes 1572872 | tf_op jit(solution)/shard_map/ppermute | solution.py:84
  98.4 24.0 %collective-permute-start.35 = (bf16[512,512]{1,0:T(8,128)(2,1)}, bf16[512,512]{1,0:T(8,128)(2,1)}, u32[]{:S(2)}, u32[]{:S(2)}) collective-permute-start(bf16[512,512]{1,0:T(8,128)(2,1)} %collective-permute-done.33.refs_33_.refs_32_), channel_id=1, source_target_pairs={{0,24},{8,0},{16,8},{24,16},{32,56},{40,32},{48,40},{56,48},{64,88... | collective-permute-start | bytes 1572872 | tf_op jit(solution)/shard_map/ppermute | solution.py:84
  140.9 15.3 %all-to-all-start.1 = ((f32[16,4,512]{2,1,0:T(4,128)}), f32[16,4,512]{2,1,0:T(4,128)S(1)}, u32[]{:S(2)}, u32[]{:S(2)}) async-start(f32[16,4,512]{2,1,0:T(4,128)} %get-tuple-element.37), calls=%async_computation.1 | async-start | bytes 262144 | tf_op jit(solution)/shard_map/all_to_all | solution.py:562
  170.3 11.1 %collective-permute-start.40 = (bf16[256,512]{1,0:T(8,128)(2,1)S(1)}, bf16[256,512]{1,0:T(8,128)(2,1)S(1)}, u32[]{:S(2)}, u32[]{:S(2)}) collective-permute-start(bf16[256,512]{1,0:T(8,128)(2,1)S(1)} %get-tuple-element.80), channel_id=1, source_target_pairs={{0,6},{1,7},{2,0},{3,1},{4,2},{5,3},{6,4},{7,5},{8,14},{9,15},{10,... | collective-permute-start | bytes 786440 | tf_op jit(solution)/shard_map/ppermute | solution.py:36
  176.5 10.9 %collective-permute-start.39 = (bf16[256,512]{1,0:T(8,128)(2,1)S(1)}, bf16[256,512]{1,0:T(8,128)(2,1)S(1)}, u32[]{:S(2)}, u32[]{:S(2)}) collective-permute-start(bf16[256,512]{1,0:T(8,128)(2,1)S(1)} %get-tuple-element.78), channel_id=1, source_target_pairs={{0,2},{1,3},{2,4},{3,5},{4,6},{5,7},{6,0},{7,1},{8,10},{9,11},{10,... | collective-permute-start | bytes 786440 | tf_op jit(solution)/shard_map/ppermute | solution.py:36
  188.6 10.8 %all-to-all-start.2 = ((bf16[8,4,512]{2,1,0:T(4,128)(2,1)}), bf16[8,4,512]{2,1,0:T(4,128)(2,1)S(1)}, u32[]{:S(2)}, u32[]{:S(2)}) async-start(bf16[8,4,512]{2,1,0:T(4,128)(2,1)} %broadcast_in_dim.5), calls=%async_computation.2 | async-start | bytes 65536 | tf_op jit(solution)/shard_map/all_to_all | solution.py:53
  194.0 17.6 %collective-permute-start.46 = (bf16[256,512]{1,0:T(8,128)(2,1)S(1)}, bf16[256,512]{1,0:T(8,128)(2,1)S(1)}, u32[]{:S(2)}, u32[]{:S(2)}) collective-permute-start(bf16[256,512]{1,0:T(8,128)(2,1)S(1)} %get-tuple-element.70.refs_4_.refs_3_), channel_id=1, source_target_pairs={{0,2},{1,3},{2,4},{3,5},{4,6},{5,7},{6,0},{7,1},{8,10},{9,11},{10,... | collective-permute-start | bytes 786440 | tf_op jit(solution)/shard_map/ppermute | solution.py:36
  195.4 16.4 %collective-permute-start.49 = (bf16[256,512]{1,0:T(8,128)(2,1)S(1)}, bf16[256,512]{1,0:T(8,128)(2,1)S(1)}, u32[]{:S(2)}, u32[]{:S(2)}) collective-permute-start(bf16[256,512]{1,0:T(8,128)(2,1)S(1)} %get-tuple-element.69.refs_5_.refs_4_), channel_id=1, source_target_pairs={{0,6},{1,7},{2,0},{3,1},{4,2},{5,3},{6,4},{7,5},{8,14},{9,15},{10,... | collective-permute-start | bytes 786440 | tf_op jit(solution)/shard_map/ppermute | solution.py:36
  196.7 15.1 %collective-permute-start.47 = (bf16[256,512]{1,0:T(8,128)(2,1)S(1)}, bf16[256,512]{1,0:T(8,128)(2,1)S(1)}, u32[]{:S(2)}, u32[]{:S(2)}) collective-permute-start(bf16[256,512]{1,0:T(8,128)(2,1)S(1)} %get-tuple-element.69.refs_5_.refs_4_), channel_id=1, source_target_pairs={{0,2},{1,3},{2,4},{3,5},{4,6},{5,7},{6,0},{7,1},{8,10},{9,11},{10,... | collective-permute-start | bytes 786440 | tf_op jit(solution)/shard_map/ppermute | solution.py:36
  196.9 17.6 %collective-permute-start.48 = (bf16[256,512]{1,0:T(8,128)(2,1)S(1)}, bf16[256,512]{1,0:T(8,128)(2,1)S(1)}, u32[]{:S(2)}, u32[]{:S(2)}) collective-permute-start(bf16[256,512]{1,0:T(8,128)(2,1)S(1)} %get-tuple-element.70.refs_4_.refs_3_), channel_id=1, source_target_pairs={{0,6},{1,7},{2,0},{3,1},{4,2},{5,3},{6,4},{7,5},{8,14},{9,15},{10,... | collective-permute-start | bytes 786440 | tf_op jit(solution)/shard_map/ppermute | solution.py:36
  242.9 19.9 %all-to-all-start.3 = ((f32[16,4,512]{2,1,0:T(4,128)}), f32[16,4,512]{2,1,0:T(4,128)S(1)}, u32[]{:S(2)}, u32[]{:S(2)}) async-start(f32[16,4,512]{2,1,0:T(4,128)} %get-tuple-element.53), calls=%async_computation.3 | async-start | bytes 262144 | tf_op jit(solution)/shard_map/all_to_all | solution.py:562
  276.0 10.5 %collective-permute-start.64 = (bf16[256,512]{1,0:T(8,128)(2,1)S(1)}, bf16[256,512]{1,0:T(8,128)(2,1)S(1)}, u32[]{:S(2)}, u32[]{:S(2)}) collective-permute-start(bf16[256,512]{1,0:T(8,128)(2,1)S(1)} %get-tuple-element.76), channel_id=1, source_target_pairs={{0,6},{1,7},{2,0},{3,1},{4,2},{5,3},{6,4},{7,5},{8,14},{9,15},{10,... | collective-permute-start | bytes 786440 | tf_op jit(solution)/shard_map/ppermute | solution.py:36
  282.1 11.0 %collective-permute-start.63 = (bf16[256,512]{1,0:T(8,128)(2,1)S(1)}, bf16[256,512]{1,0:T(8,128)(2,1)S(1)}, u32[]{:S(2)}, u32[]{:S(2)}) collective-permute-start(bf16[256,512]{1,0:T(8,128)(2,1)S(1)} %get-tuple-element.74), channel_id=1, source_target_pairs={{0,2},{1,3},{2,4},{3,5},{4,6},{5,7},{6,0},{7,1},{8,10},{9,11},{10,... | collective-permute-start | bytes 786440 | tf_op jit(solution)/shard_map/ppermute | solution.py:36
  (100 other events, 1206.2 us)
Sparse Core Ops, SparseCore 0:
  9.5 61.6 all-gather.2
  73.3 106.7 all-gather.4

commit v2 on v1

--- a/solution.py
+++ b/solution.py
@@ -14,8 +14,8 @@
 
 CHUNKS = 8
 SCAN_LIMIT = 24 * 2**20
-VALUE_LIMIT = 54 * 2**20
-GATE_LIMIT = 54 * 2**20
+PROJECT_LIMIT = 56 * 2**20
+FETCH_LIMIT = 50 * 2**20
 GIVE_LIMIT = 12 * 2**20
 KEEP_LIMIT = 8 * 2**20
 HALO = 16
@@ -165,10 +165,12 @@
     total[...] = jnp.zeros_like(total)
 
     def step(k, carry):
-        total[...] += jnp.dot(rows[k], weight[k], preferred_element_type=F32)
+        left = jnp.concatenate([rows[2 * k], rows[2 * k + 1]], axis=1)
+        right = jnp.concatenate([weight[2 * k], weight[2 * k + 1]], axis=0)
+        total[...] += jnp.dot(left, right, preferred_element_type=F32)
         return carry
 
-    lax.fori_loop(0, rows.shape[0], step, 0)
+    lax.fori_loop(0, rows.shape[0] // 2, step, 0)
 
 
 def row_scale(squares, width):
@@ -219,36 +221,33 @@
             put(halo[block], pl.ds(2 * half, HALO))
 
 
-def value_body(layer, rank, place, gain, halo, *refs):
-    pieces, sources = refs[:16], refs[16:-7]
-    out, rows, squares, value_in, total, sems, piece_sems = refs[-7:]
+def project_body(layer, rank, place, gain, halo, *refs):
+    pieces, sources = refs[:16], refs[16:-10]
+    mix, gate, rows, squares, value_in, gate_in, total, sems, gate_sems, piece_sems = refs[-10:]
     values = weight_copies(sources, 0, place[0], value_in, sems)
+    gates = weight_copies(sources, 1, place[0], gate_in, gate_sems)
     arriving = piece_copies(rank[0], pieces, rows, piece_sems)
     for copy in arriving + values:
         copy.start()
     scaled_rows(layer, rank[0], gain, arriving, halo, rows, squares)
+    for copy in gates:
+        copy.start()
     for copy in values:
         copy.wait()
+    scale = row_scale(squares, mix.shape[1] * len(ARRIVE))
     contracted(rows, value_in, total)
-    out[...] = (total[...] * row_scale(squares, out.shape[1] * len(ARRIVE))).astype(BF16)
-
-
-def gate_body(layer, which, rank, place, gain, *refs):
-    pieces, sources, full = refs[:16], refs[16:-10], refs[-10]
-    out, out_in, rows, squares, gate_in, total, sems, out_sems, piece_sems = refs[-9:]
-    gates = weight_copies(sources, 1, place[0], gate_in, sems)
-    others = block_copies(full, which, rank[0], LEAVE, out_in, out_sems)
-    arriving = piece_copies(rank[0], pieces, rows, piece_sems)
-    for copy in arriving + gates:
-        copy.start()
-    scaled_rows(layer, rank[0], gain, arriving, None, rows, squares)
+    mix[...] = (total[...] * scale).astype(BF16)
     for copy in gates:
         copy.wait()
-    for copy in others:
+    contracted(rows, gate_in, total)
+    gate[...] = (total[...] * scale)[: gate.shape[0]].astype(BF16)
+
+
+def fetch_body(which, rank, after, weight, out, sems):
+    copies = block_copies(weight, which, rank[0], LEAVE, out, sems)
+    for copy in copies:
         copy.start()
-    contracted(rows, gate_in, total)
-    out[...] = (total[...] * row_scale(squares, out.shape[1] * len(ARRIVE))).astype(BF16)
-    for copy in others:
+    for copy in copies:
         copy.wait()
 
 
@@ -272,54 +271,47 @@
     )
 
 
-def value_rows(rank, place, pieces, halo, norm_gain, layer, sources):
+def projected(rank, place, pieces, halo, norm_gain, layer, sources):
     half, width = pieces[0].shape
     count = norm_gain.shape[1] // width
     deep = 2 * half + HALO
     return pl.pallas_call(
-        lambda *refs: value_body(layer, *refs),
-        out_shape=jax.ShapeDtypeStruct((deep, width), BF16),
+        lambda *refs: project_body(layer, *refs),
+        out_shape=[
+            jax.ShapeDtypeStruct((deep, width), BF16),
+            jax.ShapeDtypeStruct((2 * half, width), BF16),
+        ],
         in_specs=[in_smem()] * 2 + [in_vmem()] * 2 + [in_hbm()] * (16 + len(sources)),
-        out_specs=in_vmem(),
+        out_specs=[in_vmem()] * 2,
         scratch_shapes=[
             pltpu.VMEM((count, deep, width), BF16),
             pltpu.VMEM((deep, 128), F32),
             pltpu.VMEM((count, width, width), BF16),
+            pltpu.VMEM((count, width, width), BF16),
             pltpu.VMEM((deep, width), F32),
+            pltpu.SemaphoreType.DMA((32,)),
             pltpu.SemaphoreType.DMA((32,)),
             pltpu.SemaphoreType.DMA((16,)),
         ],
-        compiler_params=pltpu.CompilerParams(vmem_limit_bytes=VALUE_LIMIT),
-        cost_estimate=product_cost(deep, width, count),
-        name="value_rows",
+        compiler_params=pltpu.CompilerParams(vmem_limit_bytes=PROJECT_LIMIT),
+        cost_estimate=product_cost(deep, width, 2 * count),
+        name="projected",
     )(rank, place, norm_gain, halo, *pieces, *sources)
 
 
-def gate_rows(rank, place, pieces, norm_gain, layer, sources, full, which):
-    half, width = pieces[0].shape
-    count = norm_gain.shape[1] // width
-    length = 2 * half
+def fetched(rank, after, weights, which):
+    width = weights.shape[2]
+    count = weights.shape[1] // width
     return pl.pallas_call(
-        lambda *refs: gate_body(layer, which, *refs),
-        out_shape=[
-            jax.ShapeDtypeStruct((length, width), BF16),
-            jax.ShapeDtypeStruct((count, width, width), BF16),
-        ],
-        in_specs=[in_smem()] * 2 + [in_vmem()] + [in_hbm()] * (17 + len(sources)),
-        out_specs=[in_vmem()] * 2,
-        scratch_shapes=[
-            pltpu.VMEM((count, length, width), BF16),
-            pltpu.VMEM((length, 128), F32),
-            pltpu.VMEM((count, width, width), BF16),
-            pltpu.VMEM((length, width), F32),
-            pltpu.SemaphoreType.DMA((32,)),
-            pltpu.SemaphoreType.DMA((count,)),
-            pltpu.SemaphoreType.DMA((16,)),
-        ],
-        compiler_params=pltpu.CompilerParams(vmem_limit_bytes=GATE_LIMIT),
-        cost_estimate=product_cost(length, width, count),
-        name="gate_rows",
-    )(rank, place, norm_gain, *pieces, *sources, full)
+        lambda *refs: fetch_body(which, *refs),
+        out_shape=jax.ShapeDtypeStruct((count, width, width), BF16),
+        in_specs=[in_smem(), in_vmem(), in_hbm()],
+        out_specs=in_vmem(),
+        scratch_shapes=[pltpu.SemaphoreType.DMA((count,))],
+        compiler_params=pltpu.CompilerParams(vmem_limit_bytes=FETCH_LIMIT),
+        cost_estimate=product_cost(width, width, count),
+        name="fetched",
+    )(rank, after, weights)
 
 
 def scan_body(
@@ -555,12 +547,12 @@
         sources, full, which = weights[layer]
         pieces = gathered_stream(top, end)
         halo = token_halo(top, end)
-        mix_in = value_rows(rank, place, pieces, halo, norm_gain, layer, sources)
+        mix_in, gate_z = projected(rank, place, pieces, halo, norm_gain, layer, sources)
         local, fwd_cum, bwd_cum, coef, edge = scanned(
             rank, mix_in, conv_taps, forget_rate, block_gates, layer, lax.axis_size("sp")
         )
         edges = lax.all_to_all(edge, "sp", 0, 0, tiled=True)
-        gate_z, out_weight = gate_rows(rank, place, pieces, norm_gain, layer, sources, full, which)
+        out_weight = fetched(rank, coef, full, which)
         mixed, far_give, rest_give = given(
             place, edges, local, fwd_cum, bwd_cum, coef, gate_z, out_weight
         )

time: 303 us -> 321 us (1.059)
  starting transfers between devices: 109 us -> 125 us
  waiting for transfers between devices: 92.3 us -> 104 us
  Pallas kernels: 64.1 us -> 55.2 us
    ppermute x44, starting transfers between devices: 47.7 us -> 61.3 us  [shifted(): return lax.ppermute(array, axis, [(i, move(i)) for i in range(count)])]
    pallas_call x4, Pallas kernels: 42.2 us -> 33.3 us  [the longest x2 24.8 us: projected(): pl.pallas_call(lambda *refs: project_body(layer, *refs), out_shape=[jax.S...]
    all_to_all x2, waiting for transfers between devices: 0.01 us -> 6.65 us  [per_device(): edges = lax.all_to_all(edge, 'sp', 0, 0, tiled=True)]
    all_to_all x2, waiting for transfers between devices: 1.83 us -> 7.79 us  [token_halo(): every = lax.all_to_all(copies, 'tp', 0, 0, tiled=True)]
    ppermute x20, starting transfers between devices: 27.5 us -> 32.2 us  [along_plane(): return lax.ppermute(array, 'sp', pairs)]
    ppermute x20, waiting for transfers between devices: 48.5 us -> 45 us  [along_plane(): return lax.ppermute(array, 'sp', pairs)]
    unnamed x116 -> x120, local copies, waits for them, and re-layouts: 12.2 us -> 12.1 us
  transfers between devices with their start and end apart: 74 -> 74, of which waited for: 30 -> 31; matrix products, arithmetic and copies ran while one was open for 2% -> 2% of each run, Pallas kernels for 15% -> 11%
where the time goes in v2:
time: 321 us; the launch traced here: 319 us
  starting transfers between devices  125 us (39%)
  waiting for transfers between devices  104 us (32%)
  Pallas kernels  55.2 us (17%)
  local copies, waits for them, and re-layouts  16.9 us (5%)
  between operations  14.3 us (4%)
  other arithmetic  4.3 us (1%)
    ppermute x44, starting transfers between devices, shifted(): return lax.ppermute(array, axis, [(i, move(i)) for i in range(count)])  61.3 us
    ppermute x20, waiting for transfers between devices, along_plane(): return lax.ppermute(array, 'sp', pairs)  45 us
    ppermute x44, waiting for transfers between devices, shifted(): return lax.ppermute(array, axis, [(i, move(i)) for i in range(count)])  39.8 us
    ppermute x20, starting transfers between devices, along_plane(): return lax.ppermute(array, 'sp', pairs)  32.2 us
    pallas_call x2, Pallas kernels, projected(): pl.pallas_call(lambda *refs: project_body(layer, *refs), out_shape=[jax.S...  24.8 us
    pallas_call x2, Pallas kernels, scanned(): pl.pallas_call(scan_body, grid_spec=pltpu.PrefetchScalarGridSpec(num_scal...  13 us
    unnamed x120, local copies, waits for them, and re-layouts  12.1 us
    all_to_all x2, starting transfers between devices, per_device(): edges = lax.all_to_all(edge, 'sp', 0, 0, tiled=True)  11.2 us
  transfers between devices with their start and end apart: 74, of which 31 were waited for; matrix products, arithmetic and copies ran while one was open for 2% of the time, Pallas kernels for 11%

profile of v2, /device:TPU:1, one launch (start us, length us, event | category | flops | bytes accessed | tf_op | source)
XLA Modules:
  0.0 318.8 jit_solution(7643045821573346708)
XLA Ops:
  14.6 4.5 %all-to-all-start = ((bf16[8,4,512]{2,1,0:T(4,128)(2,1)}), bf16[8,4,512]{2,1,0:T(4,128)(2,1)S(1)}, u32[]{:S(2)}, u32[]{:S(2)}) async-start(bf16[8,4,512]{2,1,0:T(4,128)(2,1)} %broadcast_in_dim.4), calls=%async_computation | async-start | bytes 65536 | tf_op jit(solution)/shard_map/all_to_all | solution.py:53
  20.6 7.2 %all-to-all-done = bf16[8,4,512]{2,1,0:T(4,128)(2,1)S(1)} async-done(((bf16[8,4,512]{2,1,0:T(4,128)(2,1)}), bf16[8,4,512]{2,1,0:T(4,128)(2,1)S(1)}, u32[]{:S(2)}, u32[]{:S(2)}) %all-to-all-start) | async-done | bytes 32800 | tf_op jit(solution)/shard_map/all_to_all | solution.py:53
  29.1 4.0 %collective-permute-start = (bf16[8,2,512]{2,1,0:T(2,128)(2,1)S(1)}, bf16[8,2,512]{2,1,0:T(2,128)(2,1)S(1)}, u32[]{:S(2)}, u32[]{:S(2)}) collective-permute-start(bf16[8,2,512]{2,1,0:T(2,128)(2,1)S(1)} %get-tuple-element.99), channel_id=1, source_target_pairs={{0,8},{8,16},{16,24},{24,32},{32,40},{40,48},{48,56},{56,64},{64,7... | collective-permute-start | bytes 49160 | tf_op jit(solution)/shard_map/ppermute | solution.py:54
  33.1 4.9 %collective-permute-start.17 = (bf16[256,512]{1,0:T(8,128)(2,1)S(1)}, bf16[256,512]{1,0:T(8,128)(2,1)S(1)}, u32[]{:S(2)}, u32[]{:S(2)}) collective-permute-start(bf16[256,512]{1,0:T(8,128)(2,1)S(1)} %pad_maximum_fusion.3), channel_id=1, source_target_pairs={{0,24},{8,0},{16,8},{24,16},{32,56},{40,32},{48,40},{56,48},{64,88... | collective-permute-start | bytes 786440 | tf_op jit(solution)/shard_map/ppermute | solution.py:84
  47.1 4.2 %collective-permute-start.9 = (bf16[256,512]{1,0:T(8,128)(2,1)S(1)}, bf16[256,512]{1,0:T(8,128)(2,1)S(1)}, u32[]{:S(2)}, u32[]{:S(2)}) collective-permute-start(bf16[256,512]{1,0:T(8,128)(2,1)S(1)} %get-tuple-element.91.refs_5_), channel_id=1, source_target_pairs={{0,1},{1,0},{2,3},{3,2},{4,5},{5,4},{6,7},{7,6},{8,9},{9,8},{10,11... | collective-permute-start | bytes 786440 | tf_op jit(solution)/shard_map/ppermute | solution.py:36
  54.3 3.4 %collective-permute-start.29 = (bf16[128,512]{1,0:T(8,128)(2,1)S(1)}, bf16[128,512]{1,0:T(8,128)(2,1)S(1)}, u32[]{:S(2)}, u32[]{:S(2)}) collective-permute-start(bf16[128,512]{1,0:T(8,128)(2,1)S(1)} %slice.250), channel_id=1, source_target_pairs={{0,96},{8,104},{16,112},{24,120},{32,0},{40,8},{48,16},{56,24},{64... | collective-permute-start | bytes 393224 | tf_op jit(solution)/shard_map/ppermute | solution.py:84
  60.5 5.1 %collective-permute-start.10 = (bf16[256,512]{1,0:T(8,128)(2,1)S(1)}, bf16[256,512]{1,0:T(8,128)(2,1)S(1)}, u32[]{:S(2)}, u32[]{:S(2)}) collective-permute-start(bf16[256,512]{1,0:T(8,128)(2,1)S(1)} %collective-permute-done.2.refs_6_), channel_id=1, source_target_pairs={{0,1},{1,0},{2,3},{3,2},{4,5},{5,4},{6,7},{7,6},{8,9},{9,8},{10,11... | collective-permute-start | bytes 786440 | tf_op jit(solution)/shard_map/ppermute | solution.py:36
  78.2 3.7 %collective-permute-done.20.refs_22_ = bf16[512,512]{1,0:T(8,128)(2,1)S(1)} collective-permute-done((bf16[512,512]{1,0:T(8,128)(2,1)S(1)}, bf16[512,512]{1,0:T(8,128)(2,1)S(1)}, u32[]{:S(2)}, u32[]{:S(2)}) %collective-permute-start.20) | collective-permute-done | bytes 524320 | tf_op jit(solution)/shard_map/ppermute | solution.py:84
  84.7 7.4 %collective-permute-done.30.refs_30_ = bf16[512,512]{1,0:T(8,128)(2,1)S(1)} collective-permute-done((bf16[512,512]{1,0:T(8,128)(2,1)S(1)}, bf16[512,512]{1,0:T(8,128)(2,1)S(1)}, u32[]{:S(2)}, u32[]{:S(2)}) %collective-permute-start.30) | collective-permute-done | bytes 524320 | tf_op jit(solution)/shard_map/ppermute | solution.py:84
  93.1 5.4 %collective-permute-done.21.refs_23_ = bf16[512,512]{1,0:T(8,128)(2,1)S(1)} collective-permute-done((bf16[512,512]{1,0:T(8,128)(2,1)S(1)}, bf16[512,512]{1,0:T(8,128)(2,1)S(1)}, u32[]{:S(2)}, u32[]{:S(2)}) %collective-permute-start.21) | collective-permute-done | bytes 524320 | tf_op jit(solution)/shard_map/ppermute | solution.py:84
  98.5 7.7 %collective-permute-done.23.refs_25_ = bf16[512,512]{1,0:T(8,128)(2,1)} collective-permute-done((bf16[512,512]{1,0:T(8,128)(2,1)S(1)}, bf16[512,512]{1,0:T(8,128)(2,1)}, u32[]{:S(2)}, u32[]{:S(2)}) %collective-permute-start.23) | collective-permute-done | bytes 524320 | tf_op jit(solution)/shard_map/ppermute | solution.py:84
  106.2 3.5 %collective-permute-start.25 = (bf16[512,512]{1,0:T(8,128)(2,1)}, bf16[512,512]{1,0:T(8,128)(2,1)}, u32[]{:S(2)}, u32[]{:S(2)}) collective-permute-start(bf16[512,512]{1,0:T(8,128)(2,1)} %collective-permute-done.23.refs_25_), channel_id=1, source_target_pairs={{0,96},{8,104},{16,112},{24,120},{32,0},{40,8},{48,16},{56,24},{64... | collective-permute-start | bytes 1572872 | tf_op jit(solution)/shard_map/ppermute | solution.py:84
  109.7 3.3 %collective-permute-done.33.refs_33_ = bf16[512,512]{1,0:T(8,128)(2,1)S(1)} collective-permute-done((bf16[512,512]{1,0:T(8,128)(2,1)S(1)}, bf16[512,512]{1,0:T(8,128)(2,1)S(1)}, u32[]{:S(2)}, u32[]{:S(2)}) %collective-permute-start.33) | collective-permute-done | bytes 524320 | tf_op jit(solution)/shard_map/ppermute | solution.py:84
  117.3 8.2 %collective-permute-done.34.refs_34_ = bf16[512,512]{1,0:T(8,128)(2,1)} collective-permute-done((bf16[512,512]{1,0:T(8,128)(2,1)S(1)}, bf16[512,512]{1,0:T(8,128)(2,1)}, u32[]{:S(2)}, u32[]{:S(2)}) %collective-permute-start.34) | collective-permute-done | bytes 524320 | tf_op jit(solution)/shard_map/ppermute | solution.py:84
  125.5 5.9 %collective-permute-done.35.refs_35_ = bf16[512,512]{1,0:T(8,128)(2,1)} collective-permute-done((bf16[512,512]{1,0:T(8,128)(2,1)S(1)}, bf16[512,512]{1,0:T(8,128)(2,1)}, u32[]{:S(2)}, u32[]{:S(2)}) %collective-permute-start.35) | collective-permute-done | bytes 524320 | tf_op jit(solution)/shard_map/ppermute | solution.py:84
  131.5 12.7 %projected.2 = (bf16[528,512]{1,0:T(8,128)(2,1)}, bf16[512,512]{1,0:T(8,128)(2,1)}) custom-call(s32[1]{0:T(128)} %bitcast.4.refs_0_.rank, s32[1]{0:T(128)} %bitcast.3.refs_1_.place, f32[2,4096]{1,0:T(2,128)} %refs_2_.3, bf16[8,16,512]{2,1,0:T(8,128)(2,1)} %maximum_maximum_fusion.refs_3_, bf16[256,512]{1,0:T(8,128)(2,1)} %copy-done.22, ...), custom_call_target="tpu_custom_call" | custom-call | flops 4429185024 | bytes 8388608 | tf_op jit(solution)/shard_map/projected/pallas_call | solution.py:278
  145.2 6.5 %scan.2 = (f32[512,512]{1,0:T(8,128)S(1)}, f32[512,512]{1,0:T(8,128)S(1)}, f32[512,512]{1,0:T(8,128)S(1)}, f32[4,8,512]{2,1,0:T(8,128)S(1)}, f32[16,4,512]{2,1,0:T(4,128)}) custom-call(s32[1]{0:T(128)} %bitcast.4.refs_0_.rank, bf16[528,512]{1,0:T(8,128)(2,1)S(1)} %copy-done.9, f32[2,4,4096]{2,1,0:T(4,128)S(1)} %copy-done.7, f32[2,2,4096]{2,1,0:T(2,128)S(1)} %copy-done.8, ...), custom_call_target="tpu_custom_call" | custom-call | flops 10000000000 | bytes 4000000 | tf_op jit(solution)/shard_map/scan/pallas_call | solution.py:404
  151.7 4.8 %all-to-all-start.1 = ((f32[16,4,512]{2,1,0:T(4,128)}), f32[16,4,512]{2,1,0:T(4,128)S(1)}, u32[]{:S(2)}, u32[]{:S(2)}) async-start(f32[16,4,512]{2,1,0:T(4,128)} %get-tuple-element.38), calls=%async_computation.1 | async-start | bytes 262144 | tf_op jit(solution)/shard_map/all_to_all | solution.py:554
  156.6 4.3 %fetched.2.weight = bf16[8,512,512]{2,1,0:T(8,128)(2,1)} custom-call(s32[1]{0:T(128)} %bitcast.4.refs_0_.rank, f32[4,8,512]{2,1,0:T(8,128)S(1)} %get-tuple-element.42.refs_1_.coef, bf16[1,4096,512]{2,1,0:T(8,128)(2,1)} %all-gather.3.cloned.1.call-done.refs_2_), custom_call_target="tpu_custom_call" | custom-call | flops 2147483648 | bytes 4194304 | tf_op jit(solution)/shard_map/fetched/pallas_call | solution.py:305
  160.9 4.0 %all-to-all-done.1.edges = f32[16,4,512]{2,1,0:T(4,128)S(1)} async-done(((f32[16,4,512]{2,1,0:T(4,128)}), f32[16,4,512]{2,1,0:T(4,128)S(1)}, u32[]{:S(2)}, u32[]{:S(2)}) %all-to-all-start.1) | async-done | bytes 131104 | tf_op jit(solution)/shard_map/all_to_all | solution.py:554
  170.8 7.5 %collective-permute-start.36 = (bf16[3,512,512]{2,1,0:T(8,128)(2,1)S(1)}, bf16[3,512,512]{2,1,0:T(8,128)(2,1)S(1)}, u32[]{:S(2)}, u32[]{:S(2)}) collective-permute-start(bf16[3,512,512]{2,1,0:T(8,128)(2,1)S(1)} %get-tuple-element.46), channel_id=1, source_target_pairs={{0,1},{1,0},{2,3},{3,2},{4,5},{5,4},{6,7},{7,6},{8,9},{9,8},{10,11... | collective-permute-start | bytes 4718600 | tf_op jit(solution)/shard_map/ppermute | solution.py:36
  183.7 6.0 %collective-permute-done.42 = bf16[256,512]{1,0:T(8,128)(2,1)S(1)} collective-permute-done((bf16[256,512]{1,0:T(8,128)(2,1)S(1)}, bf16[256,512]{1,0:T(8,128)(2,1)S(1)}, u32[]{:S(2)}, u32[]{:S(2)}) %collective-permute-start.42) | collective-permute-done | bytes 262176 | tf_op jit(solution)/shard_map/ppermute | solution.py:36
  199.2 5.6 %collective-permute-done.41 = bf16[256,512]{1,0:T(8,128)(2,1)S(1)} collective-permute-done((bf16[256,512]{1,0:T(8,128)(2,1)S(1)}, bf16[256,512]{1,0:T(8,128)(2,1)S(1)}, u32[]{:S(2)}, u32[]{:S(2)}) %collective-permute-start.41) | collective-permute-done | bytes 262176 | tf_op jit(solution)/shard_map/ppermute | solution.py:36
  206.0 6.5 %all-to-all-start.2 = ((bf16[8,4,512]{2,1,0:T(4,128)(2,1)}), bf16[8,4,512]{2,1,0:T(4,128)(2,1)S(1)}, u32[]{:S(2)}, u32[]{:S(2)}) async-start(bf16[8,4,512]{2,1,0:T(4,128)(2,1)} %broadcast_in_dim.5), calls=%async_computation.2 | async-start | bytes 65536 | tf_op jit(solution)/shard_map/all_to_all | solution.py:53
  218.6 3.5 %collective-permute-done.45 = bf16[8,2,512]{2,1,0:T(2,128)(2,1)S(1)} collective-permute-done((bf16[8,2,512]{2,1,0:T(2,128)(2,1)S(1)}, bf16[8,2,512]{2,1,0:T(2,128)(2,1)S(1)}, u32[]{:S(2)}, u32[]{:S(2)}) %collective-permute-start.45) | collective-permute-done | bytes 16416 | tf_op jit(solution)/shard_map/ppermute | solution.py:55
  232.3 3.7 %collective-permute-done.50.refs_10_ = bf16[256,512]{1,0:T(8,128)(2,1)S(1)} collective-permute-done((bf16[256,512]{1,0:T(8,128)(2,1)S(1)}, bf16[256,512]{1,0:T(8,128)(2,1)S(1)}, u32[]{:S(2)}, u32[]{:S(2)}) %collective-permute-start.50) | collective-permute-done | bytes 262176 | tf_op jit(solution)/shard_map/ppermute | solution.py:36
  240.5 12.2 %projected.3 = (bf16[528,512]{1,0:T(8,128)(2,1)}, bf16[512,512]{1,0:T(8,128)(2,1)}) custom-call(s32[1]{0:T(128)} %bitcast.4.refs_0_.rank, s32[1]{0:T(128)} %bitcast.3.refs_1_.place, f32[2,4096]{1,0:T(2,128)} %refs_2_.3, bf16[8,16,512]{2,1,0:T(8,128)(2,1)} %maximum_maximum_fusion.1.refs_3_, bf16[256,512]{1,0:T(8,128)(2,1)} %copy-done.14, ...), custom_call_target="tpu_custom_call" | custom-call | flops 4429185024 | bytes 8388608 | tf_op jit(solution)/shard_map/projected/pallas_call | solution.py:278
  254.9 6.5 %scan.3 = (f32[512,512]{1,0:T(8,128)S(1)}, f32[512,512]{1,0:T(8,128)S(1)}, f32[512,512]{1,0:T(8,128)S(1)}, f32[4,8,512]{2,1,0:T(8,128)S(1)}, f32[16,4,512]{2,1,0:T(4,128)}) custom-call(s32[1]{0:T(128)} %bitcast.4.refs_0_.rank, bf16[528,512]{1,0:T(8,128)(2,1)S(1)} %copy-done.6, f32[2,4,4096]{2,1,0:T(4,128)S(1)} %copy-done.7, f32[2,2,4096]{2,1,0:T(2,128)S(1)} %copy-done.8, ...), custom_call_target="tpu_custom_call" | custom-call | flops 10000000000 | bytes 4000000 | tf_op jit(solution)/shard_map/scan/pallas_call | solution.py:404
  261.4 6.4 %all-to-all-start.3 = ((f32[16,4,512]{2,1,0:T(4,128)}), f32[16,4,512]{2,1,0:T(4,128)S(1)}, u32[]{:S(2)}, u32[]{:S(2)}) async-start(f32[16,4,512]{2,1,0:T(4,128)} %get-tuple-element.54), calls=%async_computation.3 | async-start | bytes 262144 | tf_op jit(solution)/shard_map/all_to_all | solution.py:554
  267.8 4.2 %fetched.3.weight = bf16[8,512,512]{2,1,0:T(8,128)(2,1)} custom-call(s32[1]{0:T(128)} %bitcast.4.refs_0_.rank, f32[4,8,512]{2,1,0:T(8,128)S(1)} %get-tuple-element.58.refs_1_.coef, bf16[3,4096,512]{2,1,0:T(8,128)(2,1)} %all-gather.5.cloned.1.call-done.refs_20_.refs_2_), custom_call_target="tpu_custom_call" | custom-call | flops 2147483648 | bytes 4194304 | tf_op jit(solution)/shard_map/fetched/pallas_call | solution.py:305
  288.7 5.3 %collective-permute-done.66 = bf16[256,512]{1,0:T(8,128)(2,1)S(1)} collective-permute-done((bf16[256,512]{1,0:T(8,128)(2,1)S(1)}, bf16[256,512]{1,0:T(8,128)(2,1)S(1)}, u32[]{:S(2)}, u32[]{:S(2)}) %collective-permute-start.66) | collective-permute-done | bytes 262176 | tf_op jit(solution)/shard_map/ppermute | solution.py:36
  305.0 5.6 %collective-permute-done.65 = bf16[256,512]{1,0:T(8,128)(2,1)S(1)} collective-permute-done((bf16[256,512]{1,0:T(8,128)(2,1)S(1)}, bf16[256,512]{1,0:T(8,128)(2,1)S(1)}, u32[]{:S(2)}, u32[]{:S(2)}) %collective-permute-start.65) | collective-permute-done | bytes 262176 | tf_op jit(solution)/shard_map/ppermute | solution.py:36
  (293 shorter events, 121.0 us)
Async XLA Ops:
  6.5 150.0 %all-gather.3.cloned.1.call-start = ((), (), s32[]{:S(2)}) async-start(), calls=%async_computation.4 | async-start | bytes 4456448 | tf_op jit(solution)/shard_map/all_gather | solution.py:542
  8.4 232.0 %all-gather.5.cloned.1.call-start = ((), (), s32[]{:S(2)}) async-start(), calls=%async_computation.5 | async-start | bytes 13369344 | tf_op jit(solution)/shard_map/all_gather | solution.py:544
  10.7 29.6 %collective-permute-start.2 = (bf16[256,512]{1,0:T(8,128)(2,1)S(1)}, bf16[256,512]{1,0:T(8,128)(2,1)S(1)}, u32[]{:S(2)}, u32[]{:S(2)}) collective-permute-start(bf16[256,512]{1,0:T(8,128)(2,1)S(1)} %get-tuple-element.92.refs_4_), channel_id=1, source_target_pairs={{0,2},{1,3},{2,4},{3,5},{4,6},{5,7},{6,0},{7,1},{8,10},{9,11},{10,... | collective-permute-start | bytes 786440 | tf_op jit(solution)/shard_map/ppermute | solution.py:36
  12.8 29.9 %collective-permute-start.3 = (bf16[256,512]{1,0:T(8,128)(2,1)S(1)}, bf16[256,512]{1,0:T(8,128)(2,1)S(1)}, u32[]{:S(2)}, u32[]{:S(2)}) collective-permute-start(bf16[256,512]{1,0:T(8,128)(2,1)S(1)} %get-tuple-element.91.refs_5_), channel_id=1, source_target_pairs={{0,2},{1,3},{2,4},{3,5},{4,6},{5,7},{6,0},{7,1},{8,10},{9,11},{10,... | collective-permute-start | bytes 786440 | tf_op jit(solution)/shard_map/ppermute | solution.py:36
  14.6 13.1 %all-to-all-start = ((bf16[8,4,512]{2,1,0:T(4,128)(2,1)}), bf16[8,4,512]{2,1,0:T(4,128)(2,1)S(1)}, u32[]{:S(2)}, u32[]{:S(2)}) async-start(bf16[8,4,512]{2,1,0:T(4,128)(2,1)} %broadcast_in_dim.4), calls=%async_computation | async-start | bytes 65536 | tf_op jit(solution)/shard_map/all_to_all | solution.py:53
  19.2 24.1 %collective-permute-start.16 = (bf16[256,512]{1,0:T(8,128)(2,1)S(1)}, bf16[256,512]{1,0:T(8,128)(2,1)S(1)}, u32[]{:S(2)}, u32[]{:S(2)}) collective-permute-start(bf16[256,512]{1,0:T(8,128)(2,1)S(1)} %pad_maximum_fusion.3), channel_id=1, source_target_pairs={{0,8},{8,16},{16,24},{24,0},{32,40},{40,48},{48,56},{56,32},{64,72... | collective-permute-start | bytes 786440 | tf_op jit(solution)/shard_map/ppermute | solution.py:84
  40.2 11.1 %collective-permute-start.27 = (bf16[256,512]{1,0:T(8,128)(2,1)S(1)}, bf16[256,512]{1,0:T(8,128)(2,1)S(1)}, u32[]{:S(2)}, u32[]{:S(2)}) collective-permute-start(bf16[256,512]{1,0:T(8,128)(2,1)S(1)} %pad_maximum_fusion.4), channel_id=1, source_target_pairs={{0,96},{8,104},{16,112},{24,120},{32,0},{40,8},{48,16},{56,24},{64... | collective-permute-start | bytes 786440 | tf_op jit(solution)/shard_map/ppermute | solution.py:84
  43.3 10.9 %collective-permute-start.5 = (bf16[256,512]{1,0:T(8,128)(2,1)S(1)}, bf16[256,512]{1,0:T(8,128)(2,1)S(1)}, u32[]{:S(2)}, u32[]{:S(2)}) collective-permute-start(bf16[256,512]{1,0:T(8,128)(2,1)S(1)} %get-tuple-element.91.refs_5_), channel_id=1, source_target_pairs={{0,6},{1,7},{2,0},{3,1},{4,2},{5,3},{6,4},{7,5},{8,14},{9,15},{10,... | collective-permute-start | bytes 786440 | tf_op jit(solution)/shard_map/ppermute | solution.py:36
  54.2 11.4 %collective-permute-start.28 = (bf16[128,512]{1,0:T(8,128)(2,1)S(1)}, bf16[128,512]{1,0:T(8,128)(2,1)S(1)}, u32[]{:S(2)}, u32[]{:S(2)}) collective-permute-start(bf16[128,512]{1,0:T(8,128)(2,1)S(1)} %slice.249), channel_id=1, source_target_pairs={{0,32},{8,40},{16,48},{24,56},{32,64},{40,72},{48,80},{56,88},{64,... | collective-permute-start | bytes 393224 | tf_op jit(solution)/shard_map/ppermute | solution.py:84
  54.3 13.7 %collective-permute-start.29 = (bf16[128,512]{1,0:T(8,128)(2,1)S(1)}, bf16[128,512]{1,0:T(8,128)(2,1)S(1)}, u32[]{:S(2)}, u32[]{:S(2)}) collective-permute-start(bf16[128,512]{1,0:T(8,128)(2,1)S(1)} %slice.250), channel_id=1, source_target_pairs={{0,96},{8,104},{16,112},{24,120},{32,0},{40,8},{48,16},{56,24},{64... | collective-permute-start | bytes 393224 | tf_op jit(solution)/shard_map/ppermute | solution.py:84
  60.5 10.8 %collective-permute-start.10 = (bf16[256,512]{1,0:T(8,128)(2,1)S(1)}, bf16[256,512]{1,0:T(8,128)(2,1)S(1)}, u32[]{:S(2)}, u32[]{:S(2)}) collective-permute-start(bf16[256,512]{1,0:T(8,128)(2,1)S(1)} %collective-permute-done.2.refs_6_), channel_id=1, source_target_pairs={{0,1},{1,0},{2,3},{3,2},{4,5},{5,4},{6,7},{7,6},{8,9},{9,8},{10,11... | collective-permute-start | bytes 786440 | tf_op jit(solution)/shard_map/ppermute | solution.py:36
  68.1 13.7 %collective-permute-start.20 = (bf16[512,512]{1,0:T(8,128)(2,1)S(1)}, bf16[512,512]{1,0:T(8,128)(2,1)S(1)}, u32[]{:S(2)}, u32[]{:S(2)}) collective-permute-start(bf16[512,512]{1,0:T(8,128)(2,1)S(1)} %pad_maximum_fusion.1.refs_20_), channel_id=1, source_target_pairs={{0,32},{8,40},{16,48},{24,56},{32,64},{40,72},{48,80},{56,88},{64,... | collective-permute-start | bytes 1572872 | tf_op jit(solution)/shard_map/ppermute | solution.py:84
  69.2 15.1 %collective-permute-start.22 = (bf16[512,512]{1,0:T(8,128)(2,1)S(1)}, bf16[512,512]{1,0:T(8,128)(2,1)S(1)}, u32[]{:S(2)}, u32[]{:S(2)}) collective-permute-start(bf16[512,512]{1,0:T(8,128)(2,1)S(1)} %pad_maximum_fusion.1.refs_20_), channel_id=1, source_target_pairs={{0,96},{8,104},{16,112},{24,120},{32,0},{40,8},{48,16},{56,24},{64... | collective-permute-start | bytes 1572872 | tf_op jit(solution)/shard_map/ppermute | solution.py:84
  75.5 16.6 %collective-permute-start.30 = (bf16[512,512]{1,0:T(8,128)(2,1)S(1)}, bf16[512,512]{1,0:T(8,128)(2,1)S(1)}, u32[]{:S(2)}, u32[]{:S(2)}) collective-permute-start(bf16[512,512]{1,0:T(8,128)(2,1)S(1)} %pad_maximum_fusion.2.refs_28_), channel_id=1, source_target_pairs={{0,8},{8,16},{16,24},{24,0},{32,40},{40,48},{48,56},{56,32},{64,72... | collective-permute-start | bytes 1572872 | tf_op jit(solution)/shard_map/ppermute | solution.py:84
  75.9 17.2 %collective-permute-start.32 = (bf16[512,512]{1,0:T(8,128)(2,1)S(1)}, bf16[512,512]{1,0:T(8,128)(2,1)S(1)}, u32[]{:S(2)}, u32[]{:S(2)}) collective-permute-start(bf16[512,512]{1,0:T(8,128)(2,1)S(1)} %pad_maximum_fusion.2.refs_28_), channel_id=1, source_target_pairs={{0,24},{8,0},{16,8},{24,16},{32,56},{40,32},{48,40},{56,48},{64,88... | collective-permute-start | bytes 1572872 | tf_op jit(solution)/shard_map/ppermute | solution.py:84
  78.2 20.3 %collective-permute-start.21 = (bf16[512,512]{1,0:T(8,128)(2,1)S(1)}, bf16[512,512]{1,0:T(8,128)(2,1)S(1)}, u32[]{:S(2)}, u32[]{:S(2)}) collective-permute-start(bf16[512,512]{1,0:T(8,128)(2,1)S(1)} %constant_dynamic-update-slice_fusion.refs_21_), channel_id=1, source_target_pairs={{0,32},{8,40},{16,48},{24,56},{32,64},{40,72},{48,80},{56,88},{64,... | collective-permute-start | bytes 1572872 | tf_op jit(solution)/shard_map/ppermute | solution.py:84
  81.8 24.3 %collective-permute-start.23 = (bf16[512,512]{1,0:T(8,128)(2,1)S(1)}, bf16[512,512]{1,0:T(8,128)(2,1)}, u32[]{:S(2)}, u32[]{:S(2)}) collective-permute-start(bf16[512,512]{1,0:T(8,128)(2,1)S(1)} %constant_dynamic-update-slice_fusion.refs_21_), channel_id=1, source_target_pairs={{0,96},{8,104},{16,112},{24,120},{32,0},{40,8},{48,16},{56,24},{64... | collective-permute-start | bytes 1572872 | tf_op jit(solution)/shard_map/ppermute | solution.py:84
  84.3 28.6 %collective-permute-start.33 = (bf16[512,512]{1,0:T(8,128)(2,1)S(1)}, bf16[512,512]{1,0:T(8,128)(2,1)S(1)}, u32[]{:S(2)}, u32[]{:S(2)}) collective-permute-start(bf16[512,512]{1,0:T(8,128)(2,1)S(1)} %constant_dynamic-update-slice_fusion.3.refs_29_), channel_id=1, source_target_pairs={{0,24},{8,0},{16,8},{24,16},{32,56},{40,32},{48,40},{56,48},{64,88... | collective-permute-start | bytes 1572872 | tf_op jit(solution)/shard_map/ppermute | solution.py:84
  92.1 25.0 %collective-permute-start.31 = (bf16[512,512]{1,0:T(8,128)(2,1)S(1)}, bf16[512,512]{1,0:T(8,128)(2,1)}, u32[]{:S(2)}, u32[]{:S(2)}) collective-permute-start(bf16[512,512]{1,0:T(8,128)(2,1)S(1)} %constant_dynamic-update-slice_fusion.3.refs_29_), channel_id=1, source_target_pairs={{0,8},{8,16},{16,24},{24,0},{32,40},{40,48},{48,56},{56,32},{64,72... | collective-permute-start | bytes 1572872 | tf_op jit(solution)/shard_map/ppermute | solution.py:84
  93.1 24.2 %collective-permute-start.24 = (bf16[512,512]{1,0:T(8,128)(2,1)S(1)}, bf16[512,512]{1,0:T(8,128)(2,1)}, u32[]{:S(2)}, u32[]{:S(2)}) collective-permute-start(bf16[512,512]{1,0:T(8,128)(2,1)S(1)} %collective-permute-done.20.refs_22_), channel_id=1, source_target_pairs={{0,32},{8,40},{16,48},{24,56},{32,64},{40,72},{48,80},{56,88},{64,... | collective-permute-start | bytes 1572872 | tf_op jit(solution)/shard_map/ppermute | solution.py:84
  98.5 27.0 %collective-permute-start.34 = (bf16[512,512]{1,0:T(8,128)(2,1)S(1)}, bf16[512,512]{1,0:T(8,128)(2,1)}, u32[]{:S(2)}, u32[]{:S(2)}) collective-permute-start(bf16[512,512]{1,0:T(8,128)(2,1)S(1)} %collective-permute-done.30.refs_30_), channel_id=1, source_target_pairs={{0,8},{8,16},{16,24},{24,0},{32,40},{40,48},{48,56},{56,32},{64,72... | collective-permute-start | bytes 1572872 | tf_op jit(solution)/shard_map/ppermute | solution.py:84
  106.2 19.3 %collective-permute-start.25 = (bf16[512,512]{1,0:T(8,128)(2,1)}, bf16[512,512]{1,0:T(8,128)(2,1)}, u32[]{:S(2)}, u32[]{:S(2)}) collective-permute-start(bf16[512,512]{1,0:T(8,128)(2,1)} %collective-permute-done.23.refs_25_), channel_id=1, source_target_pairs={{0,96},{8,104},{16,112},{24,120},{32,0},{40,8},{48,16},{56,24},{64... | collective-permute-start | bytes 1572872 | tf_op jit(solution)/shard_map/ppermute | solution.py:84
  113.0 18.4 %collective-permute-start.35 = (bf16[512,512]{1,0:T(8,128)(2,1)S(1)}, bf16[512,512]{1,0:T(8,128)(2,1)}, u32[]{:S(2)}, u32[]{:S(2)}) collective-permute-start(bf16[512,512]{1,0:T(8,128)(2,1)S(1)} %collective-permute-done.33.refs_33_), channel_id=1, source_target_pairs={{0,24},{8,0},{16,8},{24,16},{32,56},{40,32},{48,40},{56,48},{64,88... | collective-permute-start | bytes 1572872 | tf_op jit(solution)/shard_map/ppermute | solution.py:84
  151.7 13.2 %all-to-all-start.1 = ((f32[16,4,512]{2,1,0:T(4,128)}), f32[16,4,512]{2,1,0:T(4,128)S(1)}, u32[]{:S(2)}, u32[]{:S(2)}) async-start(f32[16,4,512]{2,1,0:T(4,128)} %get-tuple-element.38), calls=%async_computation.1 | async-start | bytes 262144 | tf_op jit(solution)/shard_map/all_to_all | solution.py:554
  170.8 20.3 %collective-permute-start.36 = (bf16[3,512,512]{2,1,0:T(8,128)(2,1)S(1)}, bf16[3,512,512]{2,1,0:T(8,128)(2,1)S(1)}, u32[]{:S(2)}, u32[]{:S(2)}) collective-permute-start(bf16[3,512,512]{2,1,0:T(8,128)(2,1)S(1)} %get-tuple-element.46), channel_id=1, source_target_pairs={{0,1},{1,0},{2,3},{3,2},{4,5},{5,4},{6,7},{7,6},{8,9},{9,8},{10,11... | collective-permute-start | bytes 4718600 | tf_op jit(solution)/shard_map/ppermute | solution.py:36
  206.0 11.3 %all-to-all-start.2 = ((bf16[8,4,512]{2,1,0:T(4,128)(2,1)}), bf16[8,4,512]{2,1,0:T(4,128)(2,1)S(1)}, u32[]{:S(2)}, u32[]{:S(2)}) async-start(bf16[8,4,512]{2,1,0:T(4,128)(2,1)} %broadcast_in_dim.5), calls=%async_computation.2 | async-start | bytes 65536 | tf_op jit(solution)/shard_map/all_to_all | solution.py:53
  212.5 15.1 %collective-permute-start.46 = (bf16[256,512]{1,0:T(8,128)(2,1)S(1)}, bf16[256,512]{1,0:T(8,128)(2,1)S(1)}, u32[]{:S(2)}, u32[]{:S(2)}) collective-permute-start(bf16[256,512]{1,0:T(8,128)(2,1)S(1)} %get-tuple-element.70.refs_4_), channel_id=1, source_target_pairs={{0,2},{1,3},{2,4},{3,5},{4,6},{5,7},{6,0},{7,1},{8,10},{9,11},{10,... | collective-permute-start | bytes 786440 | tf_op jit(solution)/shard_map/ppermute | solution.py:36
  213.8 13.8 %collective-permute-start.47 = (bf16[256,512]{1,0:T(8,128)(2,1)S(1)}, bf16[256,512]{1,0:T(8,128)(2,1)S(1)}, u32[]{:S(2)}, u32[]{:S(2)}) collective-permute-start(bf16[256,512]{1,0:T(8,128)(2,1)S(1)} %get-tuple-element.69.refs_5_), channel_id=1, source_target_pairs={{0,2},{1,3},{2,4},{3,5},{4,6},{5,7},{6,0},{7,1},{8,10},{9,11},{10,... | collective-permute-start | bytes 786440 | tf_op jit(solution)/shard_map/ppermute | solution.py:36
  215.0 14.1 %collective-permute-start.49 = (bf16[256,512]{1,0:T(8,128)(2,1)S(1)}, bf16[256,512]{1,0:T(8,128)(2,1)S(1)}, u32[]{:S(2)}, u32[]{:S(2)}) collective-permute-start(bf16[256,512]{1,0:T(8,128)(2,1)S(1)} %get-tuple-element.69.refs_5_), channel_id=1, source_target_pairs={{0,6},{1,7},{2,0},{3,1},{4,2},{5,3},{6,4},{7,5},{8,14},{9,15},{10,... | collective-permute-start | bytes 786440 | tf_op jit(solution)/shard_map/ppermute | solution.py:36
  216.5 13.8 %collective-permute-start.48 = (bf16[256,512]{1,0:T(8,128)(2,1)S(1)}, bf16[256,512]{1,0:T(8,128)(2,1)S(1)}, u32[]{:S(2)}, u32[]{:S(2)}) collective-permute-start(bf16[256,512]{1,0:T(8,128)(2,1)S(1)} %get-tuple-element.70.refs_4_), channel_id=1, source_target_pairs={{0,6},{1,7},{2,0},{3,1},{4,2},{5,3},{6,4},{7,5},{8,14},{9,15},{10,... | collective-permute-start | bytes 786440 | tf_op jit(solution)/shard_map/ppermute | solution.py:36
  261.4 13.2 %all-to-all-start.3 = ((f32[16,4,512]{2,1,0:T(4,128)}), f32[16,4,512]{2,1,0:T(4,128)S(1)}, u32[]{:S(2)}, u32[]{:S(2)}) async-start(f32[16,4,512]{2,1,0:T(4,128)} %get-tuple-element.54), calls=%async_computation.3 | async-start | bytes 262144 | tf_op jit(solution)/shard_map/all_to_all | solution.py:554
  280.5 16.7 %collective-permute-start.60 = (bf16[3,512,512]{2,1,0:T(8,128)(2,1)S(1)}, bf16[3,512,512]{2,1,0:T(8,128)(2,1)S(1)}, u32[]{:S(2)}, u32[]{:S(2)}) collective-permute-start(bf16[3,512,512]{2,1,0:T(8,128)(2,1)S(1)} %get-tuple-element.62), channel_id=1, source_target_pairs={{0,1},{1,0},{2,3},{3,2},{4,5},{5,4},{6,7},{7,6},{8,9},{9,8},{10,11... | collective-permute-start | bytes 4718600 | tf_op jit(solution)/shard_map/ppermute | solution.py:36
  (102 other events, 1483.7 us)
Sparse Core Ops, SparseCore 0:
  9.5 59.8 all-gather.2
  71.5 108.3 all-gather.4

commit v3 on v2

--- a/solution.py
+++ b/solution.py
@@ -84,24 +84,16 @@
     return lax.ppermute(array, "sp", pairs)
 
 
-def around(array, axis):
-    half = array.shape[0] // 2
-    before = along_plane(array, axis, 1)
-    after = along_plane(array, axis, -1)
-    return (
-        before,
-        after,
-        along_plane(before[:half], axis, 1),
-        along_plane(after[half:], axis, -1),
-    )
-
-
 def gathered_pieces(weights):
     half = weights[0].shape[0] // 2
     pieces = []
-    for at, (first, second) in ((0, "yz"), (half, "zy")):
-        own = jnp.concatenate([w[at : at + half] for w in weights], axis=0)
-        before, after, far_top, far_end = around(own, first)
+    for turn, (first, second) in enumerate(("yz", "zy")):
+        own = jnp.concatenate([w[turn * half : (turn + 1) * half] for w in weights], axis=0)
+        part = own.shape[0] // 2
+        before = along_plane(own, first, 1)
+        after = along_plane(own, first, -1)
+        far_top = along_plane(before[:part], first, 1)
+        far_end = along_plane(after[part:], first, -1)
         top = jnp.concatenate([own, before], axis=0)
         end = jnp.concatenate([after, far_top, far_end], axis=0)
         top_before = along_plane(top, second, 1)

time: 321 us -> 321 us (level)
  no operation moved by 1% of the time
where the time goes in v3:
time: 321 us; the launch traced here: 319 us
  starting transfers between devices  125 us (39%)
  waiting for transfers between devices  104 us (32%)
  Pallas kernels  55.2 us (17%)
  local copies, waits for them, and re-layouts  16.9 us (5%)
  between operations  14.3 us (4%)
  other arithmetic  4.3 us (1%)
    ppermute x44, starting transfers between devices, shifted(): return lax.ppermute(array, axis, [(i, move(i)) for i in range(count)])  61.3 us
    ppermute x20, waiting for transfers between devices, along_plane(): return lax.ppermute(array, 'sp', pairs)  45 us
    ppermute x44, waiting for transfers between devices, shifted(): return lax.ppermute(array, axis, [(i, move(i)) for i in range(count)])  39.8 us
    ppermute x20, starting transfers between devices, along_plane(): return lax.ppermute(array, 'sp', pairs)  32.2 us
    pallas_call x2, Pallas kernels, projected(): pl.pallas_call(lambda *refs: project_body(layer, *refs), out_shape=[jax.S...  24.8 us
    pallas_call x2, Pallas kernels, scanned(): pl.pallas_call(scan_body, grid_spec=pltpu.PrefetchScalarGridSpec(num_scal...  13 us
    unnamed x120, local copies, waits for them, and re-layouts  12.1 us
    all_to_all x2, starting transfers between devices, per_device(): edges = lax.all_to_all(edge, 'sp', 0, 0, tiled=True)  11.2 us
  transfers between devices with their start and end apart: 74, of which 31 were waited for; matrix products, arithmetic and copies ran while one was open for 2% of the time, Pallas kernels for 11%

profile of v3, /device:TPU:1, one launch (start us, length us, event | category | flops | bytes accessed | tf_op | source)
XLA Modules:
  0.0 318.8 jit_solution(7643045821573346708)
XLA Ops:
  14.6 4.5 %all-to-all-start = ((bf16[8,4,512]{2,1,0:T(4,128)(2,1)}), bf16[8,4,512]{2,1,0:T(4,128)(2,1)S(1)}, u32[]{:S(2)}, u32[]{:S(2)}) async-start(bf16[8,4,512]{2,1,0:T(4,128)(2,1)} %broadcast_in_dim.4), calls=%async_computation | async-start | bytes 65536 | tf_op jit(solution)/shard_map/all_to_all | solution.py:53
  20.6 7.2 %all-to-all-done = bf16[8,4,512]{2,1,0:T(4,128)(2,1)S(1)} async-done(((bf16[8,4,512]{2,1,0:T(4,128)(2,1)}), bf16[8,4,512]{2,1,0:T(4,128)(2,1)S(1)}, u32[]{:S(2)}, u32[]{:S(2)}) %all-to-all-start) | async-done | bytes 32800 | tf_op jit(solution)/shard_map/all_to_all | solution.py:53
  29.1 4.0 %collective-permute-start = (bf16[8,2,512]{2,1,0:T(2,128)(2,1)S(1)}, bf16[8,2,512]{2,1,0:T(2,128)(2,1)S(1)}, u32[]{:S(2)}, u32[]{:S(2)}) collective-permute-start(bf16[8,2,512]{2,1,0:T(2,128)(2,1)S(1)} %get-tuple-element.99), channel_id=1, source_target_pairs={{0,8},{8,16},{16,24},{24,32},{32,40},{40,48},{48,56},{56,64},{64,7... | collective-permute-start | bytes 49160 | tf_op jit(solution)/shard_map/ppermute | solution.py:54
  33.1 4.9 %collective-permute-start.17 = (bf16[256,512]{1,0:T(8,128)(2,1)S(1)}, bf16[256,512]{1,0:T(8,128)(2,1)S(1)}, u32[]{:S(2)}, u32[]{:S(2)}) collective-permute-start(bf16[256,512]{1,0:T(8,128)(2,1)S(1)} %pad_maximum_fusion.3), channel_id=1, source_target_pairs={{0,24},{8,0},{16,8},{24,16},{32,56},{40,32},{48,40},{56,48},{64,88... | collective-permute-start | bytes 786440 | tf_op jit(solution)/shard_map/ppermute | solution.py:84
  47.1 4.2 %collective-permute-start.9 = (bf16[256,512]{1,0:T(8,128)(2,1)S(1)}, bf16[256,512]{1,0:T(8,128)(2,1)S(1)}, u32[]{:S(2)}, u32[]{:S(2)}) collective-permute-start(bf16[256,512]{1,0:T(8,128)(2,1)S(1)} %get-tuple-element.91.refs_5_), channel_id=1, source_target_pairs={{0,1},{1,0},{2,3},{3,2},{4,5},{5,4},{6,7},{7,6},{8,9},{9,8},{10,11... | collective-permute-start | bytes 786440 | tf_op jit(solution)/shard_map/ppermute | solution.py:36
  54.3 3.4 %collective-permute-start.29 = (bf16[128,512]{1,0:T(8,128)(2,1)S(1)}, bf16[128,512]{1,0:T(8,128)(2,1)S(1)}, u32[]{:S(2)}, u32[]{:S(2)}) collective-permute-start(bf16[128,512]{1,0:T(8,128)(2,1)S(1)} %slice.250), channel_id=1, source_target_pairs={{0,96},{8,104},{16,112},{24,120},{32,0},{40,8},{48,16},{56,24},{64... | collective-permute-start | bytes 393224 | tf_op jit(solution)/shard_map/ppermute | solution.py:84
  60.5 5.1 %collective-permute-start.10 = (bf16[256,512]{1,0:T(8,128)(2,1)S(1)}, bf16[256,512]{1,0:T(8,128)(2,1)S(1)}, u32[]{:S(2)}, u32[]{:S(2)}) collective-permute-start(bf16[256,512]{1,0:T(8,128)(2,1)S(1)} %collective-permute-done.2.refs_6_), channel_id=1, source_target_pairs={{0,1},{1,0},{2,3},{3,2},{4,5},{5,4},{6,7},{7,6},{8,9},{9,8},{10,11... | collective-permute-start | bytes 786440 | tf_op jit(solution)/shard_map/ppermute | solution.py:36
  78.2 3.7 %collective-permute-done.20.refs_22_ = bf16[512,512]{1,0:T(8,128)(2,1)S(1)} collective-permute-done((bf16[512,512]{1,0:T(8,128)(2,1)S(1)}, bf16[512,512]{1,0:T(8,128)(2,1)S(1)}, u32[]{:S(2)}, u32[]{:S(2)}) %collective-permute-start.20) | collective-permute-done | bytes 524320 | tf_op jit(solution)/shard_map/ppermute | solution.py:84
  84.7 7.4 %collective-permute-done.30.refs_30_ = bf16[512,512]{1,0:T(8,128)(2,1)S(1)} collective-permute-done((bf16[512,512]{1,0:T(8,128)(2,1)S(1)}, bf16[512,512]{1,0:T(8,128)(2,1)S(1)}, u32[]{:S(2)}, u32[]{:S(2)}) %collective-permute-start.30) | collective-permute-done | bytes 524320 | tf_op jit(solution)/shard_map/ppermute | solution.py:84
  93.1 5.4 %collective-permute-done.21.refs_23_ = bf16[512,512]{1,0:T(8,128)(2,1)S(1)} collective-permute-done((bf16[512,512]{1,0:T(8,128)(2,1)S(1)}, bf16[512,512]{1,0:T(8,128)(2,1)S(1)}, u32[]{:S(2)}, u32[]{:S(2)}) %collective-permute-start.21) | collective-permute-done | bytes 524320 | tf_op jit(solution)/shard_map/ppermute | solution.py:84
  98.5 7.7 %collective-permute-done.23.refs_25_ = bf16[512,512]{1,0:T(8,128)(2,1)} collective-permute-done((bf16[512,512]{1,0:T(8,128)(2,1)S(1)}, bf16[512,512]{1,0:T(8,128)(2,1)}, u32[]{:S(2)}, u32[]{:S(2)}) %collective-permute-start.23) | collective-permute-done | bytes 524320 | tf_op jit(solution)/shard_map/ppermute | solution.py:84
  106.2 3.5 %collective-permute-start.25 = (bf16[512,512]{1,0:T(8,128)(2,1)}, bf16[512,512]{1,0:T(8,128)(2,1)}, u32[]{:S(2)}, u32[]{:S(2)}) collective-permute-start(bf16[512,512]{1,0:T(8,128)(2,1)} %collective-permute-done.23.refs_25_), channel_id=1, source_target_pairs={{0,96},{8,104},{16,112},{24,120},{32,0},{40,8},{48,16},{56,24},{64... | collective-permute-start | bytes 1572872 | tf_op jit(solution)/shard_map/ppermute | solution.py:84
  109.7 3.3 %collective-permute-done.33.refs_33_ = bf16[512,512]{1,0:T(8,128)(2,1)S(1)} collective-permute-done((bf16[512,512]{1,0:T(8,128)(2,1)S(1)}, bf16[512,512]{1,0:T(8,128)(2,1)S(1)}, u32[]{:S(2)}, u32[]{:S(2)}) %collective-permute-start.33) | collective-permute-done | bytes 524320 | tf_op jit(solution)/shard_map/ppermute | solution.py:84
  117.3 8.2 %collective-permute-done.34.refs_34_ = bf16[512,512]{1,0:T(8,128)(2,1)} collective-permute-done((bf16[512,512]{1,0:T(8,128)(2,1)S(1)}, bf16[512,512]{1,0:T(8,128)(2,1)}, u32[]{:S(2)}, u32[]{:S(2)}) %collective-permute-start.34) | collective-permute-done | bytes 524320 | tf_op jit(solution)/shard_map/ppermute | solution.py:84
  125.5 5.9 %collective-permute-done.35.refs_35_ = bf16[512,512]{1,0:T(8,128)(2,1)} collective-permute-done((bf16[512,512]{1,0:T(8,128)(2,1)S(1)}, bf16[512,512]{1,0:T(8,128)(2,1)}, u32[]{:S(2)}, u32[]{:S(2)}) %collective-permute-start.35) | collective-permute-done | bytes 524320 | tf_op jit(solution)/shard_map/ppermute | solution.py:84
  131.5 12.7 %projected.2 = (bf16[528,512]{1,0:T(8,128)(2,1)}, bf16[512,512]{1,0:T(8,128)(2,1)}) custom-call(s32[1]{0:T(128)} %bitcast.4.refs_0_.rank, s32[1]{0:T(128)} %bitcast.3.refs_1_.place, f32[2,4096]{1,0:T(2,128)} %refs_2_.3, bf16[8,16,512]{2,1,0:T(8,128)(2,1)} %maximum_maximum_fusion.refs_3_, bf16[256,512]{1,0:T(8,128)(2,1)} %copy-done.22, ...), custom_call_target="tpu_custom_call" | custom-call | flops 4429185024 | bytes 8388608 | tf_op jit(solution)/shard_map/projected/pallas_call | solution.py:270
  145.2 6.5 %scan.2 = (f32[512,512]{1,0:T(8,128)S(1)}, f32[512,512]{1,0:T(8,128)S(1)}, f32[512,512]{1,0:T(8,128)S(1)}, f32[4,8,512]{2,1,0:T(8,128)S(1)}, f32[16,4,512]{2,1,0:T(4,128)}) custom-call(s32[1]{0:T(128)} %bitcast.4.refs_0_.rank, bf16[528,512]{1,0:T(8,128)(2,1)S(1)} %copy-done.9, f32[2,4,4096]{2,1,0:T(4,128)S(1)} %copy-done.7, f32[2,2,4096]{2,1,0:T(2,128)S(1)} %copy-done.8, ...), custom_call_target="tpu_custom_call" | custom-call | flops 10000000000 | bytes 4000000 | tf_op jit(solution)/shard_map/scan/pallas_call | solution.py:396
  151.7 4.8 %all-to-all-start.1 = ((f32[16,4,512]{2,1,0:T(4,128)}), f32[16,4,512]{2,1,0:T(4,128)S(1)}, u32[]{:S(2)}, u32[]{:S(2)}) async-start(f32[16,4,512]{2,1,0:T(4,128)} %get-tuple-element.38), calls=%async_computation.1 | async-start | bytes 262144 | tf_op jit(solution)/shard_map/all_to_all | solution.py:546
  156.6 4.3 %fetched.2.weight = bf16[8,512,512]{2,1,0:T(8,128)(2,1)} custom-call(s32[1]{0:T(128)} %bitcast.4.refs_0_.rank, f32[4,8,512]{2,1,0:T(8,128)S(1)} %get-tuple-element.42.refs_1_.coef, bf16[1,4096,512]{2,1,0:T(8,128)(2,1)} %all-gather.3.cloned.1.call-done.refs_2_), custom_call_target="tpu_custom_call" | custom-call | flops 2147483648 | bytes 4194304 | tf_op jit(solution)/shard_map/fetched/pallas_call | solution.py:297
  160.9 4.0 %all-to-all-done.1.edges = f32[16,4,512]{2,1,0:T(4,128)S(1)} async-done(((f32[16,4,512]{2,1,0:T(4,128)}), f32[16,4,512]{2,1,0:T(4,128)S(1)}, u32[]{:S(2)}, u32[]{:S(2)}) %all-to-all-start.1) | async-done | bytes 131104 | tf_op jit(solution)/shard_map/all_to_all | solution.py:546
  170.8 7.5 %collective-permute-start.36 = (bf16[3,512,512]{2,1,0:T(8,128)(2,1)S(1)}, bf16[3,512,512]{2,1,0:T(8,128)(2,1)S(1)}, u32[]{:S(2)}, u32[]{:S(2)}) collective-permute-start(bf16[3,512,512]{2,1,0:T(8,128)(2,1)S(1)} %get-tuple-element.46), channel_id=1, source_target_pairs={{0,1},{1,0},{2,3},{3,2},{4,5},{5,4},{6,7},{7,6},{8,9},{9,8},{10,11... | collective-permute-start | bytes 4718600 | tf_op jit(solution)/shard_map/ppermute | solution.py:36
  183.7 6.0 %collective-permute-done.42 = bf16[256,512]{1,0:T(8,128)(2,1)S(1)} collective-permute-done((bf16[256,512]{1,0:T(8,128)(2,1)S(1)}, bf16[256,512]{1,0:T(8,128)(2,1)S(1)}, u32[]{:S(2)}, u32[]{:S(2)}) %collective-permute-start.42) | collective-permute-done | bytes 262176 | tf_op jit(solution)/shard_map/ppermute | solution.py:36
  199.2 5.6 %collective-permute-done.41 = bf16[256,512]{1,0:T(8,128)(2,1)S(1)} collective-permute-done((bf16[256,512]{1,0:T(8,128)(2,1)S(1)}, bf16[256,512]{1,0:T(8,128)(2,1)S(1)}, u32[]{:S(2)}, u32[]{:S(2)}) %collective-permute-start.41) | collective-permute-done | bytes 262176 | tf_op jit(solution)/shard_map/ppermute | solution.py:36
  206.0 6.5 %all-to-all-start.2 = ((bf16[8,4,512]{2,1,0:T(4,128)(2,1)}), bf16[8,4,512]{2,1,0:T(4,128)(2,1)S(1)}, u32[]{:S(2)}, u32[]{:S(2)}) async-start(bf16[8,4,512]{2,1,0:T(4,128)(2,1)} %broadcast_in_dim.5), calls=%async_computation.2 | async-start | bytes 65536 | tf_op jit(solution)/shard_map/all_to_all | solution.py:53
  218.6 3.5 %collective-permute-done.45 = bf16[8,2,512]{2,1,0:T(2,128)(2,1)S(1)} collective-permute-done((bf16[8,2,512]{2,1,0:T(2,128)(2,1)S(1)}, bf16[8,2,512]{2,1,0:T(2,128)(2,1)S(1)}, u32[]{:S(2)}, u32[]{:S(2)}) %collective-permute-start.45) | collective-permute-done | bytes 16416 | tf_op jit(solution)/shard_map/ppermute | solution.py:55
  232.3 3.7 %collective-permute-done.50.refs_10_ = bf16[256,512]{1,0:T(8,128)(2,1)S(1)} collective-permute-done((bf16[256,512]{1,0:T(8,128)(2,1)S(1)}, bf16[256,512]{1,0:T(8,128)(2,1)S(1)}, u32[]{:S(2)}, u32[]{:S(2)}) %collective-permute-start.50) | collective-permute-done | bytes 262176 | tf_op jit(solution)/shard_map/ppermute | solution.py:36
  240.5 12.2 %projected.3 = (bf16[528,512]{1,0:T(8,128)(2,1)}, bf16[512,512]{1,0:T(8,128)(2,1)}) custom-call(s32[1]{0:T(128)} %bitcast.4.refs_0_.rank, s32[1]{0:T(128)} %bitcast.3.refs_1_.place, f32[2,4096]{1,0:T(2,128)} %refs_2_.3, bf16[8,16,512]{2,1,0:T(8,128)(2,1)} %maximum_maximum_fusion.1.refs_3_, bf16[256,512]{1,0:T(8,128)(2,1)} %copy-done.14, ...), custom_call_target="tpu_custom_call" | custom-call | flops 4429185024 | bytes 8388608 | tf_op jit(solution)/shard_map/projected/pallas_call | solution.py:270
  254.9 6.5 %scan.3 = (f32[512,512]{1,0:T(8,128)S(1)}, f32[512,512]{1,0:T(8,128)S(1)}, f32[512,512]{1,0:T(8,128)S(1)}, f32[4,8,512]{2,1,0:T(8,128)S(1)}, f32[16,4,512]{2,1,0:T(4,128)}) custom-call(s32[1]{0:T(128)} %bitcast.4.refs_0_.rank, bf16[528,512]{1,0:T(8,128)(2,1)S(1)} %copy-done.6, f32[2,4,4096]{2,1,0:T(4,128)S(1)} %copy-done.7, f32[2,2,4096]{2,1,0:T(2,128)S(1)} %copy-done.8, ...), custom_call_target="tpu_custom_call" | custom-call | flops 10000000000 | bytes 4000000 | tf_op jit(solution)/shard_map/scan/pallas_call | solution.py:396
  261.4 6.4 %all-to-all-start.3 = ((f32[16,4,512]{2,1,0:T(4,128)}), f32[16,4,512]{2,1,0:T(4,128)S(1)}, u32[]{:S(2)}, u32[]{:S(2)}) async-start(f32[16,4,512]{2,1,0:T(4,128)} %get-tuple-element.54), calls=%async_computation.3 | async-start | bytes 262144 | tf_op jit(solution)/shard_map/all_to_all | solution.py:546
  267.8 4.2 %fetched.3.weight = bf16[8,512,512]{2,1,0:T(8,128)(2,1)} custom-call(s32[1]{0:T(128)} %bitcast.4.refs_0_.rank, f32[4,8,512]{2,1,0:T(8,128)S(1)} %get-tuple-element.58.refs_1_.coef, bf16[3,4096,512]{2,1,0:T(8,128)(2,1)} %all-gather.5.cloned.1.call-done.refs_20_.refs_2_), custom_call_target="tpu_custom_call" | custom-call | flops 2147483648 | bytes 4194304 | tf_op jit(solution)/shard_map/fetched/pallas_call | solution.py:297
  288.7 5.3 %collective-permute-done.66 = bf16[256,512]{1,0:T(8,128)(2,1)S(1)} collective-permute-done((bf16[256,512]{1,0:T(8,128)(2,1)S(1)}, bf16[256,512]{1,0:T(8,128)(2,1)S(1)}, u32[]{:S(2)}, u32[]{:S(2)}) %collective-permute-start.66) | collective-permute-done | bytes 262176 | tf_op jit(solution)/shard_map/ppermute | solution.py:36
  305.0 5.6 %collective-permute-done.65 = bf16[256,512]{1,0:T(8,128)(2,1)S(1)} collective-permute-done((bf16[256,512]{1,0:T(8,128)(2,1)S(1)}, bf16[256,512]{1,0:T(8,128)(2,1)S(1)}, u32[]{:S(2)}, u32[]{:S(2)}) %collective-permute-start.65) | collective-permute-done | bytes 262176 | tf_op jit(solution)/shard_map/ppermute | solution.py:36
  (293 shorter events, 121.0 us)
Async XLA Ops:
  6.5 150.0 %all-gather.3.cloned.1.call-start = ((), (), s32[]{:S(2)}) async-start(), calls=%async_computation.4 | async-start | bytes 4456448 | tf_op jit(solution)/shard_map/all_gather | solution.py:534
  8.4 232.0 %all-gather.5.cloned.1.call-start = ((), (), s32[]{:S(2)}) async-start(), calls=%async_computation.5 | async-start | bytes 13369344 | tf_op jit(solution)/shard_map/all_gather | solution.py:536
  10.7 29.6 %collective-permute-start.2 = (bf16[256,512]{1,0:T(8,128)(2,1)S(1)}, bf16[256,512]{1,0:T(8,128)(2,1)S(1)}, u32[]{:S(2)}, u32[]{:S(2)}) collective-permute-start(bf16[256,512]{1,0:T(8,128)(2,1)S(1)} %get-tuple-element.92.refs_4_), channel_id=1, source_target_pairs={{0,2},{1,3},{2,4},{3,5},{4,6},{5,7},{6,0},{7,1},{8,10},{9,11},{10,... | collective-permute-start | bytes 786440 | tf_op jit(solution)/shard_map/ppermute | solution.py:36
  12.8 29.9 %collective-permute-start.3 = (bf16[256,512]{1,0:T(8,128)(2,1)S(1)}, bf16[256,512]{1,0:T(8,128)(2,1)S(1)}, u32[]{:S(2)}, u32[]{:S(2)}) collective-permute-start(bf16[256,512]{1,0:T(8,128)(2,1)S(1)} %get-tuple-element.91.refs_5_), channel_id=1, source_target_pairs={{0,2},{1,3},{2,4},{3,5},{4,6},{5,7},{6,0},{7,1},{8,10},{9,11},{10,... | collective-permute-start | bytes 786440 | tf_op jit(solution)/shard_map/ppermute | solution.py:36
  14.6 13.1 %all-to-all-start = ((bf16[8,4,512]{2,1,0:T(4,128)(2,1)}), bf16[8,4,512]{2,1,0:T(4,128)(2,1)S(1)}, u32[]{:S(2)}, u32[]{:S(2)}) async-start(bf16[8,4,512]{2,1,0:T(4,128)(2,1)} %broadcast_in_dim.4), calls=%async_computation | async-start | bytes 65536 | tf_op jit(solution)/shard_map/all_to_all | solution.py:53
  19.2 24.1 %collective-permute-start.16 = (bf16[256,512]{1,0:T(8,128)(2,1)S(1)}, bf16[256,512]{1,0:T(8,128)(2,1)S(1)}, u32[]{:S(2)}, u32[]{:S(2)}) collective-permute-start(bf16[256,512]{1,0:T(8,128)(2,1)S(1)} %pad_maximum_fusion.3), channel_id=1, source_target_pairs={{0,8},{8,16},{16,24},{24,0},{32,40},{40,48},{48,56},{56,32},{64,72... | collective-permute-start | bytes 786440 | tf_op jit(solution)/shard_map/ppermute | solution.py:84
  40.2 11.1 %collective-permute-start.27 = (bf16[256,512]{1,0:T(8,128)(2,1)S(1)}, bf16[256,512]{1,0:T(8,128)(2,1)S(1)}, u32[]{:S(2)}, u32[]{:S(2)}) collective-permute-start(bf16[256,512]{1,0:T(8,128)(2,1)S(1)} %pad_maximum_fusion.4), channel_id=1, source_target_pairs={{0,96},{8,104},{16,112},{24,120},{32,0},{40,8},{48,16},{56,24},{64... | collective-permute-start | bytes 786440 | tf_op jit(solution)/shard_map/ppermute | solution.py:84
  43.3 10.9 %collective-permute-start.5 = (bf16[256,512]{1,0:T(8,128)(2,1)S(1)}, bf16[256,512]{1,0:T(8,128)(2,1)S(1)}, u32[]{:S(2)}, u32[]{:S(2)}) collective-permute-start(bf16[256,512]{1,0:T(8,128)(2,1)S(1)} %get-tuple-element.91.refs_5_), channel_id=1, source_target_pairs={{0,6},{1,7},{2,0},{3,1},{4,2},{5,3},{6,4},{7,5},{8,14},{9,15},{10,... | collective-permute-start | bytes 786440 | tf_op jit(solution)/shard_map/ppermute | solution.py:36
  54.2 11.4 %collective-permute-start.28 = (bf16[128,512]{1,0:T(8,128)(2,1)S(1)}, bf16[128,512]{1,0:T(8,128)(2,1)S(1)}, u32[]{:S(2)}, u32[]{:S(2)}) collective-permute-start(bf16[128,512]{1,0:T(8,128)(2,1)S(1)} %slice.249), channel_id=1, source_target_pairs={{0,32},{8,40},{16,48},{24,56},{32,64},{40,72},{48,80},{56,88},{64,... | collective-permute-start | bytes 393224 | tf_op jit(solution)/shard_map/ppermute | solution.py:84
  54.3 13.7 %collective-permute-start.29 = (bf16[128,512]{1,0:T(8,128)(2,1)S(1)}, bf16[128,512]{1,0:T(8,128)(2,1)S(1)}, u32[]{:S(2)}, u32[]{:S(2)}) collective-permute-start(bf16[128,512]{1,0:T(8,128)(2,1)S(1)} %slice.250), channel_id=1, source_target_pairs={{0,96},{8,104},{16,112},{24,120},{32,0},{40,8},{48,16},{56,24},{64... | collective-permute-start | bytes 393224 | tf_op jit(solution)/shard_map/ppermute | solution.py:84
  60.5 10.8 %collective-permute-start.10 = (bf16[256,512]{1,0:T(8,128)(2,1)S(1)}, bf16[256,512]{1,0:T(8,128)(2,1)S(1)}, u32[]{:S(2)}, u32[]{:S(2)}) collective-permute-start(bf16[256,512]{1,0:T(8,128)(2,1)S(1)} %collective-permute-done.2.refs_6_), channel_id=1, source_target_pairs={{0,1},{1,0},{2,3},{3,2},{4,5},{5,4},{6,7},{7,6},{8,9},{9,8},{10,11... | collective-permute-start | bytes 786440 | tf_op jit(solution)/shard_map/ppermute | solution.py:36
  68.1 13.7 %collective-permute-start.20 = (bf16[512,512]{1,0:T(8,128)(2,1)S(1)}, bf16[512,512]{1,0:T(8,128)(2,1)S(1)}, u32[]{:S(2)}, u32[]{:S(2)}) collective-permute-start(bf16[512,512]{1,0:T(8,128)(2,1)S(1)} %pad_maximum_fusion.1.refs_20_), channel_id=1, source_target_pairs={{0,32},{8,40},{16,48},{24,56},{32,64},{40,72},{48,80},{56,88},{64,... | collective-permute-start | bytes 1572872 | tf_op jit(solution)/shard_map/ppermute | solution.py:84
  69.2 15.1 %collective-permute-start.22 = (bf16[512,512]{1,0:T(8,128)(2,1)S(1)}, bf16[512,512]{1,0:T(8,128)(2,1)S(1)}, u32[]{:S(2)}, u32[]{:S(2)}) collective-permute-start(bf16[512,512]{1,0:T(8,128)(2,1)S(1)} %pad_maximum_fusion.1.refs_20_), channel_id=1, source_target_pairs={{0,96},{8,104},{16,112},{24,120},{32,0},{40,8},{48,16},{56,24},{64... | collective-permute-start | bytes 1572872 | tf_op jit(solution)/shard_map/ppermute | solution.py:84
  75.5 16.6 %collective-permute-start.30 = (bf16[512,512]{1,0:T(8,128)(2,1)S(1)}, bf16[512,512]{1,0:T(8,128)(2,1)S(1)}, u32[]{:S(2)}, u32[]{:S(2)}) collective-permute-start(bf16[512,512]{1,0:T(8,128)(2,1)S(1)} %pad_maximum_fusion.2.refs_28_), channel_id=1, source_target_pairs={{0,8},{8,16},{16,24},{24,0},{32,40},{40,48},{48,56},{56,32},{64,72... | collective-permute-start | bytes 1572872 | tf_op jit(solution)/shard_map/ppermute | solution.py:84
  75.9 17.2 %collective-permute-start.32 = (bf16[512,512]{1,0:T(8,128)(2,1)S(1)}, bf16[512,512]{1,0:T(8,128)(2,1)S(1)}, u32[]{:S(2)}, u32[]{:S(2)}) collective-permute-start(bf16[512,512]{1,0:T(8,128)(2,1)S(1)} %pad_maximum_fusion.2.refs_28_), channel_id=1, source_target_pairs={{0,24},{8,0},{16,8},{24,16},{32,56},{40,32},{48,40},{56,48},{64,88... | collective-permute-start | bytes 1572872 | tf_op jit(solution)/shard_map/ppermute | solution.py:84
  78.2 20.3 %collective-permute-start.21 = (bf16[512,512]{1,0:T(8,128)(2,1)S(1)}, bf16[512,512]{1,0:T(8,128)(2,1)S(1)}, u32[]{:S(2)}, u32[]{:S(2)}) collective-permute-start(bf16[512,512]{1,0:T(8,128)(2,1)S(1)} %constant_dynamic-update-slice_fusion.refs_21_), channel_id=1, source_target_pairs={{0,32},{8,40},{16,48},{24,56},{32,64},{40,72},{48,80},{56,88},{64,... | collective-permute-start | bytes 1572872 | tf_op jit(solution)/shard_map/ppermute | solution.py:84
  81.8 24.3 %collective-permute-start.23 = (bf16[512,512]{1,0:T(8,128)(2,1)S(1)}, bf16[512,512]{1,0:T(8,128)(2,1)}, u32[]{:S(2)}, u32[]{:S(2)}) collective-permute-start(bf16[512,512]{1,0:T(8,128)(2,1)S(1)} %constant_dynamic-update-slice_fusion.refs_21_), channel_id=1, source_target_pairs={{0,96},{8,104},{16,112},{24,120},{32,0},{40,8},{48,16},{56,24},{64... | collective-permute-start | bytes 1572872 | tf_op jit(solution)/shard_map/ppermute | solution.py:84
  84.3 28.6 %collective-permute-start.33 = (bf16[512,512]{1,0:T(8,128)(2,1)S(1)}, bf16[512,512]{1,0:T(8,128)(2,1)S(1)}, u32[]{:S(2)}, u32[]{:S(2)}) collective-permute-start(bf16[512,512]{1,0:T(8,128)(2,1)S(1)} %constant_dynamic-update-slice_fusion.3.refs_29_), channel_id=1, source_target_pairs={{0,24},{8,0},{16,8},{24,16},{32,56},{40,32},{48,40},{56,48},{64,88... | collective-permute-start | bytes 1572872 | tf_op jit(solution)/shard_map/ppermute | solution.py:84
  92.1 25.0 %collective-permute-start.31 = (bf16[512,512]{1,0:T(8,128)(2,1)S(1)}, bf16[512,512]{1,0:T(8,128)(2,1)}, u32[]{:S(2)}, u32[]{:S(2)}) collective-permute-start(bf16[512,512]{1,0:T(8,128)(2,1)S(1)} %constant_dynamic-update-slice_fusion.3.refs_29_), channel_id=1, source_target_pairs={{0,8},{8,16},{16,24},{24,0},{32,40},{40,48},{48,56},{56,32},{64,72... | collective-permute-start | bytes 1572872 | tf_op jit(solution)/shard_map/ppermute | solution.py:84
  93.1 24.2 %collective-permute-start.24 = (bf16[512,512]{1,0:T(8,128)(2,1)S(1)}, bf16[512,512]{1,0:T(8,128)(2,1)}, u32[]{:S(2)}, u32[]{:S(2)}) collective-permute-start(bf16[512,512]{1,0:T(8,128)(2,1)S(1)} %collective-permute-done.20.refs_22_), channel_id=1, source_target_pairs={{0,32},{8,40},{16,48},{24,56},{32,64},{40,72},{48,80},{56,88},{64,... | collective-permute-start | bytes 1572872 | tf_op jit(solution)/shard_map/ppermute | solution.py:84
  98.5 27.0 %collective-permute-start.34 = (bf16[512,512]{1,0:T(8,128)(2,1)S(1)}, bf16[512,512]{1,0:T(8,128)(2,1)}, u32[]{:S(2)}, u32[]{:S(2)}) collective-permute-start(bf16[512,512]{1,0:T(8,128)(2,1)S(1)} %collective-permute-done.30.refs_30_), channel_id=1, source_target_pairs={{0,8},{8,16},{16,24},{24,0},{32,40},{40,48},{48,56},{56,32},{64,72... | collective-permute-start | bytes 1572872 | tf_op jit(solution)/shard_map/ppermute | solution.py:84
  106.2 19.3 %collective-permute-start.25 = (bf16[512,512]{1,0:T(8,128)(2,1)}, bf16[512,512]{1,0:T(8,128)(2,1)}, u32[]{:S(2)}, u32[]{:S(2)}) collective-permute-start(bf16[512,512]{1,0:T(8,128)(2,1)} %collective-permute-done.23.refs_25_), channel_id=1, source_target_pairs={{0,96},{8,104},{16,112},{24,120},{32,0},{40,8},{48,16},{56,24},{64... | collective-permute-start | bytes 1572872 | tf_op jit(solution)/shard_map/ppermute | solution.py:84
  113.0 18.4 %collective-permute-start.35 = (bf16[512,512]{1,0:T(8,128)(2,1)S(1)}, bf16[512,512]{1,0:T(8,128)(2,1)}, u32[]{:S(2)}, u32[]{:S(2)}) collective-permute-start(bf16[512,512]{1,0:T(8,128)(2,1)S(1)} %collective-permute-done.33.refs_33_), channel_id=1, source_target_pairs={{0,24},{8,0},{16,8},{24,16},{32,56},{40,32},{48,40},{56,48},{64,88... | collective-permute-start | bytes 1572872 | tf_op jit(solution)/shard_map/ppermute | solution.py:84
  151.7 13.2 %all-to-all-start.1 = ((f32[16,4,512]{2,1,0:T(4,128)}), f32[16,4,512]{2,1,0:T(4,128)S(1)}, u32[]{:S(2)}, u32[]{:S(2)}) async-start(f32[16,4,512]{2,1,0:T(4,128)} %get-tuple-element.38), calls=%async_computation.1 | async-start | bytes 262144 | tf_op jit(solution)/shard_map/all_to_all | solution.py:546
  170.8 20.3 %collective-permute-start.36 = (bf16[3,512,512]{2,1,0:T(8,128)(2,1)S(1)}, bf16[3,512,512]{2,1,0:T(8,128)(2,1)S(1)}, u32[]{:S(2)}, u32[]{:S(2)}) collective-permute-start(bf16[3,512,512]{2,1,0:T(8,128)(2,1)S(1)} %get-tuple-element.46), channel_id=1, source_target_pairs={{0,1},{1,0},{2,3},{3,2},{4,5},{5,4},{6,7},{7,6},{8,9},{9,8},{10,11... | collective-permute-start | bytes 4718600 | tf_op jit(solution)/shard_map/ppermute | solution.py:36
  206.0 11.3 %all-to-all-start.2 = ((bf16[8,4,512]{2,1,0:T(4,128)(2,1)}), bf16[8,4,512]{2,1,0:T(4,128)(2,1)S(1)}, u32[]{:S(2)}, u32[]{:S(2)}) async-start(bf16[8,4,512]{2,1,0:T(4,128)(2,1)} %broadcast_in_dim.5), calls=%async_computation.2 | async-start | bytes 65536 | tf_op jit(solution)/shard_map/all_to_all | solution.py:53
  212.5 15.1 %collective-permute-start.46 = (bf16[256,512]{1,0:T(8,128)(2,1)S(1)}, bf16[256,512]{1,0:T(8,128)(2,1)S(1)}, u32[]{:S(2)}, u32[]{:S(2)}) collective-permute-start(bf16[256,512]{1,0:T(8,128)(2,1)S(1)} %get-tuple-element.70.refs_4_), channel_id=1, source_target_pairs={{0,2},{1,3},{2,4},{3,5},{4,6},{5,7},{6,0},{7,1},{8,10},{9,11},{10,... | collective-permute-start | bytes 786440 | tf_op jit(solution)/shard_map/ppermute | solution.py:36
  213.8 13.8 %collective-permute-start.47 = (bf16[256,512]{1,0:T(8,128)(2,1)S(1)}, bf16[256,512]{1,0:T(8,128)(2,1)S(1)}, u32[]{:S(2)}, u32[]{:S(2)}) collective-permute-start(bf16[256,512]{1,0:T(8,128)(2,1)S(1)} %get-tuple-element.69.refs_5_), channel_id=1, source_target_pairs={{0,2},{1,3},{2,4},{3,5},{4,6},{5,7},{6,0},{7,1},{8,10},{9,11},{10,... | collective-permute-start | bytes 786440 | tf_op jit(solution)/shard_map/ppermute | solution.py:36
  215.0 14.1 %collective-permute-start.49 = (bf16[256,512]{1,0:T(8,128)(2,1)S(1)}, bf16[256,512]{1,0:T(8,128)(2,1)S(1)}, u32[]{:S(2)}, u32[]{:S(2)}) collective-permute-start(bf16[256,512]{1,0:T(8,128)(2,1)S(1)} %get-tuple-element.69.refs_5_), channel_id=1, source_target_pairs={{0,6},{1,7},{2,0},{3,1},{4,2},{5,3},{6,4},{7,5},{8,14},{9,15},{10,... | collective-permute-start | bytes 786440 | tf_op jit(solution)/shard_map/ppermute | solution.py:36
  216.5 13.8 %collective-permute-start.48 = (bf16[256,512]{1,0:T(8,128)(2,1)S(1)}, bf16[256,512]{1,0:T(8,128)(2,1)S(1)}, u32[]{:S(2)}, u32[]{:S(2)}) collective-permute-start(bf16[256,512]{1,0:T(8,128)(2,1)S(1)} %get-tuple-element.70.refs_4_), channel_id=1, source_target_pairs={{0,6},{1,7},{2,0},{3,1},{4,2},{5,3},{6,4},{7,5},{8,14},{9,15},{10,... | collective-permute-start | bytes 786440 | tf_op jit(solution)/shard_map/ppermute | solution.py:36
  261.4 13.2 %all-to-all-start.3 = ((f32[16,4,512]{2,1,0:T(4,128)}), f32[16,4,512]{2,1,0:T(4,128)S(1)}, u32[]{:S(2)}, u32[]{:S(2)}) async-start(f32[16,4,512]{2,1,0:T(4,128)} %get-tuple-element.54), calls=%async_computation.3 | async-start | bytes 262144 | tf_op jit(solution)/shard_map/all_to_all | solution.py:546
  280.5 16.7 %collective-permute-start.60 = (bf16[3,512,512]{2,1,0:T(8,128)(2,1)S(1)}, bf16[3,512,512]{2,1,0:T(8,128)(2,1)S(1)}, u32[]{:S(2)}, u32[]{:S(2)}) collective-permute-start(bf16[3,512,512]{2,1,0:T(8,128)(2,1)S(1)} %get-tuple-element.62), channel_id=1, source_target_pairs={{0,1},{1,0},{2,3},{3,2},{4,5},{5,4},{6,7},{7,6},{8,9},{9,8},{10,11... | collective-permute-start | bytes 4718600 | tf_op jit(solution)/shard_map/ppermute | solution.py:36
  (102 other events, 1483.7 us)
Sparse Core Ops, SparseCore 0:
  9.5 59.8 all-gather.2
  71.5 108.3 all-gather.4

commit v4 on v3

--- a/solution.py
+++ b/solution.py
@@ -15,8 +15,7 @@
 CHUNKS = 8
 SCAN_LIMIT = 24 * 2**20
 PROJECT_LIMIT = 56 * 2**20
-FETCH_LIMIT = 50 * 2**20
-GIVE_LIMIT = 12 * 2**20
+GIVE_LIMIT = 48 * 2**20
 KEEP_LIMIT = 8 * 2**20
 HALO = 16
 
@@ -235,14 +234,6 @@
     gate[...] = (total[...] * scale)[: gate.shape[0]].astype(BF16)
 
 
-def fetch_body(which, rank, after, weight, out, sems):
-    copies = block_copies(weight, which, rank[0], LEAVE, out, sems)
-    for copy in copies:
-        copy.start()
-    for copy in copies:
-        copy.wait()
-
-
 def in_smem():
     return pl.BlockSpec(memory_space=pltpu.SMEM)
 
@@ -289,21 +280,6 @@
         cost_estimate=product_cost(deep, width, 2 * count),
         name="projected",
     )(rank, place, norm_gain, halo, *pieces, *sources)
-
-
-def fetched(rank, after, weights, which):
-    width = weights.shape[2]
-    count = weights.shape[1] // width
-    return pl.pallas_call(
-        lambda *refs: fetch_body(which, *refs),
-        out_shape=jax.ShapeDtypeStruct((count, width, width), BF16),
-        in_specs=[in_smem(), in_vmem(), in_hbm()],
-        out_specs=in_vmem(),
-        scratch_shapes=[pltpu.SemaphoreType.DMA((count,))],
-        compiler_params=pltpu.CompilerParams(vmem_limit_bytes=FETCH_LIMIT),
-        cost_estimate=product_cost(width, width, count),
-        name="fetched",
-    )(rank, after, weights)
 
 
 def scan_body(
@@ -439,8 +415,13 @@
 
 
 def give_body(
-    place, edges, local, fwd_cum, bwd_cum, coef, gate, weight, mixed, far, rest
+    which, rank, place, edges, local, fwd_cum, bwd_cum, coef, gate, weight,
+    mixed, far, rest, keep_in, give_in, give_sems, keep_sems,
 ):
+    gives = block_copies(weight, which, rank[0], LEAVE[:4], give_in, give_sems)
+    keeps = block_copies(weight, which, rank[0], LEAVE[4:], keep_in, keep_sems)
+    for copy in gives:
+        copy.start()
     mine = place[0]
     count, _, width = edges.shape
     enter_f = jnp.zeros((1, width), F32)
@@ -465,37 +446,49 @@
             return carry
 
         lax.fori_loop(0, local.shape[0] // group, part, 0)
-    far[...] = features(mixed[...], weight[0])
+    for copy in keeps:
+        copy.start()
+    for copy in gives:
+        copy.wait()
+    far[...] = features(mixed[...], give_in[0])
 
     def step(n, carry):
-        rest[n] = features(mixed[...], weight[n + 1])
+        rest[n] = features(mixed[...], give_in[n + 1])
         return carry
 
     lax.fori_loop(0, 3, step, 0)
-
-
-def given(place, edges, local, fwd_cum, bwd_cum, coef, gate, weight):
+    for copy in keeps:
+        copy.wait()
+
+
+def given(rank, place, edges, local, fwd_cum, bwd_cum, coef, gate, weights, which):
     length, width = local.shape
     return pl.pallas_call(
-        give_body,
-        in_specs=[in_smem()] + [in_vmem()] * 7,
-        out_specs=[in_vmem()] * 3,
+        lambda *refs: give_body(which, *refs),
+        in_specs=[in_smem()] * 2 + [in_vmem()] * 6 + [in_hbm()],
+        out_specs=[in_vmem()] * 4,
         out_shape=[
             jax.ShapeDtypeStruct((length, width), BF16),
             jax.ShapeDtypeStruct((length, width), BF16),
             jax.ShapeDtypeStruct((3, length, width), BF16),
+            jax.ShapeDtypeStruct((4, width, width), BF16),
+        ],
+        scratch_shapes=[
+            pltpu.VMEM((4, width, width), BF16),
+            pltpu.SemaphoreType.DMA((4,)),
+            pltpu.SemaphoreType.DMA((4,)),
         ],
         compiler_params=pltpu.CompilerParams(vmem_limit_bytes=GIVE_LIMIT),
         cost_estimate=product_cost(length, width, 4),
         name="given",
-    )(place, edges, local, fwd_cum, bwd_cum, coef, gate, weight)
+    )(rank, place, edges, local, fwd_cum, bwd_cum, coef, gate, weights)
 
 
 def keep_body(mixed, weight, far, rest):
-    far[...] = features(mixed[...], weight[4])
+    far[...] = features(mixed[...], weight[0])
 
     def step(n, carry):
-        rest[n] = features(mixed[...], weight[n + 5])
+        rest[n] = features(mixed[...], weight[n + 1])
         return carry
 
     lax.fori_loop(0, 3, step, 0)
@@ -544,13 +537,12 @@
             rank, mix_in, conv_taps, forget_rate, block_gates, layer, lax.axis_size("sp")
         )
         edges = lax.all_to_all(edge, "sp", 0, 0, tiled=True)
-        out_weight = fetched(rank, coef, full, which)
-        mixed, far_give, rest_give = given(
-            place, edges, local, fwd_cum, bwd_cum, coef, gate_z, out_weight
+        mixed, far_give, rest_give, keep_weight = given(
+            rank, place, edges, local, fwd_cum, bwd_cum, coef, gate_z, full, which
         )
         far_away = across(far_give)
         rest_away = across(rest_give)
-        far_keep, rest_keep = kept(mixed, out_weight)
+        far_keep, rest_keep = kept(mixed, keep_weight)
         far = total_of(far_keep, far_away).astype(BF16)
         halves = (slice(0, half), slice(half, length))
         up, down, own = (

time: 321 us -> 298 us (0.928)
  starting transfers between devices: 125 us -> 96.3 us
  blocking collectives: 0 us -> 26.6 us
  waiting for transfers between devices: 104 us -> 89.3 us
  Pallas kernels: 55.2 us -> 51.9 us
    all_to_all x0 -> x2, blocking collectives: none -> 26.6 us  [per_device(): edges = lax.all_to_all(edge, 'sp', 0, 0, tiled=True)]
    ppermute x44, starting transfers between devices: 61.3 us -> 49.6 us  [shifted(): return lax.ppermute(array, axis, [(i, move(i)) for i in range(count)])]
    all_to_all x2 -> x0, starting transfers between devices: 11.2 us -> none  [per_device(): edges = lax.all_to_all(edge, 'sp', 0, 0, tiled=True)]
    all_to_all x2 -> x0, waiting for transfers between devices: 6.65 us -> none  [per_device(): edges = lax.all_to_all(edge, 'sp', 0, 0, tiled=True)]
    all_to_all x2, waiting for transfers between devices: 7.79 us -> 1.83 us  [token_halo(): every = lax.all_to_all(copies, 'tp', 0, 0, tiled=True)]
    ppermute x44, waiting for transfers between devices: 39.8 us -> 34 us  [shifted(): return lax.ppermute(array, axis, [(i, move(i)) for i in range(count)])]
    ppermute x20, starting transfers between devices: 32.2 us -> 27.5 us  [along_plane(): return lax.ppermute(array, 'sp', pairs)]
    ppermute x20, waiting for transfers between devices: 45 us -> 48.5 us  [along_plane(): return lax.ppermute(array, 'sp', pairs)]
  transfers between devices with their start and end apart: 74 -> 72, of which waited for: 31 -> 29; matrix products, arithmetic and copies ran while one was open for 2% -> 2% of each run, Pallas kernels for 11% -> 10%
where the time goes in v4:
time: 298 us; the launch traced here: 297 us
  starting transfers between devices  96.3 us (32%)
  waiting for transfers between devices  89.3 us (30%)
  Pallas kernels  51.9 us (17%)
  blocking collectives  26.6 us (9%)
  local copies, waits for them, and re-layouts  14.6 us (5%)
  between operations  14.4 us (5%)
  other arithmetic  4.31 us (1%)
    ppermute x44, starting transfers between devices, shifted(): return lax.ppermute(array, axis, [(i, move(i)) for i in range(count)])  49.6 us
    ppermute x20, waiting for transfers between devices, along_plane(): return lax.ppermute(array, 'sp', pairs)  48.5 us
    ppermute x44, waiting for transfers between devices, shifted(): return lax.ppermute(array, axis, [(i, move(i)) for i in range(count)])  34 us
    ppermute x20, starting transfers between devices, along_plane(): return lax.ppermute(array, 'sp', pairs)  27.5 us
    all_to_all x2, blocking collectives, per_device(): edges = lax.all_to_all(edge, 'sp', 0, 0, tiled=True)  26.6 us
    pallas_call x2, Pallas kernels, projected(): pl.pallas_call(lambda *refs: project_body(layer, *refs), out_shape=[jax.S...  25.7 us
    pallas_call x2, Pallas kernels, scanned(): pl.pallas_call(scan_body, grid_spec=pltpu.PrefetchScalarGridSpec(num_scal...  11.8 us
    all_to_all x2, starting transfers between devices, token_halo(): every = lax.all_to_all(copies, 'tp', 0, 0, tiled=True)  11.2 us
  transfers between devices with their start and end apart: 72, of which 29 were waited for; matrix products, arithmetic and copies ran while one was open for 2% of the time, Pallas kernels for 10%

profile of v4, /device:TPU:1, one launch (start us, length us, event | category | flops | bytes accessed | tf_op | source)
XLA Modules:
  0.0 297.4 jit_solution(11055061652597589557)
XLA Ops:
  11.5 5.8 %all-to-all-start = ((bf16[8,4,512]{2,1,0:T(4,128)(2,1)}), bf16[8,4,512]{2,1,0:T(4,128)(2,1)S(1)}, u32[]{:S(2)}, u32[]{:S(2)}) async-start(bf16[8,4,512]{2,1,0:T(4,128)(2,1)} %broadcast_in_dim.4), calls=%async_computation | async-start | bytes 65536 | tf_op jit(solution)/shard_map/all_to_all | solution.py:52
  17.3 2.8 collective-permute-start.17
  22.0 3.2 %collective-permute-start = (bf16[8,2,512]{2,1,0:T(2,128)(2,1)S(1)}, bf16[8,2,512]{2,1,0:T(2,128)(2,1)S(1)}, u32[]{:S(2)}, u32[]{:S(2)}) collective-permute-start(bf16[8,2,512]{2,1,0:T(2,128)(2,1)S(1)} %get-tuple-element.103), channel_id=1, source_target_pairs={{0,8},{8,16},{16,24},{24,32},{32,40},{40,48},{48,56},{56,64},{64,7... | collective-permute-start | bytes 49160 | tf_op jit(solution)/shard_map/ppermute | solution.py:53
  26.5 6.7 %collective-permute-start.27 = (bf16[256,512]{1,0:T(8,128)(2,1)S(1)}, bf16[256,512]{1,0:T(8,128)(2,1)S(1)}, u32[]{:S(2)}, u32[]{:S(2)}) collective-permute-start(bf16[256,512]{1,0:T(8,128)(2,1)S(1)} %pad_maximum_fusion.4), channel_id=1, source_target_pairs={{0,96},{8,104},{16,112},{24,120},{32,0},{40,8},{48,16},{56,24},{64... | collective-permute-start | bytes 786440 | tf_op jit(solution)/shard_map/ppermute | solution.py:83
  36.0 3.4 %collective-permute-done.27 = bf16[256,512]{1,0:T(8,128)(2,1)S(1)} collective-permute-done((bf16[256,512]{1,0:T(8,128)(2,1)S(1)}, bf16[256,512]{1,0:T(8,128)(2,1)S(1)}, u32[]{:S(2)}, u32[]{:S(2)}) %collective-permute-start.27) | collective-permute-done | bytes 262176 | tf_op jit(solution)/shard_map/ppermute | solution.py:83
  51.2 3.4 %collective-permute-done.18 = bf16[128,512]{1,0:T(8,128)(2,1)S(1)} collective-permute-done((bf16[128,512]{1,0:T(8,128)(2,1)S(1)}, bf16[128,512]{1,0:T(8,128)(2,1)S(1)}, u32[]{:S(2)}, u32[]{:S(2)}) %collective-permute-start.18) | collective-permute-done | bytes 131104 | tf_op jit(solution)/shard_map/ppermute | solution.py:83
  57.4 2.7 collective-permute-start.13
  64.8 2.7 collective-permute-start.32
  72.9 6.5 %collective-permute-done.20.refs_22_ = bf16[512,512]{1,0:T(8,128)(2,1)S(1)} collective-permute-done((bf16[512,512]{1,0:T(8,128)(2,1)S(1)}, bf16[512,512]{1,0:T(8,128)(2,1)S(1)}, u32[]{:S(2)}, u32[]{:S(2)}) %collective-permute-start.20) | collective-permute-done | bytes 524320 | tf_op jit(solution)/shard_map/ppermute | solution.py:83
  84.7 4.4 %collective-permute-done.23.refs_25_ = bf16[512,512]{1,0:T(8,128)(2,1)} collective-permute-done((bf16[512,512]{1,0:T(8,128)(2,1)S(1)}, bf16[512,512]{1,0:T(8,128)(2,1)}, u32[]{:S(2)}, u32[]{:S(2)}) %collective-permute-start.23) | collective-permute-done | bytes 524320 | tf_op jit(solution)/shard_map/ppermute | solution.py:83
  90.3 5.3 %collective-permute-done.33.refs_33_ = bf16[512,512]{1,0:T(8,128)(2,1)} collective-permute-done((bf16[512,512]{1,0:T(8,128)(2,1)S(1)}, bf16[512,512]{1,0:T(8,128)(2,1)}, u32[]{:S(2)}, u32[]{:S(2)}) %collective-permute-start.33) | collective-permute-done | bytes 524320 | tf_op jit(solution)/shard_map/ppermute | solution.py:83
  95.6 2.6 collective-permute-done.21.refs_23_
  100.1 4.7 %collective-permute-done.31.refs_31_ = bf16[512,512]{1,0:T(8,128)(2,1)S(1)} collective-permute-done((bf16[512,512]{1,0:T(8,128)(2,1)S(1)}, bf16[512,512]{1,0:T(8,128)(2,1)S(1)}, u32[]{:S(2)}, u32[]{:S(2)}) %collective-permute-start.31) | collective-permute-done | bytes 524320 | tf_op jit(solution)/shard_map/ppermute | solution.py:83
  104.8 14.6 %collective-permute-done.24.refs_26_ = bf16[512,512]{1,0:T(8,128)(2,1)} collective-permute-done((bf16[512,512]{1,0:T(8,128)(2,1)S(1)}, bf16[512,512]{1,0:T(8,128)(2,1)}, u32[]{:S(2)}, u32[]{:S(2)}) %collective-permute-start.24) | collective-permute-done | bytes 524320 | tf_op jit(solution)/shard_map/ppermute | solution.py:83
  119.4 3.0 collective-permute-done.34.refs_34_
  122.4 13.5 %projected.2 = (bf16[528,512]{1,0:T(8,128)(2,1)}, bf16[512,512]{1,0:T(8,128)(2,1)}) custom-call(s32[1]{0:T(128)} %bitcast.3.refs_0_.rank, s32[1]{0:T(128)} %bitcast.4.refs_1_, f32[2,4096]{1,0:T(2,128)} %refs_2_.3, bf16[8,16,512]{2,1,0:T(8,128)(2,1)} %maximum_maximum_fusion.refs_3_, bf16[256,512]{1,0:T(8,128)(2,1)} %copy-done.22, ...), custom_call_target="tpu_custom_call" | custom-call | flops 4429185024 | bytes 8388608 | tf_op jit(solution)/shard_map/projected/pallas_call | solution.py:261
  137.0 5.9 %scan.2 = (f32[512,512]{1,0:T(8,128)S(1)}, f32[512,512]{1,0:T(8,128)S(1)}, f32[512,512]{1,0:T(8,128)S(1)}, f32[4,8,512]{2,1,0:T(8,128)S(1)}, f32[16,4,512]{2,1,0:T(4,128)S(1)}) custom-call(s32[1]{0:T(128)} %bitcast.3.refs_0_.rank, bf16[528,512]{1,0:T(8,128)(2,1)S(1)} %copy-done.9, f32[2,4,4096]{2,1,0:T(4,128)S(1)} %copy-done.7, f32[2,2,4096]{2,1,0:T(2,128)S(1)} %copy-done.8, ...), custom_call_target="tpu_custom_call" | custom-call | flops 10000000000 | bytes 4000000 | tf_op jit(solution)/shard_map/scan/pallas_call | solution.py:372
  142.9 12.8 %all_to_all.20.refs_2_ = f32[16,4,512]{2,1,0:T(4,128)S(1)} all-to-all(f32[16,4,512]{2,1,0:T(4,128)S(1)} %get-tuple-element.40), channel_id=1, replica_groups=mesh['sp'=16,'tp'=8] {'sp'}, dimensions={0} | all-to-all | bytes 262144 | tf_op jit(solution)/shard_map/all_to_all | solution.py:539
  156.8 5.4 %given.2 = (bf16[512,512]{1,0:T(8,128)(2,1)S(1)}, bf16[512,512]{1,0:T(8,128)(2,1)S(1)}, bf16[3,512,512]{2,1,0:T(8,128)(2,1)}, bf16[4,512,512]{2,1,0:T(8,128)(2,1)}) custom-call(s32[1]{0:T(128)} %bitcast.3.refs_0_.rank, s32[1]{0:T(128)} %bitcast.4.refs_1_, f32[16,4,512]{2,1,0:T(4,128)S(1)} %all_to_all.20.refs_2_, f32[512,512]{1,0:T(8,128)S(1)} %get-tuple-element.41.refs_3_, ...), custom_call_target="tpu_custom_call" | custom-call | flops 1073741824 | bytes 2097152 | tf_op jit(solution)/shard_map/given/pallas_call | solution.py:466
  173.0 4.4 %collective-permute-done.38 = bf16[256,512]{1,0:T(8,128)(2,1)S(1)} collective-permute-done((bf16[256,512]{1,0:T(8,128)(2,1)S(1)}, bf16[256,512]{1,0:T(8,128)(2,1)S(1)}, u32[]{:S(2)}, u32[]{:S(2)}) %collective-permute-start.38) | collective-permute-done | bytes 262176 | tf_op jit(solution)/shard_map/ppermute | solution.py:35
  182.9 5.6 %collective-permute-done.39 = bf16[256,512]{1,0:T(8,128)(2,1)S(1)} collective-permute-done((bf16[256,512]{1,0:T(8,128)(2,1)S(1)}, bf16[256,512]{1,0:T(8,128)(2,1)S(1)}, u32[]{:S(2)}, u32[]{:S(2)}) %collective-permute-start.39) | collective-permute-done | bytes 262176 | tf_op jit(solution)/shard_map/ppermute | solution.py:35
  189.7 5.5 %all-to-all-start.2 = ((bf16[8,4,512]{2,1,0:T(4,128)(2,1)}), bf16[8,4,512]{2,1,0:T(4,128)(2,1)S(1)}, u32[]{:S(2)}, u32[]{:S(2)}) async-start(bf16[8,4,512]{2,1,0:T(4,128)(2,1)} %broadcast_in_dim.5), calls=%async_computation.2 | async-start | bytes 65536 | tf_op jit(solution)/shard_map/all_to_all | solution.py:52
  204.9 4.0 %collective-permute-done.45 = bf16[8,2,512]{2,1,0:T(2,128)(2,1)S(1)} collective-permute-done((bf16[8,2,512]{2,1,0:T(2,128)(2,1)S(1)}, bf16[8,2,512]{2,1,0:T(2,128)(2,1)S(1)}, u32[]{:S(2)}, u32[]{:S(2)}) %collective-permute-start.45) | collective-permute-done | bytes 16416 | tf_op jit(solution)/shard_map/ppermute | solution.py:54
  211.7 2.6 collective-permute-start.51
  215.8 4.5 %collective-permute-done.50.refs_10_ = bf16[256,512]{1,0:T(8,128)(2,1)S(1)} collective-permute-done((bf16[256,512]{1,0:T(8,128)(2,1)S(1)}, bf16[256,512]{1,0:T(8,128)(2,1)S(1)}, u32[]{:S(2)}, u32[]{:S(2)}) %collective-permute-start.50) | collective-permute-done | bytes 262176 | tf_op jit(solution)/shard_map/ppermute | solution.py:35
  225.2 12.2 %projected.3 = (bf16[528,512]{1,0:T(8,128)(2,1)}, bf16[512,512]{1,0:T(8,128)(2,1)}) custom-call(s32[1]{0:T(128)} %bitcast.3.refs_0_.rank, s32[1]{0:T(128)} %bitcast.4.refs_1_, f32[2,4096]{1,0:T(2,128)} %refs_2_.3, bf16[8,16,512]{2,1,0:T(8,128)(2,1)} %maximum_maximum_fusion.1.refs_3_, bf16[256,512]{1,0:T(8,128)(2,1)} %copy-done.14, ...), custom_call_target="tpu_custom_call" | custom-call | flops 4429185024 | bytes 8388608 | tf_op jit(solution)/shard_map/projected/pallas_call | solution.py:261
  238.5 5.9 %scan.3 = (f32[512,512]{1,0:T(8,128)S(1)}, f32[512,512]{1,0:T(8,128)S(1)}, f32[512,512]{1,0:T(8,128)S(1)}, f32[4,8,512]{2,1,0:T(8,128)S(1)}, f32[16,4,512]{2,1,0:T(4,128)S(1)}) custom-call(s32[1]{0:T(128)} %bitcast.3.refs_0_.rank, bf16[528,512]{1,0:T(8,128)(2,1)S(1)} %copy-done.6, f32[2,4,4096]{2,1,0:T(4,128)S(1)} %copy-done.7, f32[2,2,4096]{2,1,0:T(2,128)S(1)} %copy-done.8, ...), custom_call_target="tpu_custom_call" | custom-call | flops 10000000000 | bytes 4000000 | tf_op jit(solution)/shard_map/scan/pallas_call | solution.py:372
  244.4 13.7 %all_to_all.21.refs_2_ = f32[16,4,512]{2,1,0:T(4,128)S(1)} all-to-all(f32[16,4,512]{2,1,0:T(4,128)S(1)} %get-tuple-element.57), channel_id=1, replica_groups=mesh['sp'=16,'tp'=8] {'sp'}, dimensions={0} | all-to-all | bytes 262144 | tf_op jit(solution)/shard_map/all_to_all | solution.py:539
  258.1 5.3 %given.3 = (bf16[512,512]{1,0:T(8,128)(2,1)S(1)}, bf16[512,512]{1,0:T(8,128)(2,1)S(1)}, bf16[3,512,512]{2,1,0:T(8,128)(2,1)}, bf16[4,512,512]{2,1,0:T(8,128)(2,1)}) custom-call(s32[1]{0:T(128)} %bitcast.3.refs_0_.rank, s32[1]{0:T(128)} %bitcast.4.refs_1_, f32[16,4,512]{2,1,0:T(4,128)S(1)} %all_to_all.21.refs_2_, f32[512,512]{1,0:T(8,128)S(1)} %get-tuple-element.58.refs_3_, ...), custom_call_target="tpu_custom_call" | custom-call | flops 1073741824 | bytes 2097152 | tf_op jit(solution)/shard_map/given/pallas_call | solution.py:466
  269.3 2.7 collective-permute-start.66
  273.6 4.3 %collective-permute-done.62 = bf16[256,512]{1,0:T(8,128)(2,1)S(1)} collective-permute-done((bf16[256,512]{1,0:T(8,128)(2,1)S(1)}, bf16[256,512]{1,0:T(8,128)(2,1)S(1)}, u32[]{:S(2)}, u32[]{:S(2)}) %collective-permute-start.62) | collective-permute-done | bytes 262176 | tf_op jit(solution)/shard_map/ppermute | solution.py:35
  283.6 5.6 %collective-permute-done.63 = bf16[256,512]{1,0:T(8,128)(2,1)S(1)} collective-permute-done((bf16[256,512]{1,0:T(8,128)(2,1)S(1)}, bf16[256,512]{1,0:T(8,128)(2,1)S(1)}, u32[]{:S(2)}, u32[]{:S(2)}) %collective-permute-start.63) | collective-permute-done | bytes 262176 | tf_op jit(solution)/shard_map/ppermute | solution.py:35
  (289 shorter events, 97.5 us)
Async XLA Ops:
  6.5 149.2 %all-gather.3.cloned.1.call-start = ((), (), s32[]{:S(2)}) async-start(), calls=%async_computation.4 | async-start | bytes 4456448 | tf_op jit(solution)/shard_map/all_gather | solution.py:527
  8.4 216.8 %all-gather.5.cloned.1.call-start = ((), (), s32[]{:S(2)}) async-start(), calls=%async_computation.5 | async-start | bytes 13369344 | tf_op jit(solution)/shard_map/all_gather | solution.py:529
  11.5 10.5 %all-to-all-start = ((bf16[8,4,512]{2,1,0:T(4,128)(2,1)}), bf16[8,4,512]{2,1,0:T(4,128)(2,1)S(1)}, u32[]{:S(2)}, u32[]{:S(2)}) async-start(bf16[8,4,512]{2,1,0:T(4,128)(2,1)} %broadcast_in_dim.4), calls=%async_computation | async-start | bytes 65536 | tf_op jit(solution)/shard_map/all_to_all | solution.py:52
  17.3 16.3 %collective-permute-start.17 = (bf16[256,512]{1,0:T(8,128)(2,1)S(1)}, bf16[256,512]{1,0:T(8,128)(2,1)S(1)}, u32[]{:S(2)}, u32[]{:S(2)}) collective-permute-start(bf16[256,512]{1,0:T(8,128)(2,1)S(1)} %pad_maximum_fusion.3), channel_id=1, source_target_pairs={{0,24},{8,0},{16,8},{24,16},{32,56},{40,32},{48,40},{56,48},{64,88... | collective-permute-start | bytes 786440 | tf_op jit(solution)/shard_map/ppermute | solution.py:83
  20.1 15.9 %collective-permute-start.16 = (bf16[256,512]{1,0:T(8,128)(2,1)S(1)}, bf16[256,512]{1,0:T(8,128)(2,1)S(1)}, u32[]{:S(2)}, u32[]{:S(2)}) collective-permute-start(bf16[256,512]{1,0:T(8,128)(2,1)S(1)} %pad_maximum_fusion.3), channel_id=1, source_target_pairs={{0,8},{8,16},{16,24},{24,0},{32,40},{40,48},{48,56},{56,32},{64,72... | collective-permute-start | bytes 786440 | tf_op jit(solution)/shard_map/ppermute | solution.py:83
  22.0 11.3 %collective-permute-start = (bf16[8,2,512]{2,1,0:T(2,128)(2,1)S(1)}, bf16[8,2,512]{2,1,0:T(2,128)(2,1)S(1)}, u32[]{:S(2)}, u32[]{:S(2)}) collective-permute-start(bf16[8,2,512]{2,1,0:T(2,128)(2,1)S(1)} %get-tuple-element.103), channel_id=1, source_target_pairs={{0,8},{8,16},{16,24},{24,32},{32,40},{40,48},{48,56},{56,64},{64,7... | collective-permute-start | bytes 49160 | tf_op jit(solution)/shard_map/ppermute | solution.py:53
  26.5 12.9 %collective-permute-start.27 = (bf16[256,512]{1,0:T(8,128)(2,1)S(1)}, bf16[256,512]{1,0:T(8,128)(2,1)S(1)}, u32[]{:S(2)}, u32[]{:S(2)}) collective-permute-start(bf16[256,512]{1,0:T(8,128)(2,1)S(1)} %pad_maximum_fusion.4), channel_id=1, source_target_pairs={{0,96},{8,104},{16,112},{24,120},{32,0},{40,8},{48,16},{56,24},{64... | collective-permute-start | bytes 786440 | tf_op jit(solution)/shard_map/ppermute | solution.py:83
  33.3 10.2 %collective-permute-start.2 = (bf16[256,512]{1,0:T(8,128)(2,1)S(1)}, bf16[256,512]{1,0:T(8,128)(2,1)S(1)}, u32[]{:S(2)}, u32[]{:S(2)}) collective-permute-start(bf16[256,512]{1,0:T(8,128)(2,1)S(1)} %get-tuple-element.96.refs_4_), channel_id=1, source_target_pairs={{0,2},{1,3},{2,4},{3,5},{4,6},{5,7},{6,0},{7,1},{8,10},{9,11},{10,... | collective-permute-start | bytes 786440 | tf_op jit(solution)/shard_map/ppermute | solution.py:35
  33.6 11.7 %collective-permute-start.5 = (bf16[256,512]{1,0:T(8,128)(2,1)S(1)}, bf16[256,512]{1,0:T(8,128)(2,1)S(1)}, u32[]{:S(2)}, u32[]{:S(2)}) collective-permute-start(bf16[256,512]{1,0:T(8,128)(2,1)S(1)} %get-tuple-element.95.refs_5_), channel_id=1, source_target_pairs={{0,6},{1,7},{2,0},{3,1},{4,2},{5,3},{6,4},{7,5},{8,14},{9,15},{10,... | collective-permute-start | bytes 786440 | tf_op jit(solution)/shard_map/ppermute | solution.py:35
  36.0 10.4 %collective-permute-start.3 = (bf16[256,512]{1,0:T(8,128)(2,1)S(1)}, bf16[256,512]{1,0:T(8,128)(2,1)S(1)}, u32[]{:S(2)}, u32[]{:S(2)}) collective-permute-start(bf16[256,512]{1,0:T(8,128)(2,1)S(1)} %get-tuple-element.95.refs_5_), channel_id=1, source_target_pairs={{0,2},{1,3},{2,4},{3,5},{4,6},{5,7},{6,0},{7,1},{8,10},{9,11},{10,... | collective-permute-start | bytes 786440 | tf_op jit(solution)/shard_map/ppermute | solution.py:35
  60.9 18.5 %collective-permute-start.20 = (bf16[512,512]{1,0:T(8,128)(2,1)S(1)}, bf16[512,512]{1,0:T(8,128)(2,1)S(1)}, u32[]{:S(2)}, u32[]{:S(2)}) collective-permute-start(bf16[512,512]{1,0:T(8,128)(2,1)S(1)} %pad_maximum_fusion.1.refs_20_), channel_id=1, source_target_pairs={{0,32},{8,40},{16,48},{24,56},{32,64},{40,72},{48,80},{56,88},{64,... | collective-permute-start | bytes 1572872 | tf_op jit(solution)/shard_map/ppermute | solution.py:83
  62.5 19.3 %collective-permute-start.30 = (bf16[512,512]{1,0:T(8,128)(2,1)S(1)}, bf16[512,512]{1,0:T(8,128)(2,1)S(1)}, u32[]{:S(2)}, u32[]{:S(2)}) collective-permute-start(bf16[512,512]{1,0:T(8,128)(2,1)S(1)} %pad_maximum_fusion.2.refs_28_), channel_id=1, source_target_pairs={{0,8},{8,16},{16,24},{24,0},{32,40},{40,48},{48,56},{56,32},{64,72... | collective-permute-start | bytes 1572872 | tf_op jit(solution)/shard_map/ppermute | solution.py:83
  62.5 19.2 %collective-permute-start.22 = (bf16[512,512]{1,0:T(8,128)(2,1)S(1)}, bf16[512,512]{1,0:T(8,128)(2,1)S(1)}, u32[]{:S(2)}, u32[]{:S(2)}) collective-permute-start(bf16[512,512]{1,0:T(8,128)(2,1)S(1)} %pad_maximum_fusion.1.refs_20_), channel_id=1, source_target_pairs={{0,96},{8,104},{16,112},{24,120},{32,0},{40,8},{48,16},{56,24},{64... | collective-permute-start | bytes 1572872 | tf_op jit(solution)/shard_map/ppermute | solution.py:83
  64.8 18.0 %collective-permute-start.32 = (bf16[512,512]{1,0:T(8,128)(2,1)S(1)}, bf16[512,512]{1,0:T(8,128)(2,1)S(1)}, u32[]{:S(2)}, u32[]{:S(2)}) collective-permute-start(bf16[512,512]{1,0:T(8,128)(2,1)S(1)} %pad_maximum_fusion.2.refs_28_), channel_id=1, source_target_pairs={{0,24},{8,0},{16,8},{24,16},{32,56},{40,32},{48,40},{56,48},{64,88... | collective-permute-start | bytes 1572872 | tf_op jit(solution)/shard_map/ppermute | solution.py:83
  71.2 17.8 %collective-permute-start.23 = (bf16[512,512]{1,0:T(8,128)(2,1)S(1)}, bf16[512,512]{1,0:T(8,128)(2,1)}, u32[]{:S(2)}, u32[]{:S(2)}) collective-permute-start(bf16[512,512]{1,0:T(8,128)(2,1)S(1)} %constant_dynamic-update-slice_fusion.refs_21_), channel_id=1, source_target_pairs={{0,96},{8,104},{16,112},{24,120},{32,0},{40,8},{48,16},{56,24},{64... | collective-permute-start | bytes 1572872 | tf_op jit(solution)/shard_map/ppermute | solution.py:83
  79.3 16.3 %collective-permute-start.33 = (bf16[512,512]{1,0:T(8,128)(2,1)S(1)}, bf16[512,512]{1,0:T(8,128)(2,1)}, u32[]{:S(2)}, u32[]{:S(2)}) collective-permute-start(bf16[512,512]{1,0:T(8,128)(2,1)S(1)} %constant_dynamic-update-slice_fusion.3.refs_29_), channel_id=1, source_target_pairs={{0,24},{8,0},{16,8},{24,16},{32,56},{40,32},{48,40},{56,48},{64,88... | collective-permute-start | bytes 1572872 | tf_op jit(solution)/shard_map/ppermute | solution.py:83
  81.7 16.5 %collective-permute-start.21 = (bf16[512,512]{1,0:T(8,128)(2,1)S(1)}, bf16[512,512]{1,0:T(8,128)(2,1)S(1)}, u32[]{:S(2)}, u32[]{:S(2)}) collective-permute-start(bf16[512,512]{1,0:T(8,128)(2,1)S(1)} %constant_dynamic-update-slice_fusion.refs_21_), channel_id=1, source_target_pairs={{0,32},{8,40},{16,48},{24,56},{32,64},{40,72},{48,80},{56,88},{64,... | collective-permute-start | bytes 1572872 | tf_op jit(solution)/shard_map/ppermute | solution.py:83
  84.0 20.8 %collective-permute-start.31 = (bf16[512,512]{1,0:T(8,128)(2,1)S(1)}, bf16[512,512]{1,0:T(8,128)(2,1)S(1)}, u32[]{:S(2)}, u32[]{:S(2)}) collective-permute-start(bf16[512,512]{1,0:T(8,128)(2,1)S(1)} %constant_dynamic-update-slice_fusion.3.refs_29_), channel_id=1, source_target_pairs={{0,8},{8,16},{16,24},{24,0},{32,40},{40,48},{48,56},{56,32},{64,72... | collective-permute-start | bytes 1572872 | tf_op jit(solution)/shard_map/ppermute | solution.py:83
  84.4 35.0 %collective-permute-start.24 = (bf16[512,512]{1,0:T(8,128)(2,1)S(1)}, bf16[512,512]{1,0:T(8,128)(2,1)}, u32[]{:S(2)}, u32[]{:S(2)}) collective-permute-start(bf16[512,512]{1,0:T(8,128)(2,1)S(1)} %collective-permute-done.20.refs_22_), channel_id=1, source_target_pairs={{0,32},{8,40},{16,48},{24,56},{32,64},{40,72},{48,80},{56,88},{64,... | collective-permute-start | bytes 1572872 | tf_op jit(solution)/shard_map/ppermute | solution.py:83
  89.1 33.3 %collective-permute-start.34 = (bf16[512,512]{1,0:T(8,128)(2,1)S(1)}, bf16[512,512]{1,0:T(8,128)(2,1)}, u32[]{:S(2)}, u32[]{:S(2)}) collective-permute-start(bf16[512,512]{1,0:T(8,128)(2,1)S(1)} %collective-permute-done.30.refs_30_), channel_id=1, source_target_pairs={{0,8},{8,16},{16,24},{24,0},{32,40},{40,48},{48,56},{56,32},{64,72... | collective-permute-start | bytes 1572872 | tf_op jit(solution)/shard_map/ppermute | solution.py:83
  95.6 26.7 %collective-permute-start.25 = (bf16[512,512]{1,0:T(8,128)(2,1)}, bf16[512,512]{1,0:T(8,128)(2,1)}, u32[]{:S(2)}, u32[]{:S(2)}) collective-permute-start(bf16[512,512]{1,0:T(8,128)(2,1)} %collective-permute-done.23.refs_25_), channel_id=1, source_target_pairs={{0,96},{8,104},{16,112},{24,120},{32,0},{40,8},{48,16},{56,24},{64... | collective-permute-start | bytes 1572872 | tf_op jit(solution)/shard_map/ppermute | solution.py:83
  98.2 24.1 %collective-permute-start.35 = (bf16[512,512]{1,0:T(8,128)(2,1)}, bf16[512,512]{1,0:T(8,128)(2,1)}, u32[]{:S(2)}, u32[]{:S(2)}) collective-permute-start(bf16[512,512]{1,0:T(8,128)(2,1)} %collective-permute-done.33.refs_33_), channel_id=1, source_target_pairs={{0,24},{8,0},{16,8},{24,16},{32,56},{40,32},{48,40},{56,48},{64,88... | collective-permute-start | bytes 1572872 | tf_op jit(solution)/shard_map/ppermute | solution.py:83
  171.4 11.0 %collective-permute-start.40 = (bf16[256,512]{1,0:T(8,128)(2,1)S(1)}, bf16[256,512]{1,0:T(8,128)(2,1)S(1)}, u32[]{:S(2)}, u32[]{:S(2)}) collective-permute-start(bf16[256,512]{1,0:T(8,128)(2,1)S(1)} %get-tuple-element.84), channel_id=1, source_target_pairs={{0,6},{1,7},{2,0},{3,1},{4,2},{5,3},{6,4},{7,5},{8,14},{9,15},{10,... | collective-permute-start | bytes 786440 | tf_op jit(solution)/shard_map/ppermute | solution.py:35
  172.7 10.2 %collective-permute-start.41 = (bf16[256,512]{1,0:T(8,128)(2,1)S(1)}, bf16[256,512]{1,0:T(8,128)(2,1)S(1)}, u32[]{:S(2)}, u32[]{:S(2)}) collective-permute-start(bf16[256,512]{1,0:T(8,128)(2,1)S(1)} %get-tuple-element.83), channel_id=1, source_target_pairs={{0,2},{1,3},{2,4},{3,5},{4,6},{5,7},{6,0},{7,1},{8,10},{9,11},{10,... | collective-permute-start | bytes 786440 | tf_op jit(solution)/shard_map/ppermute | solution.py:35
  177.6 10.9 %collective-permute-start.39 = (bf16[256,512]{1,0:T(8,128)(2,1)S(1)}, bf16[256,512]{1,0:T(8,128)(2,1)S(1)}, u32[]{:S(2)}, u32[]{:S(2)}) collective-permute-start(bf16[256,512]{1,0:T(8,128)(2,1)S(1)} %get-tuple-element.82), channel_id=1, source_target_pairs={{0,2},{1,3},{2,4},{3,5},{4,6},{5,7},{6,0},{7,1},{8,10},{9,11},{10,... | collective-permute-start | bytes 786440 | tf_op jit(solution)/shard_map/ppermute | solution.py:35
  189.7 10.8 %all-to-all-start.2 = ((bf16[8,4,512]{2,1,0:T(4,128)(2,1)}), bf16[8,4,512]{2,1,0:T(4,128)(2,1)S(1)}, u32[]{:S(2)}, u32[]{:S(2)}) async-start(bf16[8,4,512]{2,1,0:T(4,128)(2,1)} %broadcast_in_dim.5), calls=%async_computation.2 | async-start | bytes 65536 | tf_op jit(solution)/shard_map/all_to_all | solution.py:52
  195.2 16.4 %collective-permute-start.46 = (bf16[256,512]{1,0:T(8,128)(2,1)S(1)}, bf16[256,512]{1,0:T(8,128)(2,1)S(1)}, u32[]{:S(2)}, u32[]{:S(2)}) collective-permute-start(bf16[256,512]{1,0:T(8,128)(2,1)S(1)} %get-tuple-element.74.refs_4_), channel_id=1, source_target_pairs={{0,2},{1,3},{2,4},{3,5},{4,6},{5,7},{6,0},{7,1},{8,10},{9,11},{10,... | collective-permute-start | bytes 786440 | tf_op jit(solution)/shard_map/ppermute | solution.py:35
  196.5 15.1 %collective-permute-start.49 = (bf16[256,512]{1,0:T(8,128)(2,1)S(1)}, bf16[256,512]{1,0:T(8,128)(2,1)S(1)}, u32[]{:S(2)}, u32[]{:S(2)}) collective-permute-start(bf16[256,512]{1,0:T(8,128)(2,1)S(1)} %get-tuple-element.73.refs_5_), channel_id=1, source_target_pairs={{0,6},{1,7},{2,0},{3,1},{4,2},{5,3},{6,4},{7,5},{8,14},{9,15},{10,... | collective-permute-start | bytes 786440 | tf_op jit(solution)/shard_map/ppermute | solution.py:35
  197.8 13.8 %collective-permute-start.47 = (bf16[256,512]{1,0:T(8,128)(2,1)S(1)}, bf16[256,512]{1,0:T(8,128)(2,1)S(1)}, u32[]{:S(2)}, u32[]{:S(2)}) collective-permute-start(bf16[256,512]{1,0:T(8,128)(2,1)S(1)} %get-tuple-element.73.refs_5_), channel_id=1, source_target_pairs={{0,2},{1,3},{2,4},{3,5},{4,6},{5,7},{6,0},{7,1},{8,10},{9,11},{10,... | collective-permute-start | bytes 786440 | tf_op jit(solution)/shard_map/ppermute | solution.py:35
  198.0 16.3 %collective-permute-start.48 = (bf16[256,512]{1,0:T(8,128)(2,1)S(1)}, bf16[256,512]{1,0:T(8,128)(2,1)S(1)}, u32[]{:S(2)}, u32[]{:S(2)}) collective-permute-start(bf16[256,512]{1,0:T(8,128)(2,1)S(1)} %get-tuple-element.74.refs_4_), channel_id=1, source_target_pairs={{0,6},{1,7},{2,0},{3,1},{4,2},{5,3},{6,4},{7,5},{8,14},{9,15},{10,... | collective-permute-start | bytes 786440 | tf_op jit(solution)/shard_map/ppermute | solution.py:35
  272.1 10.5 %collective-permute-start.64 = (bf16[256,512]{1,0:T(8,128)(2,1)S(1)}, bf16[256,512]{1,0:T(8,128)(2,1)S(1)}, u32[]{:S(2)}, u32[]{:S(2)}) collective-permute-start(bf16[256,512]{1,0:T(8,128)(2,1)S(1)} %get-tuple-element.80), channel_id=1, source_target_pairs={{0,6},{1,7},{2,0},{3,1},{4,2},{5,3},{6,4},{7,5},{8,14},{9,15},{10,... | collective-permute-start | bytes 786440 | tf_op jit(solution)/shard_map/ppermute | solution.py:35
  278.2 11.0 %collective-permute-start.63 = (bf16[256,512]{1,0:T(8,128)(2,1)S(1)}, bf16[256,512]{1,0:T(8,128)(2,1)S(1)}, u32[]{:S(2)}, u32[]{:S(2)}) collective-permute-start(bf16[256,512]{1,0:T(8,128)(2,1)S(1)} %get-tuple-element.78), channel_id=1, source_target_pairs={{0,2},{1,3},{2,4},{3,5},{4,6},{5,7},{6,0},{7,1},{8,10},{9,11},{10,... | collective-permute-start | bytes 786440 | tf_op jit(solution)/shard_map/ppermute | solution.py:35
  (100 other events, 1289.9 us)
Sparse Core Ops, SparseCore 0:
  9.5 61.6 all-gather.2
  73.4 106.8 all-gather.4
